TPU v7x, 512 devices: a whole 4x8x8 slice. The times are simulated.
512 devices in a mesh: sp: 128 (over z, y, core), tp: 4 (over x).
Axes of the slice: x: 4, y: 8, z: 8, core: 2. Of those that a mesh axis runs over, the one named last changes fastest.
Arguments:
- activations: bfloat16 [65536, 2048], P('sp', 'tp'), may hold values from -250 to 250
- norm_gain: bfloat16 [2048], P('tp'), may hold values from 0.099609375 to 1.8984375
- pool_weight: bfloat16 [2048, 1024], P('sp', 'tp'), may hold values from -0.125 to 0.125
- gate_weight: bfloat16 [2048, 1024], P('sp', 'tp'), may hold values from -0.125 to 0.125
- value_weight: bfloat16 [2048, 1024], P('sp', 'tp'), may hold values from -0.125 to 0.125
- key_weight: bfloat16 [2048, 256], P('sp', 'tp'), may hold values from -0.125 to 0.125
- read_weight: bfloat16 [2048, 256], P('sp', 'tp'), may hold values from -0.125 to 0.125
- step_weight: bfloat16 [2048, 16], P('sp', 'tp'), may hold values from -0.125 to 0.125
- pool_mix: bfloat16 [4, 256, 256], P('tp'), may hold values from -0.375 to 0.375
- pool_scale: float32 [1024], P('tp'), may hold values from 0.1 to 1.9
- taps_value: float32 [4, 1024], P(None, 'tp'), may hold values from -3 to 3
- taps_key: float32 [4, 256], P(None, 'tp'), may hold values from -3 to 3
- taps_read: float32 [4, 256], P(None, 'tp'), may hold values from -3 to 3
- step_bias: float32 [16], P('tp'), may hold values from -1 to 1
- decay_log: float32 [16], P('tp')
- decay_extra: float32 [65536, 16], P('sp', 'tp'), may hold values from -1 to 0
- skip_scale: float32 [16], P('tp'), may hold values from 0.5 to 2
- state_gain: float32 [1024], P('tp'), may hold values from 0.1 to 1.9
- out_pool_weight: bfloat16 [1024, 2048], P('tp', 'sp'), may hold values from -0.125 to 0.125
- out_state_weight: bfloat16 [1024, 2048], P('tp', 'sp'), may hold values from -0.125 to 0.125
Outputs:
- mixed: bfloat16 [65536, 2048], P('sp', 'tp')
All inputs are finite; a program needn't handle non-finite values.
Results may differ from a plain program's by a relative error of at most 0.007.
Values may be sent and summed in bfloat16 or wider, within the bound.
No kernel may reach another device: no remote copies, remote signals or barrier semaphores. Data moves between devices by JAX's collectives and lax.ppermute only.
A program may use at most 64 MiB of HBM per device.

v0:
```python
import jax
import jax.numpy as jnp
from jax import lax
from jax.sharding import Mesh
from jax.sharding import PartitionSpec as P

D = 2048
SSM_STATE = 64
POOL_GROUPS = 4
SCAN_BLOCK = 128
MIX_W = 1024
SP = ("sp_0", "sp_1", "sp_2")


EPSILON = 1e-06
HIGH = lax.Precision.HIGHEST


def sent_to_all(array, axis):
    copies = jnp.broadcast_to(array, (lax.axis_size(axis), *array.shape))
    return lax.all_to_all(copies, axis, split_axis=0, concat_axis=0, tiled=True)


def over_copies(array, axis):
    everything = sent_to_all(array, axis)
    return jnp.sum(everything, axis=0)


def laid_out(pieces, dim):
    pieces = jnp.moveaxis(pieces, 0, dim)
    shape = pieces.shape
    return pieces.reshape(*shape[:dim], shape[dim] * shape[dim + 1], *shape[dim + 2 :])


def collect(array, axis, dim):
    return laid_out(sent_to_all(array, axis), dim)


def shifted(value, axis, steps):
    count = lax.axis_size(axis)
    leading, last = (max(0, -steps), min(count, count - steps))
    return lax.ppermute(value, axis, [(source, source + steps) for source in range(leading, last)])


def neutral_like(array, identity):
    return jax.tree.map(
        lambda part, zero: jnp.zeros_like(part) + jnp.asarray(zero, part.dtype), array, identity
    )


def all_in_one(array, axis):
    leaves = jax.tree.leaves(array)
    order = sorted(range(len(leaves)), key=lambda k: -leaves[k].size)
    width = (1, *leaves[order[0]].shape)[-1]
    lines = [
        jnp.pad(leaves[k].reshape(-1), (0, -leaves[k].size % width)).reshape(-1, width)
        for k in order
    ]
    both, at, found = (lax.all_gather(jnp.concatenate(lines), axis), 0, {})
    for k, line in zip(order, lines):
        section = both[:, at : at + len(line)].reshape(len(both), -1)
        found[k] = section[:, : leaves[k].size].reshape(-1, *leaves[k].shape)
        at += len(line)
    numbers = iter(range(len(leaves)))
    return jax.tree.map(lambda _: found[next(numbers)], array)


def prefix_by_axis(array, axes, combine, identity):
    before = start = neutral_like(array, identity)
    running = array
    for axis in reversed(axes):
        count, place = (lax.axis_size(axis), lax.axis_index(axis))
        pieces = all_in_one(running, axis)
        inside, running = (start, start)
        for k in range(count):
            passed = k < place
            running = combine(running, jax.tree.map(lambda part: part[k], pieces))
            inside = jax.tree.map(lambda new, old: jnp.where(passed, new, old), running, inside)
        before = combine(inside, before)
    return before


def split_up(array, dim, count):
    before, after = (array.shape[:dim], array.shape[dim + 1 :])
    return jnp.moveaxis(array.reshape(*before, count, -1, *after), dim, 0)


def summed_on_arrival(array, axis, dim):
    pieces = split_up(array, dim, lax.axis_size(axis))
    arrived = lax.all_to_all(pieces, axis, split_axis=0, concat_axis=0, tiled=True)
    return arrived.astype(jnp.float32).sum(axis=0)


def backward_kernel(extended, taps):
    width = taps.shape[0]
    length = extended.shape[0] - (width - 1)
    widened_rows = extended.astype(jnp.float32)
    total = jnp.zeros((length, extended.shape[1]), jnp.float32)
    for offset in range(width):
        total = total + taps[offset][None, :] * widened_rows[offset : offset + length]
    return jax.nn.silu(total).astype(jnp.bfloat16)


def combine_states(preceding_token, later):
    return (preceding_token[0] * later[0], preceding_token[1] * later[0][:, None, None] + later[1])


def local(
    activations,
    norm_gain,
    pool_weight,
    gate_weight,
    value_weight,
    key_weight,
    read_weight,
    step_weight,
    pool_mix,
    pool_scale,
    taps_value,
    taps_key,
    taps_read,
    step_bias,
    decay_log,
    decay_extra,
    skip_scale,
    state_gain,
    out_pool_weight,
    out_state_weight,
):
    length = activations.shape[0]
    cluster_span = pool_weight.shape[1]
    local_mix = gate_weight.shape[1]
    local_state = key_weight.shape[1]
    local_heads = step_weight.shape[1]
    joined = jnp.concatenate(
        [pool_weight, gate_weight, value_weight, key_weight, read_weight, step_weight], axis=1
    )
    in_weight = lax.all_gather(joined, SP, axis=0, tiled=True)
    values = activations.astype(jnp.float32)
    squares = over_copies(jnp.sum(values * values, axis=-1), "tp")
    normed = (
        values * lax.rsqrt(squares / D + EPSILON)[:, None] * norm_gain.astype(jnp.float32)
    ).astype(jnp.bfloat16)
    projected = jnp.dot(collect(normed, "tp", 1), in_weight, preferred_element_type=jnp.float32)
    column = 0
    pool_in = projected[:, column : column + cluster_span].astype(jnp.bfloat16)
    column = column + cluster_span
    gate_in = projected[:, column : column + local_mix].astype(jnp.bfloat16)
    column = column + local_mix
    raw_value = projected[:, column : column + local_mix].astype(jnp.bfloat16)
    column = column + local_mix
    raw_key = projected[:, column : column + local_state].astype(jnp.bfloat16)
    column = column + local_state
    raw_read = projected[:, column : column + local_state].astype(jnp.bfloat16)
    column = column + local_state
    step_raw = projected[:, column : column + local_heads]
    raw_joined = jnp.concatenate([raw_value, raw_key, raw_read], axis=1)
    reach = 2**POOL_GROUPS - 1
    width = taps_value.shape[0]
    prior_pool, prior_joined = shifted(
        (pool_in[length - reach :], raw_joined[length - width + 1 :]), SP, 1
    )
    group = lax.axis_index("tp")
    running = jnp.concatenate([prior_pool, pool_in], axis=0).astype(jnp.float32)
    levels = []
    for level in range(POOL_GROUPS):
        stride = 2**level
        running = running[stride:] + running[:-stride]
        levels.append(running[running.shape[0] - length :])
    window_sum = lax.dynamic_index_in_dim(jnp.stack(levels), group, 0, keepdims=False)
    window = jnp.exp2((group + 1).astype(jnp.float32))
    position = (lax.axis_index(SP) * length + jnp.arange(length, dtype=jnp.int32)).astype(
        jnp.float32
    )
    counts = jnp.minimum(position + 1.0, window)
    pooled = (window_sum / counts[:, None] - pool_in.astype(jnp.float32)).astype(jnp.bfloat16)
    pool_out = (
        jnp.dot(pooled, pool_mix[0], preferred_element_type=jnp.float32) * pool_scale
    ).astype(jnp.bfloat16)
    all_taps = jnp.concatenate([taps_value, taps_key, taps_read], axis=1)
    convolved = backward_kernel(jnp.concatenate([prior_joined, raw_joined], axis=0), all_taps)
    head_value = convolved[:, :local_mix]
    key_vectors = convolved[:, local_mix : local_mix + local_state]
    read_vectors = convolved[:, local_mix + local_state :]
    head_dim = local_mix // local_heads
    groups_here = local_state // SSM_STATE
    repeat = local_heads // groups_here
    blocks = length // SCAN_BLOCK
    step_size = jax.nn.softplus(step_raw + step_bias)
    log_decay = -jnp.exp(decay_log) * step_size + decay_extra
    value_heads = head_value.astype(jnp.float32).reshape(length, local_heads, head_dim)
    value_blocks = value_heads.reshape(blocks, SCAN_BLOCK, local_heads, head_dim)
    key_blocks = jnp.repeat(
        key_vectors.astype(jnp.float32).reshape(length, groups_here, SSM_STATE), repeat, axis=1
    ).reshape(blocks, SCAN_BLOCK, local_heads, SSM_STATE)
    read_blocks = jnp.repeat(
        read_vectors.astype(jnp.float32).reshape(length, groups_here, SSM_STATE), repeat, axis=1
    ).reshape(blocks, SCAN_BLOCK, local_heads, SSM_STATE)
    step_blocks = step_size.reshape(blocks, SCAN_BLOCK, local_heads)
    running_decay = jnp.cumsum(log_decay.reshape(blocks, SCAN_BLOCK, local_heads), axis=1)
    lower = jnp.arange(SCAN_BLOCK)[:, None] >= jnp.arange(SCAN_BLOCK)[None, :]
    gaps = jnp.where(
        lower[None, :, :, None],
        running_decay[:, :, None, :] - running_decay[:, None, :, :],
        -jnp.inf,
    )
    weights = jnp.einsum("blhn,bshn->blsh", read_blocks, key_blocks, precision=HIGH) * jnp.exp(gaps)
    scaled_value = value_blocks * step_blocks[..., None]
    inner = jnp.einsum("blsh,bshp->blhp", weights, scaled_value, precision=HIGH)
    block_ends = running_decay[:, -1, :]
    trailing = jnp.exp(block_ends[:, None, :] - running_decay)
    fresh = jnp.einsum("bshn,bsh,bshp->bhpn", key_blocks, trailing, scaled_value, precision=HIGH)

    def advance(carry, inputs):
        block_decay, block_state = inputs
        return (carry * block_decay[:, None, None] + block_state, carry)

    local_total, prefix = lax.scan(
        advance,
        jnp.zeros((local_heads, head_dim, SSM_STATE), jnp.float32),
        (jnp.exp(block_ends), fresh),
    )
    offsets = jnp.cumsum(block_ends, axis=0) - block_ends
    device_decay = jnp.exp(offsets[-1] + block_ends[-1])
    incoming_decay, incoming = prefix_by_axis(
        (device_decay, local_total),
        SP,
        combine_states,
        (jnp.ones_like(device_decay), jnp.zeros_like(local_total)),
    )
    from_device = running_decay + offsets[:, None, :]
    local_off = (
        jnp.einsum("blhn,bhpn->blhp", read_blocks, prefix, precision=HIGH)
        * jnp.exp(running_decay)[..., None]
    )
    far_off = (
        jnp.einsum("blhn,hpn->blhp", read_blocks, incoming, precision=HIGH)
        * jnp.exp(from_device)[..., None]
    )
    scan_out = (inner + local_off + far_off).reshape(length, local_heads, head_dim) + skip_scale[
        None, :, None
    ] * value_heads
    gated = scan_out.reshape(length, local_mix) * jax.nn.silu(gate_in.astype(jnp.float32))
    gate_squares = over_copies(jnp.sum(gated * gated, axis=-1), "tp")
    state_out = (gated * lax.rsqrt(gate_squares / MIX_W + EPSILON)[:, None] * state_gain).astype(
        jnp.bfloat16
    )
    branch_rows = jnp.concatenate([pool_out, state_out], axis=1)
    out_weight = jnp.concatenate([out_pool_weight, out_state_weight], axis=0)
    terms = jnp.dot(
        branch_rows,
        lax.all_gather(out_weight, SP, axis=1, tiled=True),
        preferred_element_type=jnp.float32,
    )
    result = summed_on_arrival(terms.astype(jnp.bfloat16), "tp", 1)
    return result.astype(jnp.bfloat16)


def solution(mesh):
    torus = Mesh(mesh.devices.reshape(8, 8, 2, mesh.shape["tp"]), ("sp_0", "sp_1", "sp_2", "tp"))
    placed = (
        P(SP, "tp"),
        P("tp"),
        P(SP, "tp"),
        P(SP, "tp"),
        P(SP, "tp"),
        P(SP, "tp"),
        P(SP, "tp"),
        P(SP, "tp"),
        P("tp", None, None),
        P("tp"),
        P(None, "tp"),
        P(None, "tp"),
        P(None, "tp"),
        P("tp"),
        P("tp"),
        P(SP, "tp"),
        P("tp"),
        P("tp"),
        P("tp", SP),
        P("tp", SP),
    )
    return jax.shard_map(local, mesh=torus, in_specs=placed, out_specs=P(SP, "tp"), check_vma=False)
```

profile of v0, /device:TPU:8, one launch (start us, length us, event | category | flops | bytes accessed | tf_op | source)
XLA Modules:
  0.0 253.0 jit_solution(12574823793756148212)
XLA Ops:
  6.5 0.8 copy.224
  7.3 1.5 concatenate.30
  8.8 1.2 fusion.7
  10.6 4.3 %all-to-all-start = ((f32[4,1,512]{2,1,0:T(1,128)}), f32[4,1,512]{2,1,0:T(1,128)S(1)}, u32[]{:S(2)}, u32[]{:S(2)}) async-start(f32[4,1,512]{2,1,0:T(1,128)} %broadcast_in_dim.62), calls=%async_computation | async-start | bytes 16384 | tf_op jit(solution)/shard_map/all_to_all | solution.py:21
  15.6 4.6 %all-to-all-done = f32[4,1,512]{2,1,0:T(1,128)S(1)} async-done(((f32[4,1,512]{2,1,0:T(1,128)}), f32[4,1,512]{2,1,0:T(1,128)S(1)}, u32[]{:S(2)}, u32[]{:S(2)}) %all-to-all-start) | async-done | bytes 8224 | tf_op jit(solution)/shard_map/all_to_all | solution.py:21
  20.3 1.2 fusion.9
  21.7 1.6 broadcast_in_dim.63
  23.4 3.8 %all-to-all-start.1 = ((bf16[4,512,512]{1,2,0:T(8,128)(2,1)}), bf16[4,512,512]{1,2,0:T(8,128)(2,1)S(1)}, u32[]{:S(2)}, u32[]{:S(2)}) async-start(bf16[4,512,512]{1,2,0:T(8,128)(2,1)} %broadcast_in_dim.63), calls=%async_computation.1 | async-start | bytes 4194304 | tf_op jit(solution)/shard_map/all_to_all | solution.py:21
  30.6 21.7 %all-to-all-done.1 = bf16[4,512,512]{1,2,0:T(8,128)(2,1)S(1)} async-done(((bf16[4,512,512]{1,2,0:T(8,128)(2,1)}), bf16[4,512,512]{1,2,0:T(8,128)(2,1)S(1)}, u32[]{:S(2)}, u32[]{:S(2)}) %all-to-all-start.1) | async-done | bytes 2097184 | tf_op jit(solution)/shard_map/all_to_all | solution.py:21
  52.3 46.7 %all-gather.9.cloned.1.call-done = bf16[2048,900]{1,0:T(8,128)(2,1)} async-done(((bf16[16,900]{1,0:T(8,128)(2,1)}), bf16[2048,900]{1,0:T(8,128)(2,1)}) %all-gather.9.cloned.1.call-update) | async-done | bytes 3686416 | tf_op jit(solution)/shard_map/all_gather | solution.py:138
  99.0 4.4 %fusion.160 = (bf16[512,900]{0,1:T(8,128)(2,1)S(1)}, f32[512,900]{0,1:T(8,128)S(1)}) fusion(bf16[512,2048]{0,1:T(8,128)(2,1)S(1)} %bitcast.291, bf16[2048,900]{1,0:T(8,128)(2,1)} %all-gather.9.cloned.1.call-done), kind=kOutput, calls=%fused_computation.265 | convolution fusion | flops 1887897600 | bytes 8548352 | tf_op jit(solution)/shard_map/dot_general | solution.py:144
  104.2 2.1 collective-permute-start.1
  109.5 3.7 %collective-permute-start = (bf16[15,256]{0,1:T(8,128)(2,1)}, bf16[15,256]{0,1:T(8,128)(2,1)}, u32[]{:S(2)}, u32[]{:S(2)}) collective-permute-start(bf16[15,256]{0,1:T(8,128)(2,1)} %slice.355), channel_id=1, source_target_pairs={{0,4},{4,8},{8,12},{12,16},{16,20},{20,24},{24,28},{28,32},{32,36}... | collective-permute-start | bytes 23048 | tf_op jit(solution)/shard_map/ppermute | solution.py:42
  113.5 0.9 multiply_convert_fusion
  115.4 0.9 fusion.27
  116.3 3.1 %while.13 = (s32[]{:T(128)}, f32[4,64,64]{2,1,0:T(8,128)S(1)}, f32[4,4,64,64]{3,2,1,0:T(8,128)}, f32[4,4]{1,0:T(4,128)S(1)}, f32[4,4,64,64]{3,2,1,0:T(8,128)S(1)}, /*index=5*/s32[]{:T(128)}, s32[]{:T(128)}) while((s32[]{:T(128)}, f32[4,64,64]{2,1,0:T(8,128)S(1)}, f32[4,4,64,64]{3,2,1,0:T(8,128)}, f32[4,4]{1,0:T(4,128)S(1)}, ...), condition=%wide.region_4.5_spmd.clone, body=%wide.region_3.4_spmd.clone.sunk | while | flops 65539 | bytes 393872 | solution.py:218
  119.6 1.9 all-gather.3
  122.5 26.1 %all-gather.4 = f32[8,257,64]{1,2,0:T(8,128)S(1)} all-gather(f32[1,257,64]{1,2,0:T(8,128)S(1)} %maximum_bitcast_fusion.1), channel_id=3, replica_groups=mesh['sp_0'=8,'sp_1'=8,'sp_2'=2,'tp'=4] {'sp_1'}, dimensions={0}, use_global_device_ids=true | all-gather | bytes 592128 | tf_op jit(solution)/shard_map/all_gather | solution.py:59
  150.9 26.9 %all-gather.5 = f32[8,257,64]{1,2,0:T(8,128)S(1)} all-gather(f32[1,257,64]{1,2,0:T(8,128)S(1)} %maximum_bitcast_fusion.2), channel_id=4, replica_groups=mesh['sp_0'=8,'sp_1'=8,'sp_2'=2,'tp'=4] {'sp_0'}, dimensions={0}, use_global_device_ids=true | all-gather | bytes 592128 | tf_op jit(solution)/shard_map/all_gather | solution.py:59
  177.7 0.8 fusion.155
  178.5 1.6 copy.267
  180.1 1.6 copy.268
  181.7 1.6 copy.269
  183.3 1.6 copy.270
  184.9 1.6 copy.271
  186.5 1.6 copy.272
  188.1 1.6 copy.273
  189.7 0.8 copy.274
  191.1 0.8 fusion.156
  191.9 1.6 copy.275
  193.5 1.6 copy.276
  195.1 1.6 copy.277
  197.5 0.8 copy.279
  198.2 1.6 copy.280
  199.8 1.6 copy.281
  201.4 0.8 copy.282
  202.2 0.8 copy.283
  203.0 0.8 copy.284
  203.8 1.7 fusion.4
  205.5 2.8 %fusion.1 = f32[4,128,128,4]{1,2,3,0:T(8,128)S(1)} fusion(f32[4,128,4]{1,2,0:T(4,128)} %copy.230, pred[128,128]{0,1:T(8,128)(4,1)} %iota_compare_fusion, f32[4,128,64]{1,2,0:T(8,128)S(1)} %bitcast.295, f32[4,128,64]{1,2,0:T(8,128)S(1)} %bitcast.299), kind=kOutput, calls=%fused_computation.11 | convolution fusion | flops 202113024 | bytes 1335296 | tf_op jit(solution)/shard_map/blhn,bshn->blsh/dot_general | solution.py:207
  208.4 2.4 fusion.5
  210.9 1.1 fusion.3
  213.2 4.2 %all-to-all-start.2 = ((f32[4,1,512]{2,1,0:T(1,128)}), f32[4,1,512]{2,1,0:T(1,128)S(1)}, u32[]{:S(2)}, u32[]{:S(2)}) async-start(f32[4,1,512]{2,1,0:T(1,128)} %broadcast_in_dim.73), calls=%async_computation.2 | async-start | bytes 16384 | tf_op jit(solution)/shard_map/all_to_all | solution.py:21
  217.3 1.0 maximum_convert_fusion.1
  220.2 2.5 %all-to-all-done.2 = f32[4,1,512]{2,1,0:T(1,128)S(1)} async-done(((f32[4,1,512]{2,1,0:T(1,128)}), f32[4,1,512]{2,1,0:T(1,128)S(1)}, u32[]{:S(2)}, u32[]{:S(2)}) %all-to-all-start.2) | async-done | bytes 8224 | tf_op jit(solution)/shard_map/all_to_all | solution.py:21
  222.9 2.9 %convolution_convert_fusion = bf16[512,2048]{1,0:T(8,128)(2,1)S(1)} fusion(bf16[512,2048]{0,1:T(8,128)(2,1)} %all-gather.11.cloned.1.call-done, bf16[512,256]{0,1:T(8,128)(2,1)S(1)} %multiply_convert_fusion.1, bf16[512,256]{0,1:T(8,128)(2,1)S(1)} %fusion.6), kind=kOutput, calls=%fused_computation.4 | convolution fusion | flops 1075838976 | bytes 4718592 | tf_op jit(solution)/shard_map/dot_general | solution.py:250
  226.0 19.0 %all_to_all.22 = bf16[4,512,512]{2,1,0:T(8,128)(2,1)S(1)} all-to-all(bf16[4,512,512]{2,1,0:T(8,128)(2,1)S(1)} %bitcast.290), channel_id=1, replica_groups=mesh['sp_0'=8,'sp_1'=8,'sp_2'=2,'tp'=4] {'tp'}, dimensions={0} | all-to-all | bytes 4194304 | tf_op jit(solution)/shard_map/all_to_all | solution.py:90
  245.0 1.2 reduce_sum.52
  (193 shorter events, 21.0 us)
Async XLA Ops:
  6.5 213.1 %copy-start = (bf16[1,256,256]{2,1,0:T(8,128)(2,1)S(1)}, bf16[1,256,256]{2,1,0:T(8,128)(2,1)}, u32[]{:S(2)}) copy-start(bf16[1,256,256]{2,1,0:T(8,128)(2,1)} %param.30) | copy-start | bytes 393220
  6.5 92.5 %all-gather.9.cloned.1.call-start = ((), (), s32[]{:S(2)}) async-start(), calls=%async_computation.4 | async-start | bytes 4227072 | tf_op jit(solution)/shard_map/all_gather | solution.py:138
  10.6 9.6 %all-to-all-start = ((f32[4,1,512]{2,1,0:T(1,128)}), f32[4,1,512]{2,1,0:T(1,128)S(1)}, u32[]{:S(2)}, u32[]{:S(2)}) async-start(f32[4,1,512]{2,1,0:T(1,128)} %broadcast_in_dim.62), calls=%async_computation | async-start | bytes 16384 | tf_op jit(solution)/shard_map/all_to_all | solution.py:21
  23.3 3.9 %copy-start.15 = (bf16[256,16]{0,1:T(8,128)(2,1)S(1)}, bf16[256,16]{0,1:T(8,128)(2,1)}, u32[]{:S(2)}) copy-start(bf16[256,16]{0,1:T(8,128)(2,1)} %param.41) | copy-start | bytes 24580
  23.3 3.9 %copy-start.16 = (bf16[256,16]{0,1:T(8,128)(2,1)S(1)}, bf16[256,16]{0,1:T(8,128)(2,1)}, u32[]{:S(2)}) copy-start(bf16[256,16]{0,1:T(8,128)(2,1)} %param.40) | copy-start | bytes 24580
  23.3 4.6 %copy-start.36 = (f32[4]{0:T(128)S(1)}, f32[4]{0:T(128)}, u32[]{:S(2)}) copy-start(f32[4]{0:T(128)} %param.38) | copy-start | bytes 52
  23.3 6.0 %copy-start.26 = (f32[4,256]{1,0:T(4,128)S(1)}, f32[4,256]{1,0:T(4,128)}, u32[]{:S(2)}) copy-start(f32[4,256]{1,0:T(4,128)} %param.32) | copy-start | bytes 12292
  23.3 6.0 %copy-start.30 = (f32[4,64]{1,0:T(4,128)S(1)}, f32[4,64]{1,0:T(4,128)}, u32[]{:S(2)}) copy-start(f32[4,64]{1,0:T(4,128)} %param.34) | copy-start | bytes 3076
  23.3 5.9 %copy-start.31 = (f32[4,64]{1,0:T(4,128)S(1)}, f32[4,64]{1,0:T(4,128)}, u32[]{:S(2)}) copy-start(f32[4,64]{1,0:T(4,128)} %param.33) | copy-start | bytes 3076
  23.3 7.2 %copy-start.38 = (f32[4]{0:T(128)S(1)}, f32[4]{0:T(128)}, u32[]{:S(2)}) copy-start(f32[4]{0:T(128)} %param.36) | copy-start | bytes 52
  23.4 28.9 %all-to-all-start.1 = ((bf16[4,512,512]{1,2,0:T(8,128)(2,1)}), bf16[4,512,512]{1,2,0:T(8,128)(2,1)S(1)}, u32[]{:S(2)}, u32[]{:S(2)}) async-start(bf16[4,512,512]{1,2,0:T(8,128)(2,1)} %broadcast_in_dim.63), calls=%async_computation.1 | async-start | bytes 4194304 | tf_op jit(solution)/shard_map/all_to_all | solution.py:21
  27.1 195.8 %all-gather.11.cloned.1.call-start = ((), (), s32[]{:S(2)}) async-start(), calls=%async_computation.5 | async-start | bytes 2113536 | tf_op jit(solution)/shard_map/all_gather | solution.py:252
  99.0 4.4 %copy-start.17 = (f32[512,4]{0,1:T(4,128)S(1)}, f32[512,4]{0,1:T(4,128)}, u32[]{:S(2)}) copy-start(f32[512,4]{0,1:T(4,128)} %param.37) | copy-start | bytes 24580
  99.0 4.4 %copy-start.35 = (f32[4]{0:T(128)S(1)}, f32[4]{0:T(128)}, u32[]{:S(2)}) copy-start(f32[4]{0:T(128)} %param.35) | copy-start | bytes 52
  104.1 9.3 %copy-start.11 = (f32[384]{0:T(512)S(1)}, f32[384]{0:T(512)}, u32[]{:S(2)}) copy-start(f32[384]{0:T(512)} %get-tuple-element.53) | copy-start | bytes 4612
  104.1 9.3 %copy-start.12 = (f32[384]{0:T(512)S(1)}, f32[384]{0:T(512)}, u32[]{:S(2)}) copy-start(f32[384]{0:T(512)} %get-tuple-element.54) | copy-start | bytes 4612
  104.1 9.3 %copy-start.13 = (f32[384]{0:T(512)S(1)}, f32[384]{0:T(512)}, u32[]{:S(2)}) copy-start(f32[384]{0:T(512)} %get-tuple-element.55) | copy-start | bytes 4612
  104.1 9.3 %copy-start.14 = (f32[384]{0:T(512)S(1)}, f32[384]{0:T(512)}, u32[]{:S(2)}) copy-start(f32[384]{0:T(512)} %get-tuple-element.56) | copy-start | bytes 4612
  104.2 9.0 %collective-permute-start.1 = (bf16[3,384]{0,1:T(8,128)(2,1)S(1)}, bf16[3,384]{0,1:T(8,128)(2,1)S(1)}, u32[]{:S(2)}, u32[]{:S(2)}) collective-permute-start(bf16[3,384]{0,1:T(8,128)(2,1)S(1)} %slice.368), channel_id=1, source_target_pairs={{0,4},{4,8},{8,12},{12,16},{16,20},{20,24},{24,28},{28,32},{32,36}... | collective-permute-start | bytes 6920 | tf_op jit(solution)/shard_map/ppermute | solution.py:42
  109.5 107.8 %collective-permute-start = (bf16[15,256]{0,1:T(8,128)(2,1)}, bf16[15,256]{0,1:T(8,128)(2,1)}, u32[]{:S(2)}, u32[]{:S(2)}) collective-permute-start(bf16[15,256]{0,1:T(8,128)(2,1)} %slice.355), channel_id=1, source_target_pairs={{0,4},{4,8},{8,12},{12,16},{16,20},{20,24},{24,28},{28,32},{32,36}... | collective-permute-start | bytes 23048 | tf_op jit(solution)/shard_map/ppermute | solution.py:42
  115.2 1.1 copy-start.1
  121.6 27.1 %copy-start.25 = (f32[4]{0:T(128)}, f32[4]{0:T(128)S(1)}, u32[]{:S(2)}) copy-start(f32[4]{0:T(128)S(1)} %get-tuple-element.116) | copy-start | bytes 52
  121.6 27.1 %copy-start.33 = (f32[4]{0:T(128)}, f32[4]{0:T(128)S(1)}, u32[]{:S(2)}) copy-start(f32[4]{0:T(128)S(1)} %get-tuple-element.117) | copy-start | bytes 52
  121.7 0.6 copy-start.28
  148.8 2.0 copy-start.18
  148.8 2.0 copy-start.19
  148.8 2.0 copy-start.20
  148.8 2.0 copy-start.21
  148.8 2.0 copy-start.22
  148.8 2.0 copy-start.23
  148.8 2.0 copy-start.24
  148.9 1.1 copy-start.29
  191.1 12.6 %copy-start.3 = (f32[8,4,8,128]{3,2,1,0:T(8,128)S(1)}, f32[8,4,8,128]{3,2,1,0:T(8,128)}, u32[]{:S(2)}) copy-start(f32[8,4,8,128]{3,2,1,0:T(8,128)} %get-tuple-element.93) | copy-start | bytes 393220
  191.9 11.9 %copy-start.10 = (f32[8,1,64]{2,0,1:T(8,128)S(1)}, f32[8,1,64]{2,0,1:T(8,128)}, u32[]{:S(2)}) copy-start(f32[8,1,64]{2,0,1:T(8,128)} %copy.288) | copy-start | bytes 6148
  191.9 13.6 %copy-start.2 = (f32[8,4,8,128]{3,2,0,1:T(8,128)S(1)}, f32[8,4,8,128]{3,2,0,1:T(8,128)}, u32[]{:S(2)}) copy-start(f32[8,4,8,128]{3,2,0,1:T(8,128)} %copy-done.1) | copy-start | bytes 393220
  198.2 10.1 %copy-start.4 = (f32[1,256,64]{2,1,0:T(8,128)S(1)}, f32[1,256,64]{2,1,0:T(8,128)}, u32[]{:S(2)}) copy-start(f32[1,256,64]{2,1,0:T(8,128)} %copy.267) | copy-start | bytes 196612
  202.2 6.1 %copy-start.5 = (f32[1,256,64]{2,1,0:T(8,128)S(1)}, f32[1,256,64]{2,1,0:T(8,128)}, u32[]{:S(2)}) copy-start(f32[1,256,64]{2,1,0:T(8,128)} %copy.280) | copy-start | bytes 196612
  203.7 4.6 %copy-start.6 = (f32[1,256,64]{2,1,0:T(8,128)S(1)}, f32[1,256,64]{2,1,0:T(8,128)}, u32[]{:S(2)}) copy-start(f32[1,256,64]{2,1,0:T(8,128)} %copy.281) | copy-start | bytes 196612
  203.7 4.6 %copy-start.7 = (f32[1,256,64]{2,1,0:T(8,128)S(1)}, f32[1,256,64]{2,1,0:T(8,128)}, u32[]{:S(2)}) copy-start(f32[1,256,64]{2,1,0:T(8,128)} %copy.282) | copy-start | bytes 196612
  203.7 4.6 %copy-start.8 = (f32[1,256,64]{2,1,0:T(8,128)S(1)}, f32[1,256,64]{2,1,0:T(8,128)}, u32[]{:S(2)}) copy-start(f32[1,256,64]{2,1,0:T(8,128)} %copy.283) | copy-start | bytes 196612
  203.7 4.7 %copy-start.9 = (f32[1,256,64]{2,1,0:T(8,128)S(1)}, f32[1,256,64]{2,1,0:T(8,128)}, u32[]{:S(2)}) copy-start(f32[1,256,64]{2,1,0:T(8,128)} %copy.284) | copy-start | bytes 196612
  210.8 1.4 copy-start.27
  213.2 9.5 %all-to-all-start.2 = ((f32[4,1,512]{2,1,0:T(1,128)}), f32[4,1,512]{2,1,0:T(1,128)S(1)}, u32[]{:S(2)}, u32[]{:S(2)}) async-start(f32[4,1,512]{2,1,0:T(1,128)} %broadcast_in_dim.73), calls=%async_computation.2 | async-start | bytes 16384 | tf_op jit(solution)/shard_map/all_to_all | solution.py:21
  219.1 0.6 copy-start.32
  219.1 0.7 copy-start.37
  219.6 3.1 %copy-start.34 = (f32[256]{0:T(256)S(1)}, f32[256]{0:T(256)}, u32[]{:S(2)}) copy-start(f32[256]{0:T(256)} %param.39) | copy-start | bytes 3076
Sparse Core Ops, SparseCore 0:
  10.5 88.4 all-gather.8
  102.1 80.4 all-gather.10
where the time goes:
time: 255 us; the launch traced here: 253 us
  waiting for transfers between devices  75.7 us (30%)
  blocking collectives  73.9 us (29%)
  local copies, waits for them, and re-layouts  39.7 us (16%)
  starting transfers between devices  18.1 us (7%)
  matrix products  16.7 us (7%)
  other arithmetic  14.6 us (6%)
  between operations  14.4 us (6%)
    all_gather x3, blocking collectives, all_in_one(): both, at, found = (lax.all_gather(jnp.concatenate(lines), axis), 0, {})  54.9 us
    all_gather x1, waiting for transfers between devices, local(): in_weight = lax.all_gather(joined, SP, axis=0, tiled=True)  46.7 us
    all_to_all x3, waiting for transfers between devices, sent_to_all(): return lax.all_to_all(copies, axis, split_axis=0, concat_axis=0, tiled=True)  28.8 us
    squeeze x18, local copies, waits for them, and re-layouts, prefix_by_axis(): running = combine(running, jax.tree.map(lambda part: part[k], pieces))  23.7 us
    all_to_all x1, blocking collectives, summed_on_arrival(): lax.all_to_all(pieces, axis, split_axis=0, concat_axis=0, tiled=True)  19 us
    all_to_all x3, starting transfers between devices, sent_to_all(): return lax.all_to_all(copies, axis, split_axis=0, concat_axis=0, tiled=True)  12.2 us
    ppermute x2, starting transfers between devices, shifted(): lax.ppermute(value, axis, [(source, source + steps) for source in range(l...  5.82 us
  transfers between devices with their start and end apart: 7, of which 4 were waited for; matrix products, arithmetic and copies ran while one was open for 25% of the time, Pallas kernels for 0%

commit v1 on v0

--- a/solution.py
+++ b/solution.py
@@ -26,58 +26,40 @@
     return jnp.sum(everything, axis=0)
 
 
-def laid_out(pieces, dim):
-    pieces = jnp.moveaxis(pieces, 0, dim)
-    shape = pieces.shape
-    return pieces.reshape(*shape[:dim], shape[dim] * shape[dim + 1], *shape[dim + 2 :])
-
-
-def collect(array, axis, dim):
-    return laid_out(sent_to_all(array, axis), dim)
-
-
 def shifted(value, axis, steps):
     count = lax.axis_size(axis)
     leading, last = (max(0, -steps), min(count, count - steps))
     return lax.ppermute(value, axis, [(source, source + steps) for source in range(leading, last)])
 
 
-def neutral_like(array, identity):
-    return jax.tree.map(
-        lambda part, zero: jnp.zeros_like(part) + jnp.asarray(zero, part.dtype), array, identity
-    )
-
-
-def all_in_one(array, axis):
-    leaves = jax.tree.leaves(array)
-    order = sorted(range(len(leaves)), key=lambda k: -leaves[k].size)
-    width = (1, *leaves[order[0]].shape)[-1]
-    lines = [
-        jnp.pad(leaves[k].reshape(-1), (0, -leaves[k].size % width)).reshape(-1, width)
-        for k in order
-    ]
-    both, at, found = (lax.all_gather(jnp.concatenate(lines), axis), 0, {})
-    for k, line in zip(order, lines):
-        section = both[:, at : at + len(line)].reshape(len(both), -1)
-        found[k] = section[:, : leaves[k].size].reshape(-1, *leaves[k].shape)
-        at += len(line)
-    numbers = iter(range(len(leaves)))
-    return jax.tree.map(lambda _: found[next(numbers)], array)
-
-
-def prefix_by_axis(array, axes, combine, identity):
-    before = start = neutral_like(array, identity)
-    running = array
-    for axis in reversed(axes):
-        count, place = (lax.axis_size(axis), lax.axis_index(axis))
-        pieces = all_in_one(running, axis)
-        inside, running = (start, start)
-        for k in range(count):
-            passed = k < place
-            running = combine(running, jax.tree.map(lambda part: part[k], pieces))
-            inside = jax.tree.map(lambda new, old: jnp.where(passed, new, old), running, inside)
-        before = combine(inside, before)
-    return before
+def parts_of(value):
+    high = value.astype(jnp.bfloat16)
+    rest = value - high.astype(jnp.float32)
+    middle = rest.astype(jnp.bfloat16)
+    low = (rest - middle.astype(jnp.float32)).astype(jnp.bfloat16)
+    return jnp.concatenate([high, middle, low])
+
+
+def packed(state, log_total):
+    lanes = 128
+    numbers = parts_of(log_total)
+    tail = jnp.pad(numbers, (0, 16 * lanes - numbers.shape[0])).reshape(16, lanes)
+    return jnp.concatenate([state.astype(jnp.bfloat16).reshape(-1, lanes), tail])
+
+
+def unpacked(pieces, heads, shape):
+    rows = pieces.shape[1] - 16
+    numbers = pieces[:, rows, : 3 * heads].astype(jnp.float32).reshape(-1, 3, heads)
+    return pieces[:, :rows].reshape(-1, *shape), jnp.sum(numbers, axis=1)
+
+
+def weighted(states, logs, begin, end):
+    count = states.shape[0]
+    source = jnp.arange(count)
+    between = (source[None, :] > source[:, None]) & (source[None, :] < end)
+    total = jnp.sum(jnp.where(between[:, :, None], logs[None, :, :], 0.0), axis=1)
+    factors = jnp.where((source < end)[:, None], jnp.exp(total + begin), 0.0)
+    return jnp.sum(states.astype(jnp.float32) * factors[:, :, None, None], axis=0)
 
 
 def split_up(array, dim, count):
@@ -99,10 +81,6 @@
     for offset in range(width):
         total = total + taps[offset][None, :] * widened_rows[offset : offset + length]
     return jax.nn.silu(total).astype(jnp.bfloat16)
-
-
-def combine_states(preceding_token, later):
-    return (preceding_token[0] * later[0], preceding_token[1] * later[0][:, None, None] + later[1])
 
 
 def local(
@@ -132,36 +110,57 @@
     local_mix = gate_weight.shape[1]
     local_state = key_weight.shape[1]
     local_heads = step_weight.shape[1]
+    plane = ("sp_0", "sp_1")
+    place = lax.axis_index("tp")
+    core = lax.axis_index("sp_2")
+    sent = jnp.concatenate(
+        [activations, jnp.broadcast_to(norm_gain[None, :], (8, norm_gain.shape[0]))], axis=0
+    )
+    everything = sent_to_all(sent, "tp")
+    first_weights = jnp.concatenate([value_weight, key_weight, step_weight], axis=1)
+    mine = sent_to_all(first_weights, plane)
+    other = lax.ppermute(mine, "sp_2", [(0, 1), (1, 0)])
     joined = jnp.concatenate(
-        [pool_weight, gate_weight, value_weight, key_weight, read_weight, step_weight], axis=1
-    )
-    in_weight = lax.all_gather(joined, SP, axis=0, tiled=True)
-    values = activations.astype(jnp.float32)
-    squares = over_copies(jnp.sum(values * values, axis=-1), "tp")
+        [
+            pool_weight,
+            gate_weight,
+            read_weight,
+            jnp.transpose(out_pool_weight),
+            jnp.transpose(out_state_weight),
+        ],
+        axis=1,
+    )
+    later_weights = lax.all_gather(joined, SP, axis=0, tiled=True)
+    reach = 2**POOL_GROUPS
+    received = everything[:, :length]
+    before = shifted(received[:, length - reach :], SP, 1)
+    rows = jnp.concatenate([before, received], axis=1).astype(jnp.float32)
+    squares = jnp.sum(rows * rows, axis=(0, 2))
+    gains = everything[:, length].astype(jnp.float32)
     normed = (
-        values * lax.rsqrt(squares / D + EPSILON)[:, None] * norm_gain.astype(jnp.float32)
+        rows * lax.rsqrt(squares / D + EPSILON)[None, :, None] * gains[:, None, :]
     ).astype(jnp.bfloat16)
-    projected = jnp.dot(collect(normed, "tp", 1), in_weight, preferred_element_type=jnp.float32)
-    column = 0
-    pool_in = projected[:, column : column + cluster_span].astype(jnp.bfloat16)
-    column = column + cluster_span
-    gate_in = projected[:, column : column + local_mix].astype(jnp.bfloat16)
-    column = column + local_mix
-    raw_value = projected[:, column : column + local_mix].astype(jnp.bfloat16)
-    column = column + local_mix
-    raw_key = projected[:, column : column + local_state].astype(jnp.bfloat16)
-    column = column + local_state
-    raw_read = projected[:, column : column + local_state].astype(jnp.bfloat16)
-    column = column + local_state
-    step_raw = projected[:, column : column + local_heads]
-    raw_joined = jnp.concatenate([raw_value, raw_key, raw_read], axis=1)
-    reach = 2**POOL_GROUPS - 1
+    in_weight = jnp.stack(
+        [jnp.where(core == 0, mine, other), jnp.where(core == 0, other, mine)], axis=1
+    ).reshape(lax.axis_size("tp"), -1, first_weights.shape[1])
+    first = jnp.einsum("ktd,kdn->tn", normed, in_weight, preferred_element_type=jnp.float32)
+    raw_value = first[:, :local_mix].astype(jnp.bfloat16)
+    raw_key = first[:, local_mix : local_mix + local_state].astype(jnp.bfloat16)
+    step_raw = first[reach:, local_mix + local_state :]
+    second_weights = later_weights[:, : cluster_span + local_mix + local_state]
+    second = jnp.einsum(
+        "ktd,kdn->tn",
+        normed,
+        second_weights.reshape(lax.axis_size("tp"), -1, second_weights.shape[1]),
+        preferred_element_type=jnp.float32,
+    ).astype(jnp.bfloat16)
+    pool_all = second[:, :cluster_span]
+    pool_in = pool_all[reach:]
+    gate_in = second[reach:, cluster_span : cluster_span + local_mix]
+    raw_read = second[:, cluster_span + local_mix :]
     width = taps_value.shape[0]
-    prior_pool, prior_joined = shifted(
-        (pool_in[length - reach :], raw_joined[length - width + 1 :]), SP, 1
-    )
-    group = lax.axis_index("tp")
-    running = jnp.concatenate([prior_pool, pool_in], axis=0).astype(jnp.float32)
+    group = place
+    running = pool_all[1:].astype(jnp.float32)
     levels = []
     for level in range(POOL_GROUPS):
         stride = 2**level
@@ -177,11 +176,10 @@
     pool_out = (
         jnp.dot(pooled, pool_mix[0], preferred_element_type=jnp.float32) * pool_scale
     ).astype(jnp.bfloat16)
-    all_taps = jnp.concatenate([taps_value, taps_key, taps_read], axis=1)
-    convolved = backward_kernel(jnp.concatenate([prior_joined, raw_joined], axis=0), all_taps)
-    head_value = convolved[:, :local_mix]
-    key_vectors = convolved[:, local_mix : local_mix + local_state]
-    read_vectors = convolved[:, local_mix + local_state :]
+    start = reach - width + 1
+    head_value = backward_kernel(raw_value[start:], taps_value)
+    key_vectors = backward_kernel(raw_key[start:], taps_key)
+    read_vectors = backward_kernel(raw_read[start:], taps_read)
     head_dim = local_mix // local_heads
     groups_here = local_state // SSM_STATE
     repeat = local_heads // groups_here
@@ -221,12 +219,20 @@
         (jnp.exp(block_ends), fresh),
     )
     offsets = jnp.cumsum(block_ends, axis=0) - block_ends
-    device_decay = jnp.exp(offsets[-1] + block_ends[-1])
-    incoming_decay, incoming = prefix_by_axis(
-        (device_decay, local_total),
-        SP,
-        combine_states,
-        (jnp.ones_like(device_decay), jnp.zeros_like(local_total)),
+    device_log = offsets[-1] + block_ends[-1]
+    state_shape = local_total.shape
+    row = lax.axis_index(("sp_1", "sp_2"))
+    row_count = lax.axis_size(("sp_1", "sp_2"))
+    row_states, row_logs = unpacked(
+        lax.all_gather(packed(local_total, device_log), ("sp_1", "sp_2")), local_heads, state_shape
+    )
+    row_total = weighted(row_states, row_logs, 0.0, row_count)
+    plane_states, plane_logs = unpacked(
+        sent_to_all(packed(row_total, jnp.sum(row_logs, axis=0)), "sp_0"), local_heads, state_shape
+    )
+    row_before = jnp.sum(jnp.where((jnp.arange(row_count) < row)[:, None], row_logs, 0.0), axis=0)
+    incoming = weighted(row_states, row_logs, 0.0, row) + weighted(
+        plane_states, plane_logs, row_before, lax.axis_index("sp_0")
     )
     from_device = running_decay + offsets[:, None, :]
     local_off = (
@@ -242,16 +248,15 @@
     ] * value_heads
     gated = scan_out.reshape(length, local_mix) * jax.nn.silu(gate_in.astype(jnp.float32))
     gate_squares = over_copies(jnp.sum(gated * gated, axis=-1), "tp")
-    state_out = (gated * lax.rsqrt(gate_squares / MIX_W + EPSILON)[:, None] * state_gain).astype(
-        jnp.bfloat16
-    )
-    branch_rows = jnp.concatenate([pool_out, state_out], axis=1)
-    out_weight = jnp.concatenate([out_pool_weight, out_state_weight], axis=0)
-    terms = jnp.dot(
-        branch_rows,
-        lax.all_gather(out_weight, SP, axis=1, tiled=True),
-        preferred_element_type=jnp.float32,
-    )
+    state_rows = (gated * state_gain).astype(jnp.bfloat16)
+    out_weights = later_weights[:, second_weights.shape[1] :]
+    pool_terms = jnp.einsum(
+        "tc,dc->td", pool_out, out_weights[:, :cluster_span], preferred_element_type=jnp.float32
+    )
+    state_terms = jnp.einsum(
+        "tc,dc->td", state_rows, out_weights[:, cluster_span:], preferred_element_type=jnp.float32
+    )
+    terms = pool_terms + state_terms * lax.rsqrt(gate_squares / MIX_W + EPSILON)[:, None]
     result = summed_on_arrival(terms.astype(jnp.bfloat16), "tp", 1)
     return result.astype(jnp.bfloat16)
 

time: 255 us -> 215 us (0.84)
  blocking collectives: 73.9 us -> 45.7 us
  local copies, waits for them, and re-layouts: 39.7 us -> 20.3 us
  starting transfers between devices: 18.1 us -> 36.4 us
  waiting for transfers between devices: 75.7 us -> 60.4 us
    all_gather x2 -> x1, waiting for transfers between devices: 46.8 us -> 0.02 us  [local(): later_weights = lax.all_gather(joined, SP, axis=0, tiled=True)]
    all_gather x3 -> x1, blocking collectives: 54.9 us -> 16.4 us  [local(): lax.all_gather(packed(local_total, device_log), ('sp_1', 'sp_2'))]
    all_to_all x3 -> x4, waiting for transfers between devices: 28.8 us -> 57 us  [sent_to_all(): return lax.all_to_all(copies, axis, split_axis=0, concat_axis=0, tiled=True)]
    squeeze x18 -> x0, local copies, waits for them, and re-layouts: 23.7 us -> none  [prefix_by_axis(): running = combine(running, jax.tree.map(lambda part: part[k], pieces))]
    all_to_all x3 -> x4, starting transfers between devices: 12.2 us -> 32.6 us  [sent_to_all(): return lax.all_to_all(copies, axis, split_axis=0, concat_axis=0, tiled=True)]
    all_to_all x1, blocking collectives: 19 us -> 29.3 us  [summed_on_arrival(): lax.all_to_all(pieces, axis, split_axis=0, concat_axis=0, tiled=True)]
    ppermute x2 -> x1, starting transfers between devices: 5.82 us -> 1.91 us  [shifted(): lax.ppermute(value, axis, [(source, source + steps) for source in range(l...]
    dot_general x3 -> x4, matrix products: 7.67 us -> 11.4 us  [the longest x1 4.51 us: local(): jnp.einsum('tc,dc->td', pool_out, out_weights[:, :cluster_span], preferre...]
  transfers between devices with their start and end apart: 7 -> 7, of which waited for: 4 -> 5; matrix products, arithmetic and copies ran while one was open for 25% -> 14% of each run, Pallas kernels for 0% -> 0%
where the time goes in v1:
time: 215 us; the launch traced here: 214 us
  waiting for transfers between devices  60.4 us (28%)
  blocking collectives  45.7 us (21%)
  starting transfers between devices  36.4 us (17%)
  local copies, waits for them, and re-layouts  20.3 us (9%)
  matrix products  19.2 us (9%)
  other arithmetic  17 us (8%)
  between operations  14.5 us (7%)
    all_to_all x4, waiting for transfers between devices, sent_to_all(): return lax.all_to_all(copies, axis, split_axis=0, concat_axis=0, tiled=True)  57 us
    all_to_all x4, starting transfers between devices, sent_to_all(): return lax.all_to_all(copies, axis, split_axis=0, concat_axis=0, tiled=True)  32.6 us
    all_to_all x1, blocking collectives, summed_on_arrival(): lax.all_to_all(pieces, axis, split_axis=0, concat_axis=0, tiled=True)  29.3 us
    all_gather x1, blocking collectives, local(): lax.all_gather(packed(local_total, device_log), ('sp_1', 'sp_2'))  16.4 us
    dot_general x1, matrix products, local(): jnp.einsum('tc,dc->td', pool_out, out_weights[:, :cluster_span], preferre...  4.51 us
  transfers between devices with their start and end apart: 7, of which 5 were waited for; matrix products, arithmetic and copies ran while one was open for 14% of the time, Pallas kernels for 0%

profile of v1, /device:TPU:8, one launch (start us, length us, event | category | flops | bytes accessed | tf_op | source)
XLA Modules:
  0.0 213.7 jit_solution(2852914146801602633)
XLA Ops:
  6.5 0.8 copy.166
  7.4 0.8 pad_maximum_fusion.5
  8.2 1.0 broadcast_in_dim.180
  9.1 16.6 %all-to-all-start.1 = ((bf16[64,16,324]{2,1,0:T(8,128)(2,1)}), bf16[64,16,324]{2,1,0:T(8,128)(2,1)S(1)}, u32[]{:S(2)}, u32[]{:S(2)}) async-start(bf16[64,16,324]{2,1,0:T(8,128)(2,1)} %broadcast_in_dim.180), calls=%async_computation.1 | async-start | bytes 1572864 | tf_op jit(solution)/shard_map/all_to_all | solution.py:21
  25.8 23.9 %all-to-all-done.1 = bf16[64,16,324]{2,1,0:T(8,128)(2,1)S(1)} async-done(((bf16[64,16,324]{2,1,0:T(8,128)(2,1)}), bf16[64,16,324]{2,1,0:T(8,128)(2,1)S(1)}, u32[]{:S(2)}, u32[]{:S(2)}) %all-to-all-start.1) | async-done | bytes 663584 | tf_op jit(solution)/shard_map/all_to_all | solution.py:21
  49.7 1.6 broadcast_in_dim.179
  51.4 4.4 %all-to-all-start = ((bf16[4,520,512]{2,1,0:T(8,128)(2,1)}), bf16[4,520,512]{2,1,0:T(8,128)(2,1)S(1)}, u32[]{:S(2)}, u32[]{:S(2)}) async-start(bf16[4,520,512]{2,1,0:T(8,128)(2,1)} %broadcast_in_dim.179), calls=%async_computation | async-start | bytes 4259840 | tf_op jit(solution)/shard_map/all_to_all | solution.py:21
  55.8 0.7 concatenate.26
  56.7 0.7 mul.362
  58.2 1.9 collective-permute-start.1
  60.7 19.8 %all-to-all-done = bf16[4,520,512]{2,1,0:T(8,128)(2,1)S(1)} async-done(((bf16[4,520,512]{2,1,0:T(8,128)(2,1)}), bf16[4,520,512]{2,1,0:T(8,128)(2,1)S(1)}, u32[]{:S(2)}, u32[]{:S(2)}) %all-to-all-start) | async-done | bytes 2129952 | tf_op jit(solution)/shard_map/all_to_all | solution.py:21
  80.5 1.9 collective-permute-start
  82.7 3.4 %collective-permute-done = bf16[4,16,512]{2,1,0:T(8,128)(2,1)S(1)} collective-permute-done((bf16[4,16,512]{2,1,0:T(8,128)(2,1)S(1)}, bf16[4,16,512]{2,1,0:T(8,128)(2,1)S(1)}, u32[]{:S(2)}, u32[]{:S(2)}) %collective-permute-start) | collective-permute-done | bytes 65568 | tf_op jit(solution)/shard_map/ppermute | solution.py:32
  86.6 1.3 select_bitcast_fusion.1
  88.3 1.3 fusion.87
  90.5 0.9 fusion.83
  92.8 0.9 fusion.30
  93.8 3.1 %while.13 = (s32[]{:T(128)}, f32[4,64,64]{2,1,0:T(8,128)S(1)}, f32[4,4,64,64]{3,2,1,0:T(8,128)}, f32[4,4]{1,0:T(4,128)S(1)}, f32[4,4,64,64]{3,2,1,0:T(8,128)S(1)}, /*index=5*/s32[]{:T(128)}, s32[]{:T(128)}) while((s32[]{:T(128)}, f32[4,64,64]{2,1,0:T(8,128)S(1)}, f32[4,4,64,64]{3,2,1,0:T(8,128)}, f32[4,4]{1,0:T(4,128)S(1)}, ...), condition=%wide.region_3.4_spmd.clone, body=%wide.region_2.3_spmd.clone.sunk | while | flops 65539 | bytes 393872 | solution.py:216
  93.8 0.7 bitcast_dynamic-update-slice_fusion.2
  94.6 0.7 bitcast_dynamic-update-slice_fusion.2
  95.4 0.7 bitcast_dynamic-update-slice_fusion.2
  96.1 0.7 bitcast_dynamic-update-slice_fusion.2
  97.1 16.4 %all-gather = bf16[2304,128]{1,0:T(8,128)(2,1)S(1)} all-gather(bf16[144,128]{1,0:T(8,128)(2,1)S(1)} %pad_maximum_fusion.3), channel_id=2, replica_groups=mesh['sp_0'=8,'sp_1'=8,'sp_2'=2,'tp'=4] {'sp_1','sp_2'}, dimensions={0}, use_global_device_ids=true | all-gather | bytes 626688 | tf_op jit(solution)/shard_map/all_gather | solution.py:227
  113.7 0.7 reduce_sum.144
  114.6 1.2 select_reduce_fusion.3
  116.1 1.4 mul.351
  117.5 0.8 copy.183
  118.5 1.3 mul.354
  119.9 2.0 fusion.13
  121.9 0.8 broadcast_in_dim.198
  122.6 8.3 %all-to-all-start.2 = ((bf16[8,144,128]{2,1,0:T(8,128)(2,1)}), bf16[8,144,128]{2,1,0:T(8,128)(2,1)S(1)}, u32[]{:S(2)}, u32[]{:S(2)}) async-start(bf16[8,144,128]{2,1,0:T(8,128)(2,1)} %broadcast_in_dim.198), calls=%async_computation.2 | async-start | bytes 589824 | tf_op jit(solution)/shard_map/all_to_all | solution.py:21
  131.9 12.7 %all-to-all-done.2 = bf16[8,144,128]{2,1,0:T(8,128)(2,1)S(1)} async-done(((bf16[8,144,128]{2,1,0:T(8,128)(2,1)}), bf16[8,144,128]{2,1,0:T(8,128)(2,1)S(1)}, u32[]{:S(2)}, u32[]{:S(2)}) %all-to-all-start.2) | async-done | bytes 294944 | tf_op jit(solution)/shard_map/all_to_all | solution.py:21
  145.5 0.7 reshape.293
  146.3 1.5 copy-done.2
  147.8 0.8 slice-done
  148.6 1.9 fusion.5
  151.4 0.9 slice_bitcast_fusion
  153.3 1.5 fusion.9
  154.8 2.9 %fusion.4 = f32[4,128,128,4]{1,2,3,0:T(8,128)S(1)} fusion(f32[4,128,4]{1,2,0:T(4,128)S(1)} %copy.174, pred[128,128]{0,1:T(8,128)(4,1)S(1)} %copy-done.15, f32[4,128,64]{1,2,0:T(8,128)S(1)} %copy.172, f32[4,128,64]{1,2,0:T(8,128)} %copy-done.11), kind=kOutput, calls=%fused_computation.19 | convolution fusion | flops 202113024 | bytes 1335296 | tf_op jit(solution)/shard_map/blhn,bshn->blsh/dot_general | solution.py:205
  157.7 1.9 fusion.7
  159.6 1.4 copy.198
  161.7 1.6 multiply_reduce_fusion
  163.9 3.2 %all-to-all-start.3 = ((f32[4,1,512]{2,1,0:T(1,128)}), f32[4,1,512]{2,1,0:T(1,128)S(1)}, u32[]{:S(2)}, u32[]{:S(2)}) async-start(f32[4,1,512]{2,1,0:T(1,128)} %broadcast_in_dim.204), calls=%async_computation.3 | async-start | bytes 16384 | tf_op jit(solution)/shard_map/all_to_all | solution.py:21
  167.3 4.5 %fusion.11 = f32[512,2048]{1,0:T(8,128)} fusion(bf16[2048,1088]{1,0:T(8,128)(2,1)} %all-gather.3.cloned.1.call-done, s32[]{:T(128)S(6)} %select_n.61, f32[1,512,256]{2,1,0:T(8,128)S(1)} %get-tuple-element.76, f32[1,512,256]{2,1,0:T(8,128)S(1)} %get-tuple-element.75, f32[1,512,256]{2,1,0:T(8,128)S(1)} %get-tuple-element.104, ...), kind=kOutput, calls=%fused_computation.33 | convolution fusion | flops 605159424 | bytes 7736324 | tf_op jit(solution)/shard_map/tc,dc->td/dot_general | solution.py:253
  171.8 0.6 all-to-all-done.3
  172.5 3.6 %add_convert_fusion = bf16[512,2048]{1,0:T(8,128)(2,1)S(1)} fusion(f32[512,2048]{1,0:T(8,128)} %fusion.11, f32[512]{0:T(512)S(1)} %add_rsqrt_fusion.1, bf16[2048,1088]{1,0:T(8,128)(2,1)} %all-gather.3.cloned.1.call-done, f32[512,256]{1,0:T(8,128)S(1)} %get-tuple-element.68, f32[256]{0:T(256)S(1)} %copy-done.50), kind=kOutput, calls=%fused_computation.9 | convolution fusion | flops 540278784 | bytes 7867392 | tf_op jit(solution)/shard_map/tc,dc->td/dot_general | solution.py:256
  176.3 29.3 %all_to_all.26 = bf16[4,512,512]{2,1,0:T(8,128)(2,1)S(1)} all-to-all(bf16[4,512,512]{2,1,0:T(8,128)(2,1)S(1)} %bitcast.151), channel_id=1, replica_groups=mesh['sp_0'=8,'sp_1'=8,'sp_2'=2,'tp'=4] {'tp'}, dimensions={0} | all-to-all | bytes 4194304 | tf_op jit(solution)/shard_map/all_to_all | solution.py:72
  205.6 1.2 reduce_sum.151
  (212 shorter events, 11.2 us)
Async XLA Ops:
  6.5 160.7 %copy-start = (bf16[1,256,256]{2,1,0:T(8,128)(2,1)S(1)}, bf16[1,256,256]{2,1,0:T(8,128)(2,1)}, u32[]{:S(2)}) copy-start(bf16[1,256,256]{2,1,0:T(8,128)(2,1)} %param.30) | copy-start | bytes 393220
  6.5 19.2 %copy-start.51 = (bf16[512]{0:T(512)(128)(2,1)S(1)}, bf16[512]{0:T(512)(128)(2,1)}, u32[]{:S(2)}) copy-start(bf16[512]{0:T(512)(128)(2,1)} %param.23) | copy-start | bytes 3076
  6.5 19.2 %copy-start.12 = (bf16[512,512]{1,0:T(8,128)(2,1)S(1)}, bf16[512,512]{1,0:T(8,128)(2,1)}, u32[]{:S(2)}) copy-start(bf16[512,512]{1,0:T(8,128)(2,1)} %param.22) | copy-start | bytes 1572868
  9.1 40.6 %all-to-all-start.1 = ((bf16[64,16,324]{2,1,0:T(8,128)(2,1)}), bf16[64,16,324]{2,1,0:T(8,128)(2,1)S(1)}, u32[]{:S(2)}, u32[]{:S(2)}) async-start(bf16[64,16,324]{2,1,0:T(8,128)(2,1)} %broadcast_in_dim.180), calls=%async_computation.1 | async-start | bytes 1572864 | tf_op jit(solution)/shard_map/all_to_all | solution.py:21
  49.7 1.7 copy-start.3
  51.3 4.5 %copy-start.25 = (bf16[16,256]{1,0:T(8,128)(2,1)S(1)}, bf16[16,256]{1,0:T(8,128)(2,1)}, u32[]{:S(2)}) copy-start(bf16[16,256]{1,0:T(8,128)(2,1)} %param.24) | copy-start | bytes 24580
  51.3 4.5 %copy-start.26 = (bf16[16,256]{1,0:T(8,128)(2,1)S(1)}, bf16[16,256]{1,0:T(8,128)(2,1)}, u32[]{:S(2)}) copy-start(bf16[16,256]{1,0:T(8,128)(2,1)} %param.25) | copy-start | bytes 24580
  51.3 4.5 %copy-start.27 = (bf16[256,16]{0,1:T(8,128)(2,1)S(1)}, bf16[256,16]{0,1:T(8,128)(2,1)}, u32[]{:S(2)}) copy-start(bf16[256,16]{0,1:T(8,128)(2,1)} %param.40) | copy-start | bytes 24580
  51.3 4.5 %copy-start.28 = (bf16[256,16]{0,1:T(8,128)(2,1)S(1)}, bf16[256,16]{0,1:T(8,128)(2,1)}, u32[]{:S(2)}) copy-start(bf16[256,16]{0,1:T(8,128)(2,1)} %param.41) | copy-start | bytes 24580
  51.3 4.5 %copy-start.33 = (bf16[16,64]{1,0:T(8,128)(2,1)S(1)}, bf16[16,64]{1,0:T(8,128)(2,1)}, u32[]{:S(2)}) copy-start(bf16[16,64]{1,0:T(8,128)(2,1)} %param.28) | copy-start | bytes 6148
  51.3 5.3 %copy-start.53 = (f32[4]{0:T(128)S(1)}, f32[4]{0:T(128)}, u32[]{:S(2)}) copy-start(f32[4]{0:T(128)} %param.38) | copy-start | bytes 52
  51.3 6.8 %copy-start.54 = (f32[4]{0:T(128)S(1)}, f32[4]{0:T(128)}, u32[]{:S(2)}) copy-start(f32[4]{0:T(128)} %param.36) | copy-start | bytes 52
  51.3 6.8 %copy-start.46 = (f32[4,64]{1,0:T(4,128)S(1)}, f32[4,64]{1,0:T(4,128)}, u32[]{:S(2)}) copy-start(f32[4,64]{1,0:T(4,128)} %param.33) | copy-start | bytes 3076
  51.3 6.8 %copy-start.34 = (f32[4,256]{1,0:T(4,128)S(1)}, f32[4,256]{1,0:T(4,128)}, u32[]{:S(2)}) copy-start(f32[4,256]{1,0:T(4,128)} %param.32) | copy-start | bytes 12292
  51.4 29.1 %all-to-all-start = ((bf16[4,520,512]{2,1,0:T(8,128)(2,1)}), bf16[4,520,512]{2,1,0:T(8,128)(2,1)S(1)}, u32[]{:S(2)}, u32[]{:S(2)}) async-start(bf16[4,520,512]{2,1,0:T(8,128)(2,1)} %broadcast_in_dim.179), calls=%async_computation | async-start | bytes 4259840 | tf_op jit(solution)/shard_map/all_to_all | solution.py:21
  55.8 90.4 %all-gather.3.cloned.1.call-start = ((), (), s32[]{:S(2)}) async-start(), calls=%async_computation.5 | async-start | bytes 4755456 | tf_op jit(solution)/shard_map/all_gather | solution.py:133
  57.4 25.0 %copy-start.41 = (pred[16]{0:T(512)(128)(4,1)}, pred[16]{0:T(512)(128)(4,1)S(1)}, u32[]{:S(2)}) copy-start(pred[16]{0:T(512)(128)(4,1)S(1)} %iota_compare_fusion.6) | copy-start | bytes 52
  57.5 25.0 %copy-start.43 = (pred[16]{0:T(512)(128)(4,1)}, pred[16]{0:T(512)(128)(4,1)S(1)}, u32[]{:S(2)}) copy-start(pred[16]{0:T(512)(128)(4,1)S(1)} %iota_compare_fusion.5) | copy-start | bytes 52
  58.2 33.4 %copy-start.16 = (f32[1,256]{1,0:T(1,128)}, f32[1,256]{1,0:T(1,128)S(1)}, u32[]{:S(2)}) copy-start(f32[1,256]{1,0:T(1,128)S(1)} %get-tuple-element.83) | copy-start | bytes 3076
  58.2 33.4 %copy-start.18 = (f32[1,256]{1,0:T(1,128)}, f32[1,256]{1,0:T(1,128)S(1)}, u32[]{:S(2)}) copy-start(f32[1,256]{1,0:T(1,128)S(1)} %get-tuple-element.84) | copy-start | bytes 3076
  58.2 33.4 %copy-start.20 = (f32[1,256]{1,0:T(1,128)}, f32[1,256]{1,0:T(1,128)S(1)}, u32[]{:S(2)}) copy-start(f32[1,256]{1,0:T(1,128)S(1)} %get-tuple-element.85) | copy-start | bytes 3076
  58.2 33.4 %copy-start.22 = (f32[1,256]{1,0:T(1,128)}, f32[1,256]{1,0:T(1,128)S(1)}, u32[]{:S(2)}) copy-start(f32[1,256]{1,0:T(1,128)S(1)} %get-tuple-element.86) | copy-start | bytes 3076
  58.2 28.4 %collective-permute-start.1 = (bf16[64,16,324]{2,1,0:T(8,128)(2,1)}, bf16[64,16,324]{2,1,0:T(8,128)(2,1)}, u32[]{:S(2)}, u32[]{:S(2)}) collective-permute-start(bf16[64,16,324]{2,1,0:T(8,128)(2,1)} %copy-done.3), channel_id=1, source_target_pairs={{0,4},{4,0},{1,5},{5,1},{2,6},{6,2},{3,7},{7,3},{8,12},{12,8},{9,1... | collective-permute-start | bytes 1990664 | tf_op jit(solution)/shard_map/ppermute | solution.py:122
  80.5 5.6 %collective-permute-start = (bf16[4,16,512]{2,1,0:T(8,128)(2,1)S(1)}, bf16[4,16,512]{2,1,0:T(8,128)(2,1)S(1)}, u32[]{:S(2)}, u32[]{:S(2)}) collective-permute-start(bf16[4,16,512]{2,1,0:T(8,128)(2,1)S(1)} %slice.234), channel_id=1, source_target_pairs={{0,4},{4,8},{8,12},{12,16},{16,20},{20,24},{24,28},{28,32},{32,36}... | collective-permute-start | bytes 196616 | tf_op jit(solution)/shard_map/ppermute | solution.py:32
  82.4 5.8 %copy-start.29 = (f32[4,1,512]{2,0,1:T(4,128)}, f32[4,1,512]{2,0,1:T(4,128)S(1)}, u32[]{:S(2)}) copy-start(f32[4,1,512]{2,0,1:T(4,128)S(1)} %copy.213) | copy-start | bytes 24580
  82.5 4.2 %copy-start.4 = (bf16[64,16,324]{2,1,0:T(8,128)(2,1)S(1)}, bf16[64,16,324]{2,1,0:T(8,128)(2,1)}, u32[]{:S(2)}) copy-start(bf16[64,16,324]{2,1,0:T(8,128)(2,1)} %copy-done.3) | copy-start | bytes 1990660
  82.7 5.6 %copy-start.1 = (bf16[4,512,512]{2,1,0:T(8,128)(2,1)}, bf16[4,512,512]{2,1,0:T(8,128)(2,1)S(1)}, u32[]{:S(2)}) copy-start(bf16[4,512,512]{2,1,0:T(8,128)(2,1)S(1)} %slice.235) | copy-start | bytes 6291460
  86.1 2.1 copy-start.13
  93.8 20.8 %copy-start.42 = (pred[16]{0:T(512)(128)(4,1)S(1)}, pred[16]{0:T(512)(128)(4,1)}, u32[]{:S(2)}) copy-start(pred[16]{0:T(512)(128)(4,1)} %copy-done.41) | copy-start | bytes 52
  93.8 20.8 %copy-start.44 = (pred[16]{0:T(512)(128)(4,1)S(1)}, pred[16]{0:T(512)(128)(4,1)}, u32[]{:S(2)}) copy-start(pred[16]{0:T(512)(128)(4,1)} %copy-done.43) | copy-start | bytes 52
  113.5 2.3 %copy-start.5 = (bf16[2304,128]{1,0:T(8,128)(2,1)}, bf16[2304,128]{1,0:T(8,128)(2,1)S(1)}, u32[]{:S(2)}) copy-start(bf16[2304,128]{1,0:T(8,128)(2,1)S(1)} %all-gather) | copy-start | bytes 1769476
  119.8 11.2 %copy-start.47 = (f32[4,64]{1,0:T(4,128)S(1)}, f32[4,64]{1,0:T(4,128)}, u32[]{:S(2)}) copy-start(f32[4,64]{1,0:T(4,128)} %param.34) | copy-start | bytes 3076
  119.8 11.9 %copy-start.9 = (f32[4,128,4]{2,1,0:T(8,128)S(1)}, f32[4,128,4]{2,1,0:T(8,128)}, u32[]{:S(2)}) copy-start(f32[4,128,4]{2,1,0:T(8,128)} %get-tuple-element.80) | copy-start | bytes 24580
  119.8 12.0 %copy-start.8 = (f32[4,128,4]{2,1,0:T(8,128)S(1)}, f32[4,128,4]{2,1,0:T(8,128)}, u32[]{:S(2)}) copy-start(f32[4,128,4]{2,1,0:T(8,128)} %get-tuple-element.82) | copy-start | bytes 24580
  119.9 25.0 %copy-start.45 = (f32[4]{0:T(128)S(1)}, f32[4]{0:T(128)}, u32[]{:S(2)}) copy-start(f32[4]{0:T(128)} %get-tuple-element.97) | copy-start | bytes 52
  122.6 22.0 %all-to-all-start.2 = ((bf16[8,144,128]{2,1,0:T(8,128)(2,1)}), bf16[8,144,128]{2,1,0:T(8,128)(2,1)S(1)}, u32[]{:S(2)}, u32[]{:S(2)}) async-start(bf16[8,144,128]{2,1,0:T(8,128)(2,1)} %broadcast_in_dim.198), calls=%async_computation.2 | async-start | bytes 589824 | tf_op jit(solution)/shard_map/all_to_all | solution.py:21
  146.2 2.4 %slice-start = ((bf16[2048,1088]{1,0:T(8,128)(2,1)}), bf16[2048,576]{1,0:T(8,128)(2,1)S(1)}, s32[]{:S(2)}) async-start(bf16[2048,1088]{1,0:T(8,128)(2,1)} %all-gather.3.cloned.1.call-done), calls=%async_computation.6 | async-start | bytes 5242880 | tf_op jit(solution)/shard_map/slice | solution.py:150
  152.3 2.5 %copy-start.15 = (pred[128,128]{0,1:T(8,128)(4,1)S(1)}, pred[128,128]{0,1:T(8,128)(4,1)}, u32[]{:S(2)}) copy-start(pred[128,128]{0,1:T(8,128)(4,1)} %iota_compare_fusion) | copy-start | bytes 49156
  159.6 2.1 copy-start.17
  159.6 2.1 copy-start.19
  159.6 2.1 copy-start.21
  159.6 2.1 copy-start.23
  159.6 2.1 copy-start.32
  161.7 5.6 %copy-start.6 = (f32[1,512,256]{2,1,0:T(8,128)S(1)}, f32[1,512,256]{2,1,0:T(8,128)}, u32[]{:S(2)}) copy-start(f32[1,512,256]{2,1,0:T(8,128)} %get-tuple-element.105) | copy-start | bytes 1572868
  161.7 5.6 %copy-start.24 = (f32[512]{0:T(512)S(1)}, f32[512]{0:T(512)}, u32[]{:S(2)}) copy-start(f32[512]{0:T(512)} %add_minimum_fusion) | copy-start | bytes 6148
  161.7 5.6 %copy-start.49 = (f32[256]{0:T(256)S(1)}, f32[256]{0:T(256)}, u32[]{:S(2)}) copy-start(f32[256]{0:T(256)} %param.31) | copy-start | bytes 3076
  163.9 8.5 %all-to-all-start.3 = ((f32[4,1,512]{2,1,0:T(1,128)}), f32[4,1,512]{2,1,0:T(1,128)S(1)}, u32[]{:S(2)}, u32[]{:S(2)}) async-start(f32[4,1,512]{2,1,0:T(1,128)} %broadcast_in_dim.204), calls=%async_computation.3 | async-start | bytes 16384 | tf_op jit(solution)/shard_map/all_to_all | solution.py:21
  167.3 5.2 %copy-start.50 = (f32[256]{0:T(256)S(1)}, f32[256]{0:T(256)}, u32[]{:S(2)}) copy-start(f32[256]{0:T(256)} %param.39) | copy-start | bytes 3076
  (15 other events, 19.7 us)
Sparse Core Ops, SparseCore 0:
  59.8 81.6 all-gather.2

commit v2 on v1

v2 whole, which is shorter than its diff:
```python
import jax
import jax.numpy as jnp
from jax import lax
from jax.experimental import pallas as pl
from jax.experimental.pallas import tpu as pltpu
from jax.sharding import Mesh
from jax.sharding import PartitionSpec as P

D = 2048
POOL_GROUPS = 4
HEAD = 64
MIX_W = 1024
HALO = 16
PAY = 16
BLOCK = 128
SP = ("sp_0", "sp_1", "sp_2")
EPSILON = 1e-06
HIGH = lax.Precision.HIGHEST
F32 = jnp.float32
BF16 = jnp.bfloat16


def sent_to_all(array, axis):
    copies = jnp.broadcast_to(array, (lax.axis_size(axis), *array.shape))
    return lax.all_to_all(copies, axis, split_axis=0, concat_axis=0, tiled=True)


def dot(a, b, left=1, right=0, precision=None):
    return lax.dot_general(
        a, b, (((left,), (right,)), ((), ())), precision=precision, preferred_element_type=F32
    )


def silu(x):
    return x * jax.nn.sigmoid(x)


def heads_of_lanes(lanes):
    head = lax.broadcasted_iota(jnp.int32, (8, lanes), 0)
    lane = lax.broadcasted_iota(jnp.int32, (8, lanes), 1)
    return (head == lane // HEAD).astype(F32)


def convolved(raw, taps, length):
    width = taps.shape[0]
    total = jnp.zeros((length, raw.shape[1]), F32)
    for k in range(width):
        at = HALO - width + 1 + k
        total = total + taps[k : k + 1] * raw[at : at + length]
    return silu(total).astype(BF16)


def write_payload(ref, state, log_row):
    rows = state.shape[0]
    high = log_row.astype(BF16).astype(F32)
    middle = (log_row - high).astype(BF16).astype(F32)
    low = log_row - high - middle
    at = lax.broadcasted_iota(jnp.int32, (PAY, log_row.shape[1]), 0)
    tail = jnp.where(at == 0, high, jnp.where(at == 1, middle, jnp.where(at == 2, low, 0.0)))
    ref[:rows] = state.astype(BF16)
    ref[rows:] = tail.astype(BF16)


def read_payload(ref, k):
    rows = ref.shape[1] - PAY
    tail = ref[k, rows:].astype(F32)
    return ref[k, :rows].astype(F32), jnp.sum(tail, axis=0, keepdims=True)


def scan_payloads(ref, place):
    rows, lanes = ref.shape[1] - PAY, ref.shape[2]
    total = before = jnp.zeros((rows, lanes), F32)
    logs = logs_before = jnp.zeros((1, lanes), F32)
    for k in range(ref.shape[0]):
        state, log_row = read_payload(ref, k)
        total = total * jnp.exp(log_row) + state
        logs = logs + log_row
        before = jnp.where(k < place, total, before)
        logs_before = jnp.where(k < place, logs, logs_before)
    return total, logs, before, logs_before


def first_kernel(
    at, x0, x1, x2, x3, mine, other, taps, bias, rate, extra,
    normed, value_out, key_out, cum_out, step_out, payload, weight,
):
    core = at[1]
    weight[:, pl.ds(core, 1)] = mine[...][:, None]
    weight[:, pl.ds(1 - core, 1)] = other[...][:, None]
    pieces = (x0, x1, x2, x3)
    total_rows = x0.shape[0] - PAY
    length = total_rows - HALO
    squares = jnp.zeros((total_rows, 1), F32)
    for piece in pieces:
        values = piece[:total_rows].astype(F32)
        squares = squares + jnp.sum(values * values, axis=1, keepdims=True)
    scale = lax.rsqrt(squares / D + EPSILON)
    chips, columns = weight.shape[0] // 4, weight.shape[3]
    acc = jnp.zeros((total_rows, columns), F32)
    for k, piece in enumerate(pieces):
        gain = piece[total_rows : total_rows + 1].astype(F32)
        part = (piece[:total_rows].astype(F32) * scale * gain).astype(BF16)
        normed[k] = part
        block = weight[pl.ds(((at[0] - k) & 3) * chips, chips)]
        acc = acc + dot(part, block.reshape(-1, columns))
    mix = value_out.shape[1]
    done = convolved(acc.astype(BF16).astype(F32), taps[...], length)
    value_out[...] = done[:, :mix]
    key_out[...] = done[:, mix:]
    raw = jnp.transpose(acc[HALO:, mix:])[HEAD : HEAD + 8] + bias[...]
    step = jnp.maximum(raw, 0.0) + jnp.log1p(jnp.exp(-jnp.abs(raw)))
    decay = rate[...] * step + extra[...]
    rows = lax.broadcasted_iota(jnp.int32, (BLOCK, BLOCK), 0)
    upper = (rows <= lax.broadcasted_iota(jnp.int32, (BLOCK, BLOCK), 1)).astype(F32)
    carry, cums = jnp.zeros((8, 1), F32), []
    for b in range(length // BLOCK):
        cums.append(dot(decay[:, b * BLOCK : (b + 1) * BLOCK], upper, precision=HIGH) + carry)
        carry = cums[-1][:, BLOCK - 1 :]
    cum = jnp.concatenate(cums, axis=1)
    cum_out[...] = cum
    step_out[...] = step
    lanes = heads_of_lanes(mix)
    spread = dot(jnp.exp(carry - cum) * step, lanes, 0, 0, HIGH)
    state = dot(done[:, mix:].astype(F32), done[:, :mix].astype(F32) * spread, 0, 0, HIGH)
    write_payload(payload, state[:HEAD], jnp.sum(carry * lanes, axis=0, keepdims=True))


def row_kernel(at, rows, before_out, logs_out, payload):
    total, logs, before, logs_before = scan_payloads(rows, at[2])
    before_out[...] = before
    logs_out[...] = jnp.broadcast_to(logs_before, logs_out.shape)
    write_payload(payload, total, logs)


def second_kernel(
    at, normed, weight, weight_read, value, key, cum, step, taps, mix_weight, pool_scale, skip,
    pool_out, gate_out, read_out, local_out,
):
    length, span = pool_out.shape
    total_rows = normed.shape[1]
    acc = jnp.zeros((total_rows, weight.shape[1]), F32)
    acc_read = jnp.zeros((total_rows, weight_read.shape[1]), F32)
    width = normed.shape[2]
    for k in range(normed.shape[0]):
        start = pl.multiple_of(((at[0] - k) & 3) * width, width)
        acc = acc + dot(normed[k], weight[pl.ds(start, width)])
        acc_read = acc_read + dot(normed[k], weight_read[pl.ds(start, width)])
    gate_out[...] = acc[HALO:, span:].astype(BF16)
    running = acc[:, :span].astype(BF16).astype(F32)
    own = running[HALO:]
    chosen = own
    for level in range(POOL_GROUPS):
        stride = 2**level
        running = running[stride:] + running[:-stride]
        chosen = jnp.where(at[0] == level, running[running.shape[0] - length :], chosen)
    position = at[4] * length + lax.broadcasted_iota(jnp.int32, (length, 1), 0) + 1
    counts = jnp.minimum(position, 2 << at[0]).astype(F32)
    pooled = (chosen / counts - own).astype(BF16)
    pool_out[...] = (dot(pooled, mix_weight[...]) * pool_scale[...]).astype(BF16)
    reads = convolved(acc_read.astype(BF16).astype(F32), taps[...], length)
    read_out[...] = reads
    lanes = heads_of_lanes(span)
    values = value[...].astype(F32)
    scaled = (values * dot(step[...], lanes, 0, 0, HIGH)).astype(BF16)
    columns = jnp.transpose(cum[...])
    lower = lax.broadcasted_iota(jnp.int32, (BLOCK, BLOCK), 0) >= lax.broadcasted_iota(
        jnp.int32, (BLOCK, BLOCK), 1
    )
    for i in range(length // BLOCK):
        here = slice(i * BLOCK, (i + 1) * BLOCK)
        products = [
            dot(reads[here], key[j * BLOCK : (j + 1) * BLOCK], 1, 1) for j in range(i + 1)
        ]
        results = []
        for h in range(span // HEAD):
            parts = []
            for j in range(i + 1):
                gap = columns[here, h : h + 1] - cum[h : h + 1, j * BLOCK : (j + 1) * BLOCK]
                if i == j:
                    gap = jnp.where(lower, gap, -jnp.inf)
                parts.append((products[j] * jnp.exp(gap)).astype(BF16))
            left = jnp.concatenate(parts, axis=1)
            right = scaled[: (i + 1) * BLOCK, h * HEAD : (h + 1) * HEAD]
            results.append(dot(left, right))
        local_out[here] = jnp.concatenate(results, axis=1) + skip[...] * values[here]


def third_kernel(
    at, planes, before, logs_before, reads, local_in, gate, cum, gain, rows_out, squares_out
):
    _, _, earlier, _ = scan_payloads(planes, at[3])
    incoming = earlier * jnp.exp(logs_before[:1]) + before[...]
    lanes = heads_of_lanes(local_in.shape[1])
    decay = dot(jnp.exp(cum[...]), lanes, 0, 0, HIGH)
    far = dot(reads[:, :HEAD].astype(F32), incoming, precision=HIGH) * decay
    gated = (local_in[...] + far) * silu(gate[...].astype(F32))
    ones = jnp.ones((8, gated.shape[1]), F32)
    squares_out[...] = dot(ones, gated * gated, 1, 1, HIGH)
    rows_out[...] = (gated * gain[...]).astype(BF16)


def out_kernel(pool, rows, squares, weight, out):
    span = pool.shape[1]
    mean = jnp.sum(squares[...], axis=0) / MIX_W
    scale = jnp.transpose(lax.rsqrt(mean + EPSILON))[:, :1]
    for d in range(out.shape[0]):
        width = out.shape[2]
        block = weight[d * width : (d + 1) * width]
        terms = dot(pool[...], block[:, :span], 1, 1)
        terms = terms + dot(rows[...], block[:, span:], 1, 1) * scale
        out[d] = terms.astype(BF16)


def whole(shape):
    return pl.BlockSpec(shape, lambda *_: (0,) * len(shape))


SMEM = pl.BlockSpec(memory_space=pltpu.SMEM)


def call(kernel, args, outs, flops, scratch=(), specs=None):
    specs = specs or {}
    moved = sum(a.size * a.dtype.itemsize for a in args)
    return pl.pallas_call(
        kernel,
        grid=(1,),
        in_specs=[specs.get(k, whole(a.shape)) for k, a in enumerate(args)],
        out_specs=[whole(o.shape) for o in outs],
        out_shape=outs,
        scratch_shapes=list(scratch),
        compiler_params=pltpu.CompilerParams(vmem_limit_bytes=48 * 1024 * 1024),
        cost_estimate=pl.CostEstimate(flops=flops, transcendentals=0, bytes_accessed=moved),
    )(*args)


def shape_of(shape, dtype):
    return jax.ShapeDtypeStruct(shape, dtype)


def columns_of(array):
    return jnp.pad(array[:, None], ((0, 8 - array.shape[0]), (0, 0)))


def local(
    activations,
    norm_gain,
    pool_weight,
    gate_weight,
    value_weight,
    key_weight,
    read_weight,
    step_weight,
    pool_mix,
    pool_scale,
    taps_value,
    taps_key,
    taps_read,
    step_bias,
    decay_log,
    decay_extra,
    skip_scale,
    state_gain,
    out_pool_weight,
    out_state_weight,
):
    length, width = activations.shape
    mix = value_weight.shape[1]
    state = key_weight.shape[1]
    heads = step_weight.shape[1]
    count = lax.axis_size("tp")
    at = jnp.stack(
        [
            lax.axis_index("tp"),
            lax.axis_index("sp_2"),
            lax.axis_index(("sp_1", "sp_2")),
            lax.axis_index("sp_0"),
            lax.axis_index(SP),
        ]
    ).astype(jnp.int32)
    fill = jnp.zeros((read_weight.shape[0], BLOCK - state), BF16)
    joined = jnp.concatenate(
        [
            pool_weight,
            gate_weight,
            jnp.transpose(out_pool_weight),
            jnp.transpose(out_state_weight),
            read_weight,
            fill,
        ],
        axis=1,
    )
    later_weights = lax.all_gather(joined, SP, axis=0, tiled=True)
    fill = jnp.zeros((key_weight.shape[0], BLOCK - state - heads), BF16)
    first_weights = jnp.concatenate([value_weight, key_weight, step_weight, fill], axis=1)
    mine = sent_to_all(first_weights, ("sp_0", "sp_1"))
    other = lax.ppermute(mine, "sp_2", [(0, 1), (1, 0)])
    size = lax.axis_size(SP)
    before = lax.ppermute(activations[length - HALO :], SP, [(k, k + 1) for k in range(size - 1)])
    gains = jnp.broadcast_to(norm_gain[None, :], (PAY, width))
    sent = jnp.concatenate([before, activations, gains], axis=0)
    pieces = [sent] + [
        lax.ppermute(sent, "tp", [(k, (k + shift) % count) for k in range(count)])
        for shift in range(1, count)
    ]
    taps = jnp.pad(
        jnp.concatenate([taps_value, taps_key], axis=1), ((0, 0), (0, BLOCK - state))
    )
    extra = jnp.pad(jnp.transpose(decay_extra), ((0, 8 - heads), (0, 0)))
    rows = HALO + length
    columns = mix + BLOCK
    pay = shape_of((HEAD + PAY, mix), BF16)
    normed, value, key, cum, step, payload = call(
        first_kernel,
        (at, *pieces, mine, other, taps, columns_of(step_bias), columns_of(-jnp.exp(decay_log)), extra),
        (
            shape_of((count, rows, width), BF16),
            shape_of((length, mix), BF16),
            shape_of((length, BLOCK), BF16),
            shape_of((8, length), F32),
            shape_of((8, length), F32),
            pay,
        ),
        2 * rows * D * columns,
        [pltpu.VMEM((mine.shape[0], 2, mine.shape[1], columns), BF16)],
        {0: SMEM},
    )
    row_pieces = lax.all_gather(payload, ("sp_1", "sp_2"))
    before_row, logs_row, payload = call(
        row_kernel,
        (at, row_pieces),
        (shape_of((HEAD, mix), F32), shape_of((8, mix), F32), pay),
        10**6,
        specs={0: SMEM},
    )
    plane_pieces = sent_to_all(payload, "sp_0")
    taps_r = jnp.pad(taps_read, ((0, 0), (0, BLOCK - state)))
    pool_out, gate, reads, inside = call(
        second_kernel,
        (
            at, normed, later_weights, later_weights, value, key, cum, step, taps_r,
            pool_mix[0], pool_scale[None, :], jnp.repeat(skip_scale, HEAD)[None, :],
        ),
        (
            shape_of((length, mix), BF16),
            shape_of((length, mix), BF16),
            shape_of((length, BLOCK), BF16),
            shape_of((length, mix), F32),
        ),
        2 * rows * D * (2 * mix + BLOCK),
        specs={
            0: SMEM,
            2: pl.BlockSpec((D, 2 * mix), lambda *_: (0, 0)),
            3: pl.BlockSpec((D, BLOCK), lambda *_: (0, 4 * mix // BLOCK)),
        },
    )
    gated, squares = call(
        third_kernel,
        (at, plane_pieces, before_row, logs_row, reads, inside, gate, cum, state_gain[None, :]),
        (shape_of((length, mix), BF16), shape_of((8, length), F32)),
        10**7,
        specs={0: SMEM},
    )
    all_squares = sent_to_all(squares, "tp")
    terms = call(
        out_kernel,
        (pool_out, gated, all_squares, later_weights),
        (shape_of((count, length, width), BF16),),
        2 * length * 2 * mix * D,
        specs={3: pl.BlockSpec((D, 2 * mix), lambda *_: (0, 1))},
    )[0]
    arrived = lax.all_to_all(terms, "tp", split_axis=0, concat_axis=0, tiled=True)
    return arrived.astype(F32).sum(axis=0).astype(BF16)


def solution(mesh):
    torus = Mesh(mesh.devices.reshape(8, 8, 2, mesh.shape["tp"]), ("sp_0", "sp_1", "sp_2", "tp"))
    placed = (
        P(SP, "tp"),
        P("tp"),
        P(SP, "tp"),
        P(SP, "tp"),
        P(SP, "tp"),
        P(SP, "tp"),
        P(SP, "tp"),
        P(SP, "tp"),
        P("tp", None, None),
        P("tp"),
        P(None, "tp"),
        P(None, "tp"),
        P(None, "tp"),
        P("tp"),
        P("tp"),
        P(SP, "tp"),
        P("tp"),
        P("tp"),
        P("tp", SP),
        P("tp", SP),
    )
    return jax.shard_map(local, mesh=torus, in_specs=placed, out_specs=P(SP, "tp"), check_vma=False)
```

time: 215 us -> 187 us (0.87)
  the two profiles are of different devices: /device:TPU:8 before, /device:TPU:2 now
where the time goes in v2:
time: 187 us; the launch traced here: 186 us
  blocking collectives  95 us (51%)
  waiting for transfers between devices  26.3 us (14%)
  starting transfers between devices  19.9 us (11%)
  Pallas kernels  17.3 us (9%)
  between operations  13.7 us (7%)
  local copies, waits for them, and re-layouts  12.2 us (7%)
  other arithmetic  2.08 us (1%)
    all_to_all x2, blocking collectives, sent_to_all(): return lax.all_to_all(copies, axis, split_axis=0, concat_axis=0, tiled=True)  49.3 us
    all_to_all x1, blocking collectives, local(): lax.all_to_all(terms, 'tp', split_axis=0, concat_axis=0, tiled=True)  27.8 us
    ppermute x3, waiting for transfers between devices, local(): lax.ppermute(sent, 'tp', [(k, (k + shift) % count) for k in range(count)])  21.2 us
    all_gather x1, blocking collectives, local(): row_pieces = lax.all_gather(payload, ('sp_1', 'sp_2'))  17.9 us
    pallas_call x5, Pallas kernels, call(): pl.pallas_call(kernel, grid=(1,), in_specs=[specs.get(k, whole(a.shape))...  17.3 us
    ppermute x3, starting transfers between devices, local(): lax.ppermute(sent, 'tp', [(k, (k + shift) % count) for k in range(count)])  10.5 us
    unnamed x51, local copies, waits for them, and re-layouts  7.68 us
    all_to_all x1, starting transfers between devices, sent_to_all(): return lax.all_to_all(copies, axis, split_axis=0, concat_axis=0, tiled=True)  5.13 us
  transfers between devices with their start and end apart: 7, of which 5 were waited for; matrix products, arithmetic and copies ran while one was open for 3% of the time, Pallas kernels for 7%

profile of v2, /device:TPU:2, one launch (start us, length us, event | category | flops | bytes accessed | tf_op | source)
XLA Modules:
  0.0 186.5 jit_solution(6738050947183245561)
XLA Ops:
  6.5 1.4 concatenate.15
  8.0 0.0 all-gather.3.cloned.1.call-update
  8.0 0.8 copy.21
  8.8 0.1 pad.29.clone
  8.9 0.8 maximum_maximum_fusion
  9.7 0.1 broadcast_in_dim.38
  9.7 0.0 copy-start.24
  9.7 0.0 copy-start.17
  9.8 0.0 copy-start.20
  9.8 41.5 %all_to_all.20.mine = bf16[64,16,384]{2,1,0:T(8,128)(2,1)S(1)} all-to-all(bf16[64,16,384]{2,1,0:T(8,128)(2,1)S(1)} %broadcast_in_dim.38), channel_id=1, replica_groups=mesh['sp_0'=8,'sp_1'=8,'sp_2'=2,'tp'=4] {'sp_0','sp_1'}, dimensions={0} | all-to-all | bytes 1572864 | tf_op jit(solution)/shard_map/all_to_all | solution.py:25
  51.3 1.9 %collective-permute-start.4 = (bf16[64,16,384]{2,1,0:T(8,128)(2,1)S(1)}, bf16[64,16,384]{2,1,0:T(8,128)(2,1)S(1)}, u32[]{:S(2)}, u32[]{:S(2)}) collective-permute-start(bf16[64,16,384]{2,1,0:T(8,128)(2,1)S(1)} %all_to_all.20.mine), channel_id=1, source_target_pairs={{0,4},{4,0},{1,5},{5,1},{2,6},{6,2},{3,7},{7,3},{8,12},{12,8},{9,1... | collective-permute-start | bytes 2359304 | tf_op jit(solution)/shard_map/ppermute | solution.py:296
  53.2 2.4 %collective-permute-start = (bf16[16,512]{1,0:T(8,128)(2,1)S(1)}, bf16[16,512]{1,0:T(8,128)(2,1)S(1)}, u32[]{:S(2)}, u32[]{:S(2)}) collective-permute-start(bf16[16,512]{1,0:T(8,128)(2,1)S(1)} %slice.3), channel_id=1, source_target_pairs={{0,4},{4,8},{8,12},{12,16},{16,20},{20,24},{24,28},{28,32},{32,36}... | collective-permute-start | bytes 49160 | tf_op jit(solution)/shard_map/ppermute | solution.py:298
  55.6 0.8 collective-permute-done
  56.5 3.4 %collective-permute-start.1 = (bf16[544,512]{1,0:T(8,128)(2,1)S(1)}, bf16[544,512]{1,0:T(8,128)(2,1)S(1)}, u32[]{:S(2)}, u32[]{:S(2)}) collective-permute-start(bf16[544,512]{1,0:T(8,128)(2,1)S(1)} %pad_maximum_fusion.x0), channel_id=1, source_target_pairs={{0,1},{1,2},{2,3},{3,0},{4,5},{5,6},{6,7},{7,4},{8,9},{9,10},{10,1... | collective-permute-start | bytes 1671176 | tf_op jit(solution)/shard_map/ppermute | solution.py:302
  59.9 3.0 %collective-permute-start.2 = (bf16[544,512]{1,0:T(8,128)(2,1)S(1)}, bf16[544,512]{1,0:T(8,128)(2,1)S(1)}, u32[]{:S(2)}, u32[]{:S(2)}) collective-permute-start(bf16[544,512]{1,0:T(8,128)(2,1)S(1)} %pad_maximum_fusion.x0), channel_id=1, source_target_pairs={{0,2},{1,3},{2,0},{3,1},{4,6},{5,7},{6,4},{7,5},{8,10},{9,11},{10,... | collective-permute-start | bytes 1671176 | tf_op jit(solution)/shard_map/ppermute | solution.py:302
  62.9 4.1 %collective-permute-start.3 = (bf16[544,512]{1,0:T(8,128)(2,1)S(1)}, bf16[544,512]{1,0:T(8,128)(2,1)}, u32[]{:S(2)}, u32[]{:S(2)}) collective-permute-start(bf16[544,512]{1,0:T(8,128)(2,1)S(1)} %pad_maximum_fusion.x0), channel_id=1, source_target_pairs={{0,3},{1,0},{2,1},{3,2},{4,7},{5,4},{6,5},{7,6},{8,11},{9,8},{10,9... | collective-permute-start | bytes 1671176 | tf_op jit(solution)/shard_map/ppermute | solution.py:302
  67.0 0.1 copy.23
  67.1 0.6 pad.21.rate
  67.7 0.1 copy.22
  67.8 0.6 pad.20.bias
  68.4 0.6 stack.23.at
  69.0 4.8 %collective-permute-done.1.x1 = bf16[544,512]{1,0:T(8,128)(2,1)S(1)} collective-permute-done((bf16[544,512]{1,0:T(8,128)(2,1)S(1)}, bf16[544,512]{1,0:T(8,128)(2,1)S(1)}, u32[]{:S(2)}, u32[]{:S(2)}) %collective-permute-start.1) | collective-permute-done | bytes 557088 | tf_op jit(solution)/shard_map/ppermute | solution.py:302
  73.9 5.0 %collective-permute-done.2.x2 = bf16[544,512]{1,0:T(8,128)(2,1)S(1)} collective-permute-done((bf16[544,512]{1,0:T(8,128)(2,1)S(1)}, bf16[544,512]{1,0:T(8,128)(2,1)S(1)}, u32[]{:S(2)}, u32[]{:S(2)}) %collective-permute-start.2) | collective-permute-done | bytes 557088 | tf_op jit(solution)/shard_map/ppermute | solution.py:302
  78.8 11.4 %collective-permute-done.3.x3 = bf16[544,512]{1,0:T(8,128)(2,1)} collective-permute-done((bf16[544,512]{1,0:T(8,128)(2,1)S(1)}, bf16[544,512]{1,0:T(8,128)(2,1)}, u32[]{:S(2)}, u32[]{:S(2)}) %collective-permute-start.3) | collective-permute-done | bytes 557088 | tf_op jit(solution)/shard_map/ppermute | solution.py:302
  90.3 0.7 copy-done.10
  91.0 0.7 copy-done.11
  91.6 0.6 copy-done.12
  92.2 5.1 %shard_map.190 = (bf16[4,528,512]{2,1,0:T(8,128)(2,1)}, bf16[512,256]{1,0:T(8,128)(2,1)S(1)}, bf16[512,128]{1,0:T(8,128)(2,1)S(1)}, f32[8,512]{1,0:T(8,128)S(1)}...) custom-call(s32[5]{0:T(128)S(1)} %copy-done.12, bf16[544,512]{1,0:T(8,128)(2,1)S(1)} %pad_maximum_fusion.x0, ...), custom_call_target="tpu_custom_call" | custom-call | flops 830472192 | bytes 3823700 | tf_op jit(solution)/shard_map/pallas_call | solution.py:224
  97.4 17.9 %all-gather = bf16[1280,256]{1,0:T(8,128)(2,1)S(1)} all-gather(bf16[80,256]{1,0:T(8,128)(2,1)S(1)} %get-tuple-element.26), channel_id=2, replica_groups=mesh['sp_0'=8,'sp_1'=8,'sp_2'=2,'tp'=4] {'sp_1','sp_2'}, dimensions={0}, use_global_device_ids=true | all-gather | bytes 696320 | tf_op jit(solution)/shard_map/all_gather | solution.py:327
  115.3 0.8 shard_map.192
  116.0 0.7 broadcast_in_dim.44
  116.8 5.1 %all-to-all-start.1 = ((bf16[8,80,256]{2,1,0:T(8,128)(2,1)}), bf16[8,80,256]{2,1,0:T(8,128)(2,1)S(1)}, u32[]{:S(2)}, u32[]{:S(2)}) async-start(bf16[8,80,256]{2,1,0:T(8,128)(2,1)} %broadcast_in_dim.44), calls=%async_computation.1 | async-start | bytes 655360 | tf_op jit(solution)/shard_map/all_to_all | solution.py:25
  121.9 0.1 broadcast_in_dim.43
  122.0 0.1 broadcast_in_dim_reshape.3.skip
  122.1 0.0 all-gather.3.cloned.1.call-done.weight.weight_read
  122.1 0.9 copy-done.7
  123.0 6.4 %shard_map.191 = (bf16[512,256]{1,0:T(8,128)(2,1)S(1)}, bf16[512,256]{1,0:T(8,128)(2,1)S(1)}, bf16[512,128]{1,0:T(8,128)(2,1)S(1)}, f32[512,256]{1,0:T(8,128)S(1)}) custom-call(s32[5]{0:T(128)S(1)} %copy-done.13, bf16[4,528,512]{2,1,0:T(8,128)(2,1)S(1)} %copy-done, bf16[2048,1152]{1,0:T(8,128)(2,1)} %all-gather.3.cloned.1.call-done.weight.weight_read, ...), custom_call_target="tpu_custom_call" | custom-call | flops 1384120320 | bytes 12161044 | tf_op jit(solution)/shard_map/pallas_call | solution.py:224
  129.4 0.7 copy-done.1
  130.1 0.7 copy-done.3
  130.8 0.7 copy-done.8
  131.5 4.2 %all-to-all-done.1.planes = bf16[8,80,256]{2,1,0:T(8,128)(2,1)S(1)} async-done(((bf16[8,80,256]{2,1,0:T(8,128)(2,1)}), bf16[8,80,256]{2,1,0:T(8,128)(2,1)S(1)}, u32[]{:S(2)}, u32[]{:S(2)}) %all-to-all-start.1) | async-done | bytes 327712 | tf_op jit(solution)/shard_map/all_to_all | solution.py:25
  135.7 1.0 copy-done.4
  136.7 0.9 copy-done.9
  137.6 2.1 %shard_map.193 = (bf16[512,256]{1,0:T(8,128)(2,1)S(1)}, f32[8,512]{1,0:T(8,128)S(1)}) custom-call(s32[5]{0:T(128)S(1)} %copy-done.13, bf16[8,80,256]{2,1,0:T(8,128)(2,1)S(1)} %all-to-all-done.1.planes, f32[64,256]{1,0:T(8,128)S(1)} %get-tuple-element.28.before, f32[8,256]{1,0:T(8,128)S(1)} %get-tuple-element.29.logs_before, bf16[512,128]{1,0:T(8,128)(2,1)S(1)} %copy-done.9, ...), custom_call_target="tpu_custom_call" | custom-call | flops 10000000 | bytes 1336340 | tf_op jit(solution)/shard_map/pallas_call | solution.py:224
  139.8 7.9 %all_to_all.21.squares = f32[4,8,512]{2,1,0:T(8,128)S(1)} all-to-all(f32[4,8,512]{2,1,0:T(8,128)S(1)} %broadcast_in_dim.46), channel_id=1, replica_groups=mesh['sp_0'=8,'sp_1'=8,'sp_2'=2,'tp'=4] {'tp'}, dimensions={0} | all-to-all | bytes 131072 | tf_op jit(solution)/shard_map/all_to_all | solution.py:25
  147.6 2.9 %shard_map.194 = bf16[4,512,512]{2,1,0:T(8,128)(2,1)S(1)} custom-call(bf16[512,256]{1,0:T(8,128)(2,1)S(1)} %copy-done.2, bf16[512,256]{1,0:T(8,128)(2,1)S(1)} %get-tuple-element.33.rows, f32[4,8,512]{2,1,0:T(8,128)S(1)} %all_to_all.21.squares, bf16[2048,1152]{1,0:T(8,128)(2,1)} %all-gather.3.cloned.1.call-done.weight.weight_read), custom_call_target="tpu_custom_call" | custom-call | flops 1073741824 | bytes 5308416 | tf_op jit(solution)/shard_map/pallas_call | solution.py:224
  150.6 27.8 %all_to_all.22 = bf16[4,512,512]{2,1,0:T(8,128)(2,1)S(1)} all-to-all(bf16[4,512,512]{2,1,0:T(8,128)(2,1)S(1)} %shard_map.194), channel_id=1, replica_groups=mesh['sp_0'=8,'sp_1'=8,'sp_2'=2,'tp'=4] {'tp'}, dimensions={0} | all-to-all | bytes 4194304 | tf_op jit(solution)/shard_map/all_to_all | solution.py:371
  178.4 1.2 reduce_sum.12
  (50 shorter events, 0.2 us)
Async XLA Ops:
  6.5 115.6 %all-gather.3.cloned.1.call-start = ((), (), s32[]{:S(2)}) async-start(), calls=%async_computation.4 | async-start | bytes 4755456 | tf_op jit(solution)/shard_map/all_gather | solution.py:292
  9.7 43.5 %copy-start.16 = (bf16[512,512]{1,0:T(8,128)(2,1)S(1)}, bf16[512,512]{1,0:T(8,128)(2,1)}, u32[]{:S(2)}) copy-start(bf16[512,512]{1,0:T(8,128)(2,1)} %param.20) | copy-start | bytes 1572868
  9.7 46.8 %copy-start.21 = (bf16[512]{0:T(512)(128)(2,1)S(1)}, bf16[512]{0:T(512)(128)(2,1)}, u32[]{:S(2)}) copy-start(bf16[512]{0:T(512)(128)(2,1)} %param.21) | copy-start | bytes 3076
  9.7 57.3 %copy-start.24 = (f32[4]{0:T(128)S(1)}, f32[4]{0:T(128)}, u32[]{:S(2)}) copy-start(f32[4]{0:T(128)} %param.34) | copy-start | bytes 52
  9.7 57.4 %copy-start.17 = (f32[512,4]{0,1:T(4,128)S(1)}, f32[512,4]{0,1:T(4,128)}, u32[]{:S(2)}) copy-start(f32[512,4]{0,1:T(4,128)} %param.35) | copy-start | bytes 24580
  9.8 58.0 %copy-start.22 = (f32[4]{0:T(128)S(1)}, f32[4]{0:T(128)}, u32[]{:S(2)}) copy-start(f32[4]{0:T(128)} %param.33) | copy-start | bytes 52
  9.8 59.2 %copy-start.18 = (f32[4,256]{1,0:T(4,128)S(1)}, f32[4,256]{1,0:T(4,128)}, u32[]{:S(2)}) copy-start(f32[4,256]{1,0:T(4,128)} %param.30) | copy-start | bytes 12292
  9.8 59.2 %copy-start.20 = (f32[4,64]{1,0:T(4,128)S(1)}, f32[4,64]{1,0:T(4,128)}, u32[]{:S(2)}) copy-start(f32[4,64]{1,0:T(4,128)} %param.31) | copy-start | bytes 3076
  51.3 39.0 %collective-permute-start.4 = (bf16[64,16,384]{2,1,0:T(8,128)(2,1)S(1)}, bf16[64,16,384]{2,1,0:T(8,128)(2,1)S(1)}, u32[]{:S(2)}, u32[]{:S(2)}) collective-permute-start(bf16[64,16,384]{2,1,0:T(8,128)(2,1)S(1)} %all_to_all.20.mine), channel_id=1, source_target_pairs={{0,4},{4,0},{1,5},{5,1},{2,6},{6,2},{3,7},{7,3},{8,12},{12,8},{9,1... | collective-permute-start | bytes 2359304 | tf_op jit(solution)/shard_map/ppermute | solution.py:296
  53.2 3.2 %collective-permute-start = (bf16[16,512]{1,0:T(8,128)(2,1)S(1)}, bf16[16,512]{1,0:T(8,128)(2,1)S(1)}, u32[]{:S(2)}, u32[]{:S(2)}) collective-permute-start(bf16[16,512]{1,0:T(8,128)(2,1)S(1)} %slice.3), channel_id=1, source_target_pairs={{0,4},{4,8},{8,12},{12,16},{16,20},{20,24},{24,28},{28,32},{32,36}... | collective-permute-start | bytes 49160 | tf_op jit(solution)/shard_map/ppermute | solution.py:298
  56.5 17.4 %collective-permute-start.1 = (bf16[544,512]{1,0:T(8,128)(2,1)S(1)}, bf16[544,512]{1,0:T(8,128)(2,1)S(1)}, u32[]{:S(2)}, u32[]{:S(2)}) collective-permute-start(bf16[544,512]{1,0:T(8,128)(2,1)S(1)} %pad_maximum_fusion.x0), channel_id=1, source_target_pairs={{0,1},{1,2},{2,3},{3,0},{4,5},{5,6},{6,7},{7,4},{8,9},{9,10},{10,1... | collective-permute-start | bytes 1671176 | tf_op jit(solution)/shard_map/ppermute | solution.py:302
  59.9 18.9 %collective-permute-start.2 = (bf16[544,512]{1,0:T(8,128)(2,1)S(1)}, bf16[544,512]{1,0:T(8,128)(2,1)S(1)}, u32[]{:S(2)}, u32[]{:S(2)}) collective-permute-start(bf16[544,512]{1,0:T(8,128)(2,1)S(1)} %pad_maximum_fusion.x0), channel_id=1, source_target_pairs={{0,2},{1,3},{2,0},{3,1},{4,6},{5,7},{6,4},{7,5},{8,10},{9,11},{10,... | collective-permute-start | bytes 1671176 | tf_op jit(solution)/shard_map/ppermute | solution.py:302
  62.9 27.4 %collective-permute-start.3 = (bf16[544,512]{1,0:T(8,128)(2,1)S(1)}, bf16[544,512]{1,0:T(8,128)(2,1)}, u32[]{:S(2)}, u32[]{:S(2)}) collective-permute-start(bf16[544,512]{1,0:T(8,128)(2,1)S(1)} %pad_maximum_fusion.x0), channel_id=1, source_target_pairs={{0,3},{1,0},{2,1},{3,2},{4,7},{5,4},{6,5},{7,6},{8,11},{9,8},{10,9... | collective-permute-start | bytes 1671176 | tf_op jit(solution)/shard_map/ppermute | solution.py:302
  90.3 0.7 copy-start.10
  91.0 0.7 copy-start.11
  91.6 0.6 copy-start.12
  97.3 18.7 %copy-start.6 = (bf16[512,128]{1,0:T(8,128)(2,1)}, bf16[512,128]{1,0:T(8,128)(2,1)S(1)}, u32[]{:S(2)}) copy-start(bf16[512,128]{1,0:T(8,128)(2,1)S(1)} %get-tuple-element.22.key) | copy-start | bytes 393220
  97.3 24.6 %copy-start.23 = (f32[4]{0:T(128)S(1)}, f32[4]{0:T(128)}, u32[]{:S(2)}) copy-start(f32[4]{0:T(128)} %param.36) | copy-start | bytes 52
  97.4 24.7 %copy-start.19 = (f32[4,64]{1,0:T(4,128)S(1)}, f32[4,64]{1,0:T(4,128)}, u32[]{:S(2)}) copy-start(f32[4,64]{1,0:T(4,128)} %param.32) | copy-start | bytes 3076
  97.4 24.7 %copy-start = (bf16[4,528,512]{2,1,0:T(8,128)(2,1)S(1)}, bf16[4,528,512]{2,1,0:T(8,128)(2,1)}, u32[]{:S(2)}) copy-start(bf16[4,528,512]{2,1,0:T(8,128)(2,1)} %get-tuple-element.20.normed) | copy-start | bytes 6488068
  97.4 24.7 %copy-start.5 = (bf16[1,256,256]{2,1,0:T(8,128)(2,1)S(1)}, bf16[1,256,256]{2,1,0:T(8,128)(2,1)}, u32[]{:S(2)}) copy-start(bf16[1,256,256]{2,1,0:T(8,128)(2,1)} %param.28) | copy-start | bytes 393220
  97.4 24.7 %copy-start.13 = (s32[5]{0:T(128)S(1)}, s32[5]{0:T(128)}, u32[]{:S(2)}) copy-start(s32[5]{0:T(128)} %stack.23.at) | copy-start | bytes 64
  97.4 24.7 %copy-start.14 = (f32[256]{0:T(256)S(1)}, f32[256]{0:T(256)}, u32[]{:S(2)}) copy-start(f32[256]{0:T(256)} %param.29) | copy-start | bytes 3076
  116.8 18.9 %all-to-all-start.1 = ((bf16[8,80,256]{2,1,0:T(8,128)(2,1)}), bf16[8,80,256]{2,1,0:T(8,128)(2,1)S(1)}, u32[]{:S(2)}, u32[]{:S(2)}) async-start(bf16[8,80,256]{2,1,0:T(8,128)(2,1)} %broadcast_in_dim.44), calls=%async_computation.1 | async-start | bytes 655360 | tf_op jit(solution)/shard_map/all_to_all | solution.py:25
  122.1 0.9 copy-start.7
  123.0 12.7 %copy-start.15 = (f32[256]{0:T(256)S(1)}, f32[256]{0:T(256)}, u32[]{:S(2)}) copy-start(f32[256]{0:T(256)} %param.37) | copy-start | bytes 3076
  129.4 0.7 copy-start.1
  130.1 0.7 copy-start.3
  130.8 0.7 copy-start.8
  135.7 11.9 %copy-start.2 = (bf16[512,256]{1,0:T(8,128)(2,1)S(1)}, bf16[512,256]{1,0:T(8,128)(2,1)}, u32[]{:S(2)}) copy-start(bf16[512,256]{1,0:T(8,128)(2,1)} %copy-done.1) | copy-start | bytes 786436
  135.7 1.0 copy-start.4
  136.7 0.9 copy-start.9
Sparse Core Ops, SparseCore 0:
  10.5 95.6 all-gather.2

commit v3 on v2

--- a/solution.py
+++ b/solution.py
@@ -5,6 +5,7 @@
 from jax.experimental.pallas import tpu as pltpu
 from jax.sharding import Mesh
 from jax.sharding import PartitionSpec as P
+
 
 D = 2048
 POOL_GROUPS = 4
@@ -80,29 +81,40 @@
     return total, logs, before, logs_before
 
 
+def squares_of(pieces, total_rows):
+    squares = jnp.zeros((total_rows, 1), F32)
+    for piece in pieces:
+        values = piece[:total_rows].astype(F32)
+        squares = squares + jnp.sum(values * values, axis=1, keepdims=True)
+    return squares
+
+
+def early_kernel(x0, x3, out):
+    out[...] = squares_of((x0, x3), out.shape[0])
+
+
+def norm_kernel(early, x0, x1, x2, x3, normed):
+    total_rows = normed.shape[1]
+    scale = lax.rsqrt((early[...] + squares_of((x1, x2), total_rows)) / D + EPSILON)
+    for k, piece in enumerate((x0, x1, x2, x3)):
+        gain = piece[total_rows : total_rows + 1].astype(F32)
+        normed[k] = (piece[:total_rows].astype(F32) * scale * gain).astype(BF16)
+
+
 def first_kernel(
-    at, x0, x1, x2, x3, mine, other, taps, bias, rate, extra,
-    normed, value_out, key_out, cum_out, step_out, payload, weight,
+    at, normed, mine, other, taps, bias, rate, extra,
+    value_out, key_out, cum_out, step_out, payload, weight,
 ):
     core = at[1]
     weight[:, pl.ds(core, 1)] = mine[...][:, None]
     weight[:, pl.ds(1 - core, 1)] = other[...][:, None]
-    pieces = (x0, x1, x2, x3)
-    total_rows = x0.shape[0] - PAY
+    total_rows = normed.shape[1]
     length = total_rows - HALO
-    squares = jnp.zeros((total_rows, 1), F32)
-    for piece in pieces:
-        values = piece[:total_rows].astype(F32)
-        squares = squares + jnp.sum(values * values, axis=1, keepdims=True)
-    scale = lax.rsqrt(squares / D + EPSILON)
     chips, columns = weight.shape[0] // 4, weight.shape[3]
     acc = jnp.zeros((total_rows, columns), F32)
-    for k, piece in enumerate(pieces):
-        gain = piece[total_rows : total_rows + 1].astype(F32)
-        part = (piece[:total_rows].astype(F32) * scale * gain).astype(BF16)
-        normed[k] = part
+    for k in range(normed.shape[0]):
         block = weight[pl.ds(((at[0] - k) & 3) * chips, chips)]
-        acc = acc + dot(part, block.reshape(-1, columns))
+        acc = acc + dot(normed[k], block.reshape(-1, columns))
     mix = value_out.shape[1]
     done = convolved(acc.astype(BF16).astype(F32), taps[...], length)
     value_out[...] = done[:, :mix]
@@ -298,22 +310,23 @@
     before = lax.ppermute(activations[length - HALO :], SP, [(k, k + 1) for k in range(size - 1)])
     gains = jnp.broadcast_to(norm_gain[None, :], (PAY, width))
     sent = jnp.concatenate([before, activations, gains], axis=0)
-    pieces = [sent] + [
-        lax.ppermute(sent, "tp", [(k, (k + shift) % count) for k in range(count)])
-        for shift in range(1, count)
-    ]
+    pieces = [sent]
+    for shift in range(1, count):
+        pairs = [(k, (k + shift) % count) for k in range(count)]
+        pieces.append(lax.ppermute(sent, "tp", pairs))
+    rows = HALO + length
+    early = call(early_kernel, (pieces[0], pieces[-1]), (shape_of((rows, 1), F32),), 10**6)[0]
+    normed = call(norm_kernel, (early, *pieces), (shape_of((count, rows, width), BF16),), 10**6)[0]
     taps = jnp.pad(
         jnp.concatenate([taps_value, taps_key], axis=1), ((0, 0), (0, BLOCK - state))
     )
     extra = jnp.pad(jnp.transpose(decay_extra), ((0, 8 - heads), (0, 0)))
-    rows = HALO + length
     columns = mix + BLOCK
     pay = shape_of((HEAD + PAY, mix), BF16)
-    normed, value, key, cum, step, payload = call(
+    value, key, cum, step, payload = call(
         first_kernel,
-        (at, *pieces, mine, other, taps, columns_of(step_bias), columns_of(-jnp.exp(decay_log)), extra),
+        (at, normed, mine, other, taps, columns_of(step_bias), columns_of(-jnp.exp(decay_log)), extra),
         (
-            shape_of((count, rows, width), BF16),
             shape_of((length, mix), BF16),
             shape_of((length, BLOCK), BF16),
             shape_of((8, length), F32),

time: 187 us -> 196 us (1.048)
  the two profiles are of different devices: /device:TPU:2 before, /device:TPU:64 now
where the time goes in v3:
time: 196 us; the launch traced here: 194 us
  blocking collectives  96 us (49%)
  waiting for transfers between devices  24.8 us (13%)
  local copies, waits for them, and re-layouts  21.4 us (11%)
  starting transfers between devices  18.5 us (9%)
  Pallas kernels  17.9 us (9%)
  between operations  13.7 us (7%)
  other arithmetic  2.08 us (1%)
    all_to_all x2, blocking collectives, sent_to_all(): return lax.all_to_all(copies, axis, split_axis=0, concat_axis=0, tiled=True)  47.3 us
    all_to_all x1, blocking collectives, local(): lax.all_to_all(terms, 'tp', split_axis=0, concat_axis=0, tiled=True)  28.4 us
    all_gather x1, blocking collectives, local(): row_pieces = lax.all_gather(payload, ('sp_1', 'sp_2'))  20.3 us
    ppermute x3, waiting for transfers between devices, local(): pieces.append(lax.ppermute(sent, 'tp', pairs))  20 us
    pallas_call x7, Pallas kernels, call(): pl.pallas_call(kernel, grid=(1,), in_specs=[specs.get(k, whole(a.shape))...  17.9 us
    unnamed x75, local copies, waits for them, and re-layouts  17.5 us
    ppermute x3, starting transfers between devices, local(): pieces.append(lax.ppermute(sent, 'tp', pairs))  10.8 us
    ppermute x1, waiting for transfers between devices, local(): lax.ppermute(activations[length - HALO:], SP, [(k, k + 1) for k in range(...  4.75 us
  transfers between devices with their start and end apart: 7, of which 3 were waited for; matrix products, arithmetic and copies ran while one was open for 2% of the time, Pallas kernels for 7%

profile of v3, /device:TPU:64, one launch (start us, length us, event | category | flops | bytes accessed | tf_op | source)
XLA Modules:
  0.0 194.5 jit_solution(7644856082981797838)
XLA Ops:
  6.5 1.4 concatenate.13
  8.0 0.8 copy.21
  8.9 0.8 maximum_maximum_fusion
  9.8 39.3 %all_to_all.20.mine = bf16[64,16,384]{2,1,0:T(8,128)(2,1)S(1)} all-to-all(bf16[64,16,384]{2,1,0:T(8,128)(2,1)S(1)} %broadcast_in_dim.39), channel_id=1, replica_groups=mesh['sp_0'=8,'sp_1'=8,'sp_2'=2,'tp'=4] {'sp_0','sp_1'}, dimensions={0} | all-to-all | bytes 1572864 | tf_op jit(solution)/shard_map/all_to_all | solution.py:26
  49.1 1.9 collective-permute-start.4
  51.0 2.4 %collective-permute-start = (bf16[16,512]{1,0:T(8,128)(2,1)S(1)}, bf16[16,512]{1,0:T(8,128)(2,1)S(1)}, u32[]{:S(2)}, u32[]{:S(2)}) collective-permute-start(bf16[16,512]{1,0:T(8,128)(2,1)S(1)} %slice.3), channel_id=1, source_target_pairs={{0,4},{4,8},{8,12},{12,16},{16,20},{20,24},{24,28},{28,32},{32,36}... | collective-permute-start | bytes 49160 | tf_op jit(solution)/shard_map/ppermute | solution.py:310
  53.4 4.8 %collective-permute-done = bf16[16,512]{1,0:T(8,128)(2,1)S(1)} collective-permute-done((bf16[16,512]{1,0:T(8,128)(2,1)S(1)}, bf16[16,512]{1,0:T(8,128)(2,1)S(1)}, u32[]{:S(2)}, u32[]{:S(2)}) %collective-permute-start) | collective-permute-done | bytes 16416 | tf_op jit(solution)/shard_map/ppermute | solution.py:310
  58.2 4.7 %collective-permute-start.1 = (bf16[544,512]{1,0:T(8,128)(2,1)S(1)}, bf16[544,512]{1,0:T(8,128)(2,1)S(1)}, u32[]{:S(2)}, u32[]{:S(2)}) collective-permute-start(bf16[544,512]{1,0:T(8,128)(2,1)S(1)} %pad_maximum_fusion.x0), channel_id=1, source_target_pairs={{0,3},{1,0},{2,1},{3,2},{4,7},{5,4},{6,5},{7,6},{8,11},{9,8},{10,9... | collective-permute-start | bytes 1671176 | tf_op jit(solution)/shard_map/ppermute | solution.py:316
  62.9 1.9 collective-permute-start.2
  64.8 4.2 %collective-permute-start.3 = (bf16[544,512]{1,0:T(8,128)(2,1)S(1)}, bf16[544,512]{1,0:T(8,128)(2,1)S(1)}, u32[]{:S(2)}, u32[]{:S(2)}) collective-permute-start(bf16[544,512]{1,0:T(8,128)(2,1)S(1)} %pad_maximum_fusion.x0), channel_id=1, source_target_pairs={{0,2},{1,3},{2,0},{3,1},{4,6},{5,7},{6,4},{7,5},{8,10},{9,11},{10,... | collective-permute-start | bytes 1671176 | tf_op jit(solution)/shard_map/ppermute | solution.py:316
  69.4 15.0 %collective-permute-done.1.x3 = bf16[544,512]{1,0:T(8,128)(2,1)S(1)} collective-permute-done((bf16[544,512]{1,0:T(8,128)(2,1)S(1)}, bf16[544,512]{1,0:T(8,128)(2,1)S(1)}, u32[]{:S(2)}, u32[]{:S(2)}) %collective-permute-start.1) | collective-permute-done | bytes 557088 | tf_op jit(solution)/shard_map/ppermute | solution.py:316
  84.3 0.3 shard_map.190.early
  84.6 5.0 %collective-permute-done.2.x1 = bf16[544,512]{1,0:T(8,128)(2,1)S(1)} collective-permute-done((bf16[544,512]{1,0:T(8,128)(2,1)S(1)}, bf16[544,512]{1,0:T(8,128)(2,1)S(1)}, u32[]{:S(2)}, u32[]{:S(2)}) %collective-permute-start.2) | collective-permute-done | bytes 557088 | tf_op jit(solution)/shard_map/ppermute | solution.py:316
  89.6 0.8 copy-done.2
  90.4 0.8 copy-done.4
  91.3 1.1 copy-done.1
  92.4 1.1 copy-done.3
  93.5 1.1 copy-done.5
  94.5 0.8 shard_map.191.normed
  95.3 4.7 %shard_map.192 = (bf16[512,256]{1,0:T(8,128)(2,1)S(1)}, bf16[512,128]{1,0:T(8,128)(2,1)S(1)}, f32[8,512]{1,0:T(8,128)S(1)}, f32[8,512]{1,0:T(8,128)S(1)}, bf16[80,256]{1,0:T(8,128)(2,1)S(1)}) custom-call(s32[5]{0:T(128)S(1)} %stack.23.at, bf16[4,528,512]{2,1,0:T(8,128)(2,1)S(1)} %shard_map.191.normed, bf16[64,16,384]{2,1,0:T(8,128)(2,1)S(1)} %all_to_all.20.mine, ...), custom_call_target="tpu_custom_call" | custom-call | flops 830472192 | bytes 3758164 | tf_op jit(solution)/shard_map/pallas_call | solution.py:236
  100.1 20.3 %all-gather = bf16[1280,256]{1,0:T(8,128)(2,1)S(1)} all-gather(bf16[80,256]{1,0:T(8,128)(2,1)S(1)} %get-tuple-element.24), channel_id=2, replica_groups=mesh['sp_0'=8,'sp_1'=8,'sp_2'=2,'tp'=4] {'sp_1','sp_2'}, dimensions={0}, use_global_device_ids=true | all-gather | bytes 696320 | tf_op jit(solution)/shard_map/all_gather | solution.py:340
  120.4 0.8 shard_map.194
  121.2 0.6 copy-done.15
  121.8 0.7 broadcast_in_dim.44
  122.6 3.4 %all-to-all-start.1 = ((bf16[8,80,256]{2,1,0:T(8,128)(2,1)}), bf16[8,80,256]{2,1,0:T(8,128)(2,1)S(1)}, u32[]{:S(2)}, u32[]{:S(2)}) async-start(bf16[8,80,256]{2,1,0:T(8,128)(2,1)} %broadcast_in_dim.44), calls=%async_computation.1 | async-start | bytes 655360 | tf_op jit(solution)/shard_map/all_to_all | solution.py:26
  126.1 0.6 broadcast_in_dim_reshape.3.skip
  126.7 0.6 pad.23.taps
  127.3 0.9 copy-done.10
  128.2 0.9 copy-done.12
  129.1 0.7 copy-done.18
  129.8 0.6 copy-done.20
  130.5 0.7 copy-done.24
  131.1 0.6 copy-done.25
  131.8 0.7 copy-done.26
  132.4 6.4 %shard_map.193 = (bf16[512,256]{1,0:T(8,128)(2,1)S(1)}, bf16[512,256]{1,0:T(8,128)(2,1)S(1)}, bf16[512,128]{1,0:T(8,128)(2,1)S(1)}, f32[512,256]{1,0:T(8,128)S(1)}) custom-call(s32[5]{0:T(128)S(1)} %copy-done.20, bf16[4,528,512]{2,1,0:T(8,128)(2,1)S(1)} %shard_map.191.normed, bf16[2048,1152]{1,0:T(8,128)(2,1)} %all-gather.3.cloned.1.call-done.weight.weight_read, ...), custom_call_target="tpu_custom_call" | custom-call | flops 1384120320 | bytes 12161044 | tf_op jit(solution)/shard_map/pallas_call | solution.py:236
  138.8 0.7 copy-done.8
  139.5 0.7 copy-done.13
  140.2 0.9 copy-done.9
  141.1 0.9 copy-done.14
  142.1 0.8 copy-done.16
  142.9 0.6 copy-done.21
  143.5 0.7 copy-done.23
  144.2 0.7 copy-done.27
  144.9 2.1 %shard_map.195 = (bf16[512,256]{1,0:T(8,128)(2,1)S(1)}, f32[8,512]{1,0:T(8,128)S(1)}) custom-call(s32[5]{0:T(128)S(1)} %copy-done.21, bf16[8,80,256]{2,1,0:T(8,128)(2,1)S(1)} %all-to-all-done.1.planes, f32[64,256]{1,0:T(8,128)S(1)} %copy-done.16, f32[8,256]{1,0:T(8,128)S(1)} %copy-done.23, bf16[512,128]{1,0:T(8,128)(2,1)S(1)} %copy-done.14, ...), custom_call_target="tpu_custom_call" | custom-call | flops 10000000 | bytes 1336340 | tf_op jit(solution)/shard_map/pallas_call | solution.py:236
  147.0 8.0 %all_to_all.21.squares = f32[4,8,512]{2,1,0:T(8,128)S(1)} all-to-all(f32[4,8,512]{2,1,0:T(8,128)S(1)} %broadcast_in_dim.46), channel_id=1, replica_groups=mesh['sp_0'=8,'sp_1'=8,'sp_2'=2,'tp'=4] {'tp'}, dimensions={0} | all-to-all | bytes 131072 | tf_op jit(solution)/shard_map/all_to_all | solution.py:26
  155.1 2.9 %shard_map.196 = bf16[4,512,512]{2,1,0:T(8,128)(2,1)S(1)} custom-call(bf16[512,256]{1,0:T(8,128)(2,1)S(1)} %get-tuple-element.23.pool, bf16[512,256]{1,0:T(8,128)(2,1)S(1)} %get-tuple-element.31.rows, f32[4,8,512]{2,1,0:T(8,128)S(1)} %all_to_all.21.squares, bf16[2048,1152]{1,0:T(8,128)(2,1)} %all-gather.3.cloned.1.call-done.weight.weight_read), custom_call_target="tpu_custom_call" | custom-call | flops 1073741824 | bytes 5308416 | tf_op jit(solution)/shard_map/pallas_call | solution.py:236
  158.0 28.4 %all_to_all.22 = bf16[4,512,512]{2,1,0:T(8,128)(2,1)S(1)} all-to-all(bf16[4,512,512]{2,1,0:T(8,128)(2,1)S(1)} %shard_map.196), channel_id=1, replica_groups=mesh['sp_0'=8,'sp_1'=8,'sp_2'=2,'tp'=4] {'tp'}, dimensions={0} | all-to-all | bytes 4194304 | tf_op jit(solution)/shard_map/all_to_all | solution.py:384
  186.4 1.2 reduce_sum.12
  (76 shorter events, 0.7 us)
Async XLA Ops:
  6.5 120.8 %all-gather.3.cloned.1.call-start = ((), (), s32[]{:S(2)}) async-start(), calls=%async_computation.4 | async-start | bytes 4755456 | tf_op jit(solution)/shard_map/all_gather | solution.py:304
  9.7 41.3 %copy-start.28 = (bf16[512,512]{1,0:T(8,128)(2,1)S(1)}, bf16[512,512]{1,0:T(8,128)(2,1)}, u32[]{:S(2)}) copy-start(bf16[512,512]{1,0:T(8,128)(2,1)} %param.20) | copy-start | bytes 1572868
  9.7 48.5 %copy-start.33 = (bf16[512]{0:T(512)(128)(2,1)S(1)}, bf16[512]{0:T(512)(128)(2,1)}, u32[]{:S(2)}) copy-start(bf16[512]{0:T(512)(128)(2,1)} %param.21) | copy-start | bytes 3076
  9.7 59.3 %copy-start.36 = (f32[4]{0:T(128)S(1)}, f32[4]{0:T(128)}, u32[]{:S(2)}) copy-start(f32[4]{0:T(128)} %param.34) | copy-start | bytes 52
  9.7 59.4 %copy-start.29 = (f32[512,4]{0,1:T(4,128)S(1)}, f32[512,4]{0,1:T(4,128)}, u32[]{:S(2)}) copy-start(f32[512,4]{0,1:T(4,128)} %param.35) | copy-start | bytes 24580
  9.8 59.4 %copy-start.34 = (f32[4]{0:T(128)S(1)}, f32[4]{0:T(128)}, u32[]{:S(2)}) copy-start(f32[4]{0:T(128)} %param.33) | copy-start | bytes 52
  9.8 59.6 %copy-start.30 = (f32[4,256]{1,0:T(4,128)S(1)}, f32[4,256]{1,0:T(4,128)}, u32[]{:S(2)}) copy-start(f32[4,256]{1,0:T(4,128)} %param.30) | copy-start | bytes 12292
  9.8 59.6 %copy-start.32 = (f32[4,64]{1,0:T(4,128)S(1)}, f32[4,64]{1,0:T(4,128)}, u32[]{:S(2)}) copy-start(f32[4,64]{1,0:T(4,128)} %param.31) | copy-start | bytes 3076
  49.1 46.2 %collective-permute-start.4 = (bf16[64,16,384]{2,1,0:T(8,128)(2,1)S(1)}, bf16[64,16,384]{2,1,0:T(8,128)(2,1)}, u32[]{:S(2)}, u32[]{:S(2)}) collective-permute-start(bf16[64,16,384]{2,1,0:T(8,128)(2,1)S(1)} %all_to_all.20.mine), channel_id=1, source_target_pairs={{0,4},{4,0},{1,5},{5,1},{2,6},{6,2},{3,7},{7,3},{8,12},{12,8},{9,1... | collective-permute-start | bytes 2359304 | tf_op jit(solution)/shard_map/ppermute | solution.py:308
  51.0 7.2 %collective-permute-start = (bf16[16,512]{1,0:T(8,128)(2,1)S(1)}, bf16[16,512]{1,0:T(8,128)(2,1)S(1)}, u32[]{:S(2)}, u32[]{:S(2)}) collective-permute-start(bf16[16,512]{1,0:T(8,128)(2,1)S(1)} %slice.3), channel_id=1, source_target_pairs={{0,4},{4,8},{8,12},{12,16},{16,20},{20,24},{24,28},{28,32},{32,36}... | collective-permute-start | bytes 49160 | tf_op jit(solution)/shard_map/ppermute | solution.py:310
  58.2 26.1 %collective-permute-start.1 = (bf16[544,512]{1,0:T(8,128)(2,1)S(1)}, bf16[544,512]{1,0:T(8,128)(2,1)S(1)}, u32[]{:S(2)}, u32[]{:S(2)}) collective-permute-start(bf16[544,512]{1,0:T(8,128)(2,1)S(1)} %pad_maximum_fusion.x0), channel_id=1, source_target_pairs={{0,3},{1,0},{2,1},{3,2},{4,7},{5,4},{6,5},{7,6},{8,11},{9,8},{10,9... | collective-permute-start | bytes 1671176 | tf_op jit(solution)/shard_map/ppermute | solution.py:316
  62.9 26.7 %collective-permute-start.2 = (bf16[544,512]{1,0:T(8,128)(2,1)S(1)}, bf16[544,512]{1,0:T(8,128)(2,1)S(1)}, u32[]{:S(2)}, u32[]{:S(2)}) collective-permute-start(bf16[544,512]{1,0:T(8,128)(2,1)S(1)} %pad_maximum_fusion.x0), channel_id=1, source_target_pairs={{0,1},{1,2},{2,3},{3,0},{4,5},{5,6},{6,7},{7,4},{8,9},{9,10},{10,1... | collective-permute-start | bytes 1671176 | tf_op jit(solution)/shard_map/ppermute | solution.py:316
  64.8 25.6 %collective-permute-start.3 = (bf16[544,512]{1,0:T(8,128)(2,1)S(1)}, bf16[544,512]{1,0:T(8,128)(2,1)S(1)}, u32[]{:S(2)}, u32[]{:S(2)}) collective-permute-start(bf16[544,512]{1,0:T(8,128)(2,1)S(1)} %pad_maximum_fusion.x0), channel_id=1, source_target_pairs={{0,2},{1,3},{2,0},{3,1},{4,6},{5,7},{6,4},{7,5},{8,10},{9,11},{10,... | collective-permute-start | bytes 1671176 | tf_op jit(solution)/shard_map/ppermute | solution.py:316
  69.4 51.1 %copy-start.19 = (s32[5]{0:T(128)}, s32[5]{0:T(128)S(1)}, u32[]{:S(2)}) copy-start(s32[5]{0:T(128)S(1)} %stack.23.at) | copy-start | bytes 64
  84.3 5.3 %copy-start = (bf16[544,512]{1,0:T(8,128)(2,1)}, bf16[544,512]{1,0:T(8,128)(2,1)S(1)}, u32[]{:S(2)}) copy-start(bf16[544,512]{1,0:T(8,128)(2,1)S(1)} %collective-permute-done.1.x3) | copy-start | bytes 1671172
  89.6 0.8 copy-start.2
  90.4 0.8 copy-start.4
  91.3 1.1 copy-start.1
  92.4 1.1 copy-start.3
  93.5 1.1 copy-start.5
  100.0 21.2 %copy-start.6 = (bf16[512,256]{1,0:T(8,128)(2,1)}, bf16[512,256]{1,0:T(8,128)(2,1)S(1)}, u32[]{:S(2)}) copy-start(bf16[512,256]{1,0:T(8,128)(2,1)S(1)} %get-tuple-element.19.value) | copy-start | bytes 786436
  100.0 21.8 %copy-start.11 = (bf16[512,128]{1,0:T(8,128)(2,1)}, bf16[512,128]{1,0:T(8,128)(2,1)S(1)}, u32[]{:S(2)}) copy-start(bf16[512,128]{1,0:T(8,128)(2,1)S(1)} %get-tuple-element.20.key) | copy-start | bytes 393220
  100.0 21.8 %copy-start.17 = (f32[8,512]{1,0:T(8,128)}, f32[8,512]{1,0:T(8,128)S(1)}, u32[]{:S(2)}) copy-start(f32[8,512]{1,0:T(8,128)S(1)} %get-tuple-element.22.step) | copy-start | bytes 49156
  100.1 26.0 %copy-start.35 = (f32[4]{0:T(128)S(1)}, f32[4]{0:T(128)}, u32[]{:S(2)}) copy-start(f32[4]{0:T(128)} %param.36) | copy-start | bytes 52
  100.1 26.6 %copy-start.31 = (f32[4,64]{1,0:T(4,128)S(1)}, f32[4,64]{1,0:T(4,128)}, u32[]{:S(2)}) copy-start(f32[4,64]{1,0:T(4,128)} %param.32) | copy-start | bytes 3076
  121.2 0.6 copy-start.15
  121.8 5.5 %copy-start.22 = (f32[8,256]{1,0:T(8,128)}, f32[8,256]{1,0:T(8,128)S(1)}, u32[]{:S(2)}) copy-start(f32[8,256]{1,0:T(8,128)S(1)} %get-tuple-element.27.logs_before) | copy-start | bytes 24580
  121.8 5.5 %copy-start.7 = (bf16[512,256]{1,0:T(8,128)(2,1)S(1)}, bf16[512,256]{1,0:T(8,128)(2,1)}, u32[]{:S(2)}) copy-start(bf16[512,256]{1,0:T(8,128)(2,1)} %copy-done.6) | copy-start | bytes 786436
  122.6 17.6 %all-to-all-start.1 = ((bf16[8,80,256]{2,1,0:T(8,128)(2,1)}), bf16[8,80,256]{2,1,0:T(8,128)(2,1)S(1)}, u32[]{:S(2)}, u32[]{:S(2)}) async-start(bf16[8,80,256]{2,1,0:T(8,128)(2,1)} %broadcast_in_dim.44), calls=%async_computation.1 | async-start | bytes 655360 | tf_op jit(solution)/shard_map/all_to_all | solution.py:26
  127.3 0.9 copy-start.10
  128.2 0.9 copy-start.12
  129.1 0.7 copy-start.18
  129.8 0.6 copy-start.20
  130.5 0.7 copy-start.24
  131.1 0.6 copy-start.25
  131.8 0.7 copy-start.26
  138.8 0.7 copy-start.8
  139.5 0.7 copy-start.13
  140.2 1.0 copy-start.9
  141.1 0.9 copy-start.14
  142.1 0.8 copy-start.16
  142.9 0.6 copy-start.21
  143.5 0.7 copy-start.23
  144.2 0.7 copy-start.27
Sparse Core Ops, SparseCore 0:
  10.5 93.9 all-gather.2

commit v4 on v3

--- a/solution.py
+++ b/solution.py
@@ -102,10 +102,11 @@
 
 
 def first_kernel(
-    at, normed, mine, other, taps, bias, rate, extra,
+    normed, mine, other, params, extra,
     value_out, key_out, cum_out, step_out, payload, weight,
 ):
-    core = at[1]
+    core = lax.axis_index("sp_2")
+    place = lax.axis_index("tp")
     weight[:, pl.ds(core, 1)] = mine[...][:, None]
     weight[:, pl.ds(1 - core, 1)] = other[...][:, None]
     total_rows = normed.shape[1]
@@ -113,15 +114,15 @@
     chips, columns = weight.shape[0] // 4, weight.shape[3]
     acc = jnp.zeros((total_rows, columns), F32)
     for k in range(normed.shape[0]):
-        block = weight[pl.ds(((at[0] - k) & 3) * chips, chips)]
+        block = weight[pl.ds(((place - k) & 3) * chips, chips)]
         acc = acc + dot(normed[k], block.reshape(-1, columns))
     mix = value_out.shape[1]
-    done = convolved(acc.astype(BF16).astype(F32), taps[...], length)
+    done = convolved(acc.astype(BF16).astype(F32), params[:4], length)
     value_out[...] = done[:, :mix]
     key_out[...] = done[:, mix:]
-    raw = jnp.transpose(acc[HALO:, mix:])[HEAD : HEAD + 8] + bias[...]
+    raw = jnp.transpose(acc[HALO:, mix:])[HEAD : HEAD + 8] + params[8:16, :1]
     step = jnp.maximum(raw, 0.0) + jnp.log1p(jnp.exp(-jnp.abs(raw)))
-    decay = rate[...] * step + extra[...]
+    decay = params[16:24, :1] * step + extra[...]
     rows = lax.broadcasted_iota(jnp.int32, (BLOCK, BLOCK), 0)
     upper = (rows <= lax.broadcasted_iota(jnp.int32, (BLOCK, BLOCK), 1)).astype(F32)
     carry, cums = jnp.zeros((8, 1), F32), []
@@ -137,24 +138,25 @@
     write_payload(payload, state[:HEAD], jnp.sum(carry * lanes, axis=0, keepdims=True))
 
 
-def row_kernel(at, rows, before_out, logs_out, payload):
-    total, logs, before, logs_before = scan_payloads(rows, at[2])
+def row_kernel(rows, before_out, logs_out, payload):
+    total, logs, before, logs_before = scan_payloads(rows, lax.axis_index(("sp_1", "sp_2")))
     before_out[...] = before
     logs_out[...] = jnp.broadcast_to(logs_before, logs_out.shape)
     write_payload(payload, total, logs)
 
 
 def second_kernel(
-    at, normed, weight, weight_read, value, key, cum, step, taps, mix_weight, pool_scale, skip,
+    normed, weight, weight_read, value, key, cum, step, params, mix_weight,
     pool_out, gate_out, read_out, local_out,
 ):
     length, span = pool_out.shape
+    place = lax.axis_index("tp")
     total_rows = normed.shape[1]
     acc = jnp.zeros((total_rows, weight.shape[1]), F32)
     acc_read = jnp.zeros((total_rows, weight_read.shape[1]), F32)
     width = normed.shape[2]
     for k in range(normed.shape[0]):
-        start = pl.multiple_of(((at[0] - k) & 3) * width, width)
+        start = pl.multiple_of(((place - k) & 3) * width, width)
         acc = acc + dot(normed[k], weight[pl.ds(start, width)])
         acc_read = acc_read + dot(normed[k], weight_read[pl.ds(start, width)])
     gate_out[...] = acc[HALO:, span:].astype(BF16)
@@ -164,12 +166,12 @@
     for level in range(POOL_GROUPS):
         stride = 2**level
         running = running[stride:] + running[:-stride]
-        chosen = jnp.where(at[0] == level, running[running.shape[0] - length :], chosen)
-    position = at[4] * length + lax.broadcasted_iota(jnp.int32, (length, 1), 0) + 1
-    counts = jnp.minimum(position, 2 << at[0]).astype(F32)
+        chosen = jnp.where(place == level, running[running.shape[0] - length :], chosen)
+    position = lax.axis_index(SP) * length + lax.broadcasted_iota(jnp.int32, (length, 1), 0) + 1
+    counts = jnp.minimum(position, 2 << place).astype(F32)
     pooled = (chosen / counts - own).astype(BF16)
-    pool_out[...] = (dot(pooled, mix_weight[...]) * pool_scale[...]).astype(BF16)
-    reads = convolved(acc_read.astype(BF16).astype(F32), taps[...], length)
+    pool_out[...] = (dot(pooled, mix_weight[...]) * params[25:26, :span]).astype(BF16)
+    reads = convolved(acc_read.astype(BF16).astype(F32), params[4:8, :BLOCK], length)
     read_out[...] = reads
     lanes = heads_of_lanes(span)
     values = value[...].astype(F32)
@@ -194,13 +196,13 @@
             left = jnp.concatenate(parts, axis=1)
             right = scaled[: (i + 1) * BLOCK, h * HEAD : (h + 1) * HEAD]
             results.append(dot(left, right))
-        local_out[here] = jnp.concatenate(results, axis=1) + skip[...] * values[here]
+        local_out[here] = jnp.concatenate(results, axis=1) + params[24:25, :span] * values[here]
 
 
 def third_kernel(
-    at, planes, before, logs_before, reads, local_in, gate, cum, gain, rows_out, squares_out
+    planes, before, logs_before, reads, local_in, gate, cum, params, rows_out, squares_out
 ):
-    _, _, earlier, _ = scan_payloads(planes, at[3])
+    _, _, earlier, _ = scan_payloads(planes, lax.axis_index("sp_0"))
     incoming = earlier * jnp.exp(logs_before[:1]) + before[...]
     lanes = heads_of_lanes(local_in.shape[1])
     decay = dot(jnp.exp(cum[...]), lanes, 0, 0, HIGH)
@@ -208,7 +210,7 @@
     gated = (local_in[...] + far) * silu(gate[...].astype(F32))
     ones = jnp.ones((8, gated.shape[1]), F32)
     squares_out[...] = dot(ones, gated * gated, 1, 1, HIGH)
-    rows_out[...] = (gated * gain[...]).astype(BF16)
+    rows_out[...] = (gated * params[26:27, : gated.shape[1]]).astype(BF16)
 
 
 def out_kernel(pool, rows, squares, weight, out):
@@ -227,12 +229,16 @@
     return pl.BlockSpec(shape, lambda *_: (0,) * len(shape))
 
 
-SMEM = pl.BlockSpec(memory_space=pltpu.SMEM)
-
-
-def call(kernel, args, outs, flops, scratch=(), specs=None):
+LIMITS = {"early": 8, "norm": 16, "first": 16, "row": 6, "second": 24, "third": 10, "out": 16}
+
+
+def call(kernel, name, args, outs, flops, scratch=(), specs=None, far=()):
     specs = specs or {}
     moved = sum(a.size * a.dtype.itemsize for a in args)
+    args = [
+        pltpu.with_memory_space_constraint(a, pltpu.HBM) if k in far else a
+        for k, a in enumerate(args)
+    ]
     return pl.pallas_call(
         kernel,
         grid=(1,),
@@ -240,17 +246,25 @@
         out_specs=[whole(o.shape) for o in outs],
         out_shape=outs,
         scratch_shapes=list(scratch),
-        compiler_params=pltpu.CompilerParams(vmem_limit_bytes=48 * 1024 * 1024),
+        compiler_params=pltpu.CompilerParams(vmem_limit_bytes=LIMITS[name] * 2**20),
         cost_estimate=pl.CostEstimate(flops=flops, transcendentals=0, bytes_accessed=moved),
     )(*args)
 
 
+def far_of(shape, dtype):
+    return pltpu.HBM(shape, dtype)
+
+
 def shape_of(shape, dtype):
     return jax.ShapeDtypeStruct(shape, dtype)
 
 
-def columns_of(array):
-    return jnp.pad(array[:, None], ((0, 8 - array.shape[0]), (0, 0)))
+def columns_of(array, lanes):
+    return jnp.broadcast_to(jnp.pad(array, (0, 8 - array.shape[0]))[:, None], (8, lanes))
+
+
+def padded(array, lanes):
+    return jnp.pad(array, ((0, 0), (0, lanes - array.shape[1])))
 
 
 def local(
@@ -280,15 +294,6 @@
     state = key_weight.shape[1]
     heads = step_weight.shape[1]
     count = lax.axis_size("tp")
-    at = jnp.stack(
-        [
-            lax.axis_index("tp"),
-            lax.axis_index("sp_2"),
-            lax.axis_index(("sp_1", "sp_2")),
-            lax.axis_index("sp_0"),
-            lax.axis_index(SP),
-        ]
-    ).astype(jnp.int32)
     fill = jnp.zeros((read_weight.shape[0], BLOCK - state), BF16)
     joined = jnp.concatenate(
         [
@@ -315,71 +320,91 @@
         pairs = [(k, (k + shift) % count) for k in range(count)]
         pieces.append(lax.ppermute(sent, "tp", pairs))
     rows = HALO + length
-    early = call(early_kernel, (pieces[0], pieces[-1]), (shape_of((rows, 1), F32),), 10**6)[0]
-    normed = call(norm_kernel, (early, *pieces), (shape_of((count, rows, width), BF16),), 10**6)[0]
-    taps = jnp.pad(
-        jnp.concatenate([taps_value, taps_key], axis=1), ((0, 0), (0, BLOCK - state))
+    early = call(
+        early_kernel, "early", (pieces[0], pieces[-1]), (far_of((rows, 1), F32),), 10**6
+    )[0]
+    normed = call(
+        norm_kernel,
+        "norm",
+        (early, *pieces),
+        (shape_of((count, rows, width), BF16),),
+        10**6,
+        far=range(5),
+    )[0]
+    lanes = mix + BLOCK
+    params = jnp.concatenate(
+        [
+            padded(jnp.concatenate([taps_value, taps_key], axis=1), lanes),
+            padded(taps_read, lanes),
+            columns_of(step_bias, lanes),
+            columns_of(-jnp.exp(decay_log), lanes),
+            padded(jnp.repeat(skip_scale, HEAD)[None, :], lanes),
+            padded(pool_scale[None, :], lanes),
+            padded(state_gain[None, :], lanes),
+            jnp.zeros((5, lanes), F32),
+        ]
     )
     extra = jnp.pad(jnp.transpose(decay_extra), ((0, 8 - heads), (0, 0)))
     columns = mix + BLOCK
     pay = shape_of((HEAD + PAY, mix), BF16)
     value, key, cum, step, payload = call(
         first_kernel,
-        (at, normed, mine, other, taps, columns_of(step_bias), columns_of(-jnp.exp(decay_log)), extra),
+        "first",
+        (normed, mine, other, params, extra),
         (
-            shape_of((length, mix), BF16),
-            shape_of((length, BLOCK), BF16),
-            shape_of((8, length), F32),
-            shape_of((8, length), F32),
+            far_of((length, mix), BF16),
+            far_of((length, BLOCK), BF16),
+            far_of((8, length), F32),
+            far_of((8, length), F32),
             pay,
         ),
         2 * rows * D * columns,
         [pltpu.VMEM((mine.shape[0], 2, mine.shape[1], columns), BF16)],
-        {0: SMEM},
+        far=(3, 4),
     )
     row_pieces = lax.all_gather(payload, ("sp_1", "sp_2"))
     before_row, logs_row, payload = call(
         row_kernel,
-        (at, row_pieces),
-        (shape_of((HEAD, mix), F32), shape_of((8, mix), F32), pay),
+        "row",
+        (row_pieces,),
+        (far_of((HEAD, mix), F32), far_of((8, mix), F32), pay),
         10**6,
-        specs={0: SMEM},
     )
     plane_pieces = sent_to_all(payload, "sp_0")
-    taps_r = jnp.pad(taps_read, ((0, 0), (0, BLOCK - state)))
     pool_out, gate, reads, inside = call(
         second_kernel,
+        "second",
+        (normed, later_weights, later_weights, value, key, cum, step, params, pool_mix[0]),
         (
-            at, normed, later_weights, later_weights, value, key, cum, step, taps_r,
-            pool_mix[0], pool_scale[None, :], jnp.repeat(skip_scale, HEAD)[None, :],
-        ),
-        (
-            shape_of((length, mix), BF16),
-            shape_of((length, mix), BF16),
-            shape_of((length, BLOCK), BF16),
-            shape_of((length, mix), F32),
+            far_of((length, mix), BF16),
+            far_of((length, mix), BF16),
+            far_of((length, BLOCK), BF16),
+            far_of((length, mix), F32),
         ),
         2 * rows * D * (2 * mix + BLOCK),
         specs={
-            0: SMEM,
-            2: pl.BlockSpec((D, 2 * mix), lambda *_: (0, 0)),
-            3: pl.BlockSpec((D, BLOCK), lambda *_: (0, 4 * mix // BLOCK)),
+            1: pl.BlockSpec((D, 2 * mix), lambda *_: (0, 0)),
+            2: pl.BlockSpec((D, BLOCK), lambda *_: (0, 4 * mix // BLOCK)),
         },
+        far=range(9),
     )
     gated, squares = call(
         third_kernel,
-        (at, plane_pieces, before_row, logs_row, reads, inside, gate, cum, state_gain[None, :]),
+        "third",
+        (plane_pieces, before_row, logs_row, reads, inside, gate, cum, params),
         (shape_of((length, mix), BF16), shape_of((8, length), F32)),
         10**7,
-        specs={0: SMEM},
+        far=range(1, 8),
     )
     all_squares = sent_to_all(squares, "tp")
     terms = call(
         out_kernel,
+        "out",
         (pool_out, gated, all_squares, later_weights),
         (shape_of((count, length, width), BF16),),
         2 * length * 2 * mix * D,
         specs={3: pl.BlockSpec((D, 2 * mix), lambda *_: (0, 1))},
+        far=(0, 3),
     )[0]
     arrived = lax.all_to_all(terms, "tp", split_axis=0, concat_axis=0, tiled=True)
     return arrived.astype(F32).sum(axis=0).astype(BF16)

time: 196 us -> 188 us (0.959)
  the two profiles are of different devices: /device:TPU:64 before, /device:TPU:2 now
where the time goes in v4:
time: 188 us; the launch traced here: 187 us
  blocking collectives  99.7 us (53%)
  Pallas kernels  23.5 us (12%)
  starting transfers between devices  20.3 us (11%)
  waiting for transfers between devices  20.3 us (11%)
  between operations  13.7 us (7%)
  local copies, waits for them, and re-layouts  7.37 us (4%)
  other arithmetic  2.08 us (1%)
    all_to_all x2, blocking collectives, sent_to_all(): return lax.all_to_all(copies, axis, split_axis=0, concat_axis=0, tiled=True)  53.1 us
    all_to_all x1, blocking collectives, local(): lax.all_to_all(terms, 'tp', split_axis=0, concat_axis=0, tiled=True)  28.1 us
    pallas_call x7, Pallas kernels, call(): pl.pallas_call(kernel, grid=(1,), in_specs=[specs.get(k, whole(a.shape))...  23.5 us
    all_gather x1, blocking collectives, local(): row_pieces = lax.all_gather(payload, ('sp_1', 'sp_2'))  18.5 us
    ppermute x3, waiting for transfers between devices, local(): pieces.append(lax.ppermute(sent, 'tp', pairs))  13.7 us
    ppermute x3, starting transfers between devices, local(): pieces.append(lax.ppermute(sent, 'tp', pairs))  11.1 us
    all_to_all x1, waiting for transfers between devices, sent_to_all(): return lax.all_to_all(copies, axis, split_axis=0, concat_axis=0, tiled=True)  5.76 us
    all_to_all x1, starting transfers between devices, sent_to_all(): return lax.all_to_all(copies, axis, split_axis=0, concat_axis=0, tiled=True)  4.92 us
  transfers between devices with their start and end apart: 7, of which 5 were waited for; matrix products, arithmetic and copies ran while one was open for 3% of the time, Pallas kernels for 9%

profile of v4, /device:TPU:2, one launch (start us, length us, event | category | flops | bytes accessed | tf_op | source)
XLA Modules:
  0.0 187.0 jit_solution(2236474873725891715)
XLA Ops:
  6.5 1.5 concatenate.16
  8.0 0.0 all-gather.3.cloned.1.call-update
  8.0 0.8 copy.21
  8.8 0.1 pad.42.clone
  8.9 0.8 maximum_maximum_fusion
  9.7 0.1 broadcast_in_dim.48
  9.7 0.0 copy-start.13
  9.8 0.0 copy-start.14
  9.8 0.0 copy-start.7
  9.8 0.0 copy-start.12
  9.8 0.0 copy-start.10
  9.8 0.0 copy-start.11
  9.8 0.0 copy-start.5
  9.8 0.0 copy-start.6
  9.8 0.0 copy-start.8
  9.8 41.5 %all_to_all.20.mine = bf16[64,16,384]{2,1,0:T(8,128)(2,1)S(1)} all-to-all(bf16[64,16,384]{2,1,0:T(8,128)(2,1)S(1)} %broadcast_in_dim.48), channel_id=1, replica_groups=mesh['sp_0'=8,'sp_1'=8,'sp_2'=2,'tp'=4] {'sp_0','sp_1'}, dimensions={0} | all-to-all | bytes 1572864 | tf_op jit(solution)/shard_map/all_to_all | solution.py:26
  51.3 1.9 %collective-permute-start.4 = (bf16[64,16,384]{2,1,0:T(8,128)(2,1)S(1)}, bf16[64,16,384]{2,1,0:T(8,128)(2,1)}, u32[]{:S(2)}, u32[]{:S(2)}) collective-permute-start(bf16[64,16,384]{2,1,0:T(8,128)(2,1)S(1)} %all_to_all.20.mine), channel_id=1, source_target_pairs={{0,4},{4,0},{1,5},{5,1},{2,6},{6,2},{3,7},{7,3},{8,12},{12,8},{9,1... | collective-permute-start | bytes 2359304 | tf_op jit(solution)/shard_map/ppermute | solution.py:313
  53.2 2.4 %collective-permute-start = (bf16[16,512]{1,0:T(8,128)(2,1)S(1)}, bf16[16,512]{1,0:T(8,128)(2,1)S(1)}, u32[]{:S(2)}, u32[]{:S(2)}) collective-permute-start(bf16[16,512]{1,0:T(8,128)(2,1)S(1)} %slice.3), channel_id=1, source_target_pairs={{0,4},{4,8},{8,12},{12,16},{16,20},{20,24},{24,28},{28,32},{32,36}... | collective-permute-start | bytes 49160 | tf_op jit(solution)/shard_map/ppermute | solution.py:315
  55.7 0.8 collective-permute-done
  56.5 2.4 %collective-permute-start.1 = (bf16[544,512]{1,0:T(8,128)(2,1)S(1)}, bf16[544,512]{1,0:T(8,128)(2,1)S(1)}, u32[]{:S(2)}, u32[]{:S(2)}) collective-permute-start(bf16[544,512]{1,0:T(8,128)(2,1)S(1)} %pad_maximum_fusion.x0), channel_id=1, source_target_pairs={{0,3},{1,0},{2,1},{3,2},{4,7},{5,4},{6,5},{7,6},{8,11},{9,8},{10,9... | collective-permute-start | bytes 1671176 | tf_op jit(solution)/shard_map/ppermute | solution.py:321
  59.0 3.4 %collective-permute-start.2 = (bf16[544,512]{1,0:T(8,128)(2,1)S(1)}, bf16[544,512]{1,0:T(8,128)(2,1)S(1)}, u32[]{:S(2)}, u32[]{:S(2)}) collective-permute-start(bf16[544,512]{1,0:T(8,128)(2,1)S(1)} %pad_maximum_fusion.x0), channel_id=1, source_target_pairs={{0,1},{1,2},{2,3},{3,0},{4,5},{5,6},{6,7},{7,4},{8,9},{9,10},{10,1... | collective-permute-start | bytes 1671176 | tf_op jit(solution)/shard_map/ppermute | solution.py:321
  62.4 5.3 %collective-permute-start.3 = (bf16[544,512]{1,0:T(8,128)(2,1)S(1)}, bf16[544,512]{1,0:T(8,128)(2,1)}, u32[]{:S(2)}, u32[]{:S(2)}) collective-permute-start(bf16[544,512]{1,0:T(8,128)(2,1)S(1)} %pad_maximum_fusion.x0), channel_id=1, source_target_pairs={{0,2},{1,3},{2,0},{3,1},{4,6},{5,7},{6,4},{7,5},{8,10},{9,11},{10,... | collective-permute-start | bytes 1671176 | tf_op jit(solution)/shard_map/ppermute | solution.py:321
  67.7 0.1 broadcast_in_dim.51
  67.8 0.1 broadcast_in_dim_reshape.3
  68.0 0.6 pad.36.extra
  68.6 0.1 broadcast_in_dim.50
  68.6 0.1 broadcast_in_dim.49
  68.7 2.4 %concatenate.19.params = f32[32,384]{1,0:T(8,128)} concatenate(f32[4,384]{1,0:T(4,128)S(1)} %select_maximum_fusion, f32[4,384]{1,0:T(4,128)S(1)} %pad.30, f32[8,384]{1,0:T(8,128)S(1)} %broadcast_in_dim.49, f32[8,384]{1,0:T(8,128)S(1)} %broadcast_in_dim.50, f32[1,384]{1,0:T(1,128)S(1)} %pad.33, f32[1,384]{1,0:T(1,128)S(1)} %pad.34, f32[1,384]{1,0:T(1,128)S(1)} %pad.35, ...), dimensions={0} | concatenate | bytes 98304 | tf_op jit(solution)/shard_map/concatenate | solution.py:335
  71.1 2.5 %collective-permute-done.1.x3 = bf16[544,512]{1,0:T(8,128)(2,1)S(1)} collective-permute-done((bf16[544,512]{1,0:T(8,128)(2,1)S(1)}, bf16[544,512]{1,0:T(8,128)(2,1)S(1)}, u32[]{:S(2)}, u32[]{:S(2)}) %collective-permute-start.1) | collective-permute-done | bytes 557088 | tf_op jit(solution)/shard_map/ppermute | solution.py:321
  73.6 1.0 shard_map.190.early
  74.6 2.5 %collective-permute-done.2.x1 = bf16[544,512]{1,0:T(8,128)(2,1)S(1)} collective-permute-done((bf16[544,512]{1,0:T(8,128)(2,1)S(1)}, bf16[544,512]{1,0:T(8,128)(2,1)S(1)}, u32[]{:S(2)}, u32[]{:S(2)}) %collective-permute-start.2) | collective-permute-done | bytes 557088 | tf_op jit(solution)/shard_map/ppermute | solution.py:321
  77.1 0.8 copy-done.4
  77.9 8.7 %collective-permute-done.3.x2 = bf16[544,512]{1,0:T(8,128)(2,1)} collective-permute-done((bf16[544,512]{1,0:T(8,128)(2,1)S(1)}, bf16[544,512]{1,0:T(8,128)(2,1)}, u32[]{:S(2)}, u32[]{:S(2)}) %collective-permute-start.3) | collective-permute-done | bytes 557088 | tf_op jit(solution)/shard_map/ppermute | solution.py:321
  86.6 2.4 %shard_map.191.normed = bf16[4,528,512]{2,1,0:T(8,128)(2,1)S(1)} custom-call(f32[528,1]{1,0:T(8,128)} %shard_map.190.early, bf16[544,512]{1,0:T(8,128)(2,1)} %copy-done.1, bf16[544,512]{1,0:T(8,128)(2,1)} %copy-done.4, bf16[544,512]{1,0:T(8,128)(2,1)} %collective-permute-done.3.x2, bf16[544,512]{1,0:T(8,128)(2,1)} %copy-done.2), custom_call_target="tpu_custom_call" | custom-call | flops 1000000 | bytes 2230336 | tf_op jit(solution)/shard_map/pallas_call | solution.py:242
  89.1 0.0 collective-permute-done.4.other
  89.1 5.4 %shard_map.192 = (bf16[512,256]{1,0:T(8,128)(2,1)}, bf16[512,128]{1,0:T(8,128)(2,1)}, f32[8,512]{1,0:T(8,128)}, f32[8,512]{1,0:T(8,128)}, bf16[80,256]{1,0:T(8,128)(2,1)S(1)}) custom-call(bf16[4,528,512]{2,1,0:T(8,128)(2,1)S(1)} %shard_map.191.normed, bf16[64,16,384]{2,1,0:T(8,128)(2,1)S(1)} %all_to_all.20.mine, ...), custom_call_target="tpu_custom_call" | custom-call | flops 830472192 | bytes 3801088 | tf_op jit(solution)/shard_map/pallas_call | solution.py:242
  94.5 18.5 %all-gather = bf16[1280,256]{1,0:T(8,128)(2,1)S(1)} all-gather(bf16[80,256]{1,0:T(8,128)(2,1)S(1)} %get-tuple-element.24), channel_id=2, replica_groups=mesh['sp_0'=8,'sp_1'=8,'sp_2'=2,'tp'=4] {'sp_1','sp_2'}, dimensions={0}, use_global_device_ids=true | all-gather | bytes 696320 | tf_op jit(solution)/shard_map/all_gather | solution.py:365
  113.0 0.8 shard_map.194
  113.9 0.7 broadcast_in_dim.55
  114.6 4.9 %all-to-all-start.1 = ((bf16[8,80,256]{2,1,0:T(8,128)(2,1)}), bf16[8,80,256]{2,1,0:T(8,128)(2,1)S(1)}, u32[]{:S(2)}, u32[]{:S(2)}) async-start(bf16[8,80,256]{2,1,0:T(8,128)(2,1)} %broadcast_in_dim.55), calls=%async_computation.1 | async-start | bytes 655360 | tf_op jit(solution)/shard_map/all_to_all | solution.py:26
  119.5 0.0 all-gather.3.cloned.1.call-done.weight.weight_read
  119.5 8.0 %shard_map.193 = (bf16[512,256]{1,0:T(8,128)(2,1)}, bf16[512,256]{1,0:T(8,128)(2,1)}, bf16[512,128]{1,0:T(8,128)(2,1)}, f32[512,256]{1,0:T(8,128)}) custom-call(bf16[4,528,512]{2,1,0:T(8,128)(2,1)} %copy-done, bf16[2048,1152]{1,0:T(8,128)(2,1)} %all-gather.3.cloned.1.call-done.weight.weight_read, ...), custom_call_target="tpu_custom_call" | custom-call | flops 1384120320 | bytes 12206080 | tf_op jit(solution)/shard_map/pallas_call | solution.py:242
  127.6 5.8 %all-to-all-done.1.planes = bf16[8,80,256]{2,1,0:T(8,128)(2,1)S(1)} async-done(((bf16[8,80,256]{2,1,0:T(8,128)(2,1)}), bf16[8,80,256]{2,1,0:T(8,128)(2,1)S(1)}, u32[]{:S(2)}, u32[]{:S(2)}) %all-to-all-start.1) | async-done | bytes 327712 | tf_op jit(solution)/shard_map/all_to_all | solution.py:26
  133.3 2.8 %shard_map.195 = (bf16[512,256]{1,0:T(8,128)(2,1)S(1)}, f32[8,512]{1,0:T(8,128)S(1)}) custom-call(bf16[8,80,256]{2,1,0:T(8,128)(2,1)S(1)} %all-to-all-done.1.planes, f32[64,256]{1,0:T(8,128)} %get-tuple-element.26.before, f32[8,256]{1,0:T(8,128)} %get-tuple-element.27.logs_before, bf16[512,128]{1,0:T(8,128)(2,1)} %get-tuple-element.28.reads, ...), custom_call_target="tpu_custom_call" | custom-call | flops 10000000 | bytes 1384448 | tf_op jit(solution)/shard_map/pallas_call | solution.py:242
  136.1 11.6 %all_to_all.21.squares = f32[4,8,512]{2,1,0:T(8,128)S(1)} all-to-all(f32[4,8,512]{2,1,0:T(8,128)S(1)} %broadcast_in_dim.56), channel_id=1, replica_groups=mesh['sp_0'=8,'sp_1'=8,'sp_2'=2,'tp'=4] {'tp'}, dimensions={0} | all-to-all | bytes 131072 | tf_op jit(solution)/shard_map/all_to_all | solution.py:26
  147.7 3.0 %shard_map.196 = bf16[4,512,512]{2,1,0:T(8,128)(2,1)S(1)} custom-call(bf16[512,256]{1,0:T(8,128)(2,1)} %get-tuple-element.23.pool, bf16[512,256]{1,0:T(8,128)(2,1)S(1)} %get-tuple-element.31.rows, f32[4,8,512]{2,1,0:T(8,128)S(1)} %all_to_all.21.squares, bf16[2048,1152]{1,0:T(8,128)(2,1)} %all-gather.3.cloned.1.call-done.weight.weight_read), custom_call_target="tpu_custom_call" | custom-call | flops 1073741824 | bytes 5308416 | tf_op jit(solution)/shard_map/pallas_call | solution.py:242
  150.8 28.1 %all_to_all.22 = bf16[4,512,512]{2,1,0:T(8,128)(2,1)S(1)} all-to-all(bf16[4,512,512]{2,1,0:T(8,128)(2,1)S(1)} %shard_map.196), channel_id=1, replica_groups=mesh['sp_0'=8,'sp_1'=8,'sp_2'=2,'tp'=4] {'tp'}, dimensions={0} | all-to-all | bytes 4194304 | tf_op jit(solution)/shard_map/all_to_all | solution.py:409
  178.9 1.2 reduce_sum.12
  (36 shorter events, 0.1 us)
Async XLA Ops:
  6.5 113.0 %all-gather.3.cloned.1.call-start = ((), (), s32[]{:S(2)}) async-start(), calls=%async_computation.4 | async-start | bytes 4755456 | tf_op jit(solution)/shard_map/all_gather | solution.py:309
  9.7 43.6 %copy-start.3 = (bf16[512,512]{1,0:T(8,128)(2,1)S(1)}, bf16[512,512]{1,0:T(8,128)(2,1)}, u32[]{:S(2)}) copy-start(bf16[512,512]{1,0:T(8,128)(2,1)} %param.20) | copy-start | bytes 1572868
  9.7 46.8 %copy-start.9 = (bf16[512]{0:T(512)(128)(2,1)S(1)}, bf16[512]{0:T(512)(128)(2,1)}, u32[]{:S(2)}) copy-start(bf16[512]{0:T(512)(128)(2,1)} %param.21) | copy-start | bytes 3076
  9.7 57.9 %copy-start.13 = (f32[4]{0:T(128)S(1)}, f32[4]{0:T(128)}, u32[]{:S(2)}) copy-start(f32[4]{0:T(128)} %param.34) | copy-start | bytes 52
  9.8 57.9 %copy-start.14 = (f32[4]{0:T(128)S(1)}, f32[4]{0:T(128)}, u32[]{:S(2)}) copy-start(f32[4]{0:T(128)} %param.33) | copy-start | bytes 52
  9.8 58.0 %copy-start.7 = (f32[4,64]{1,0:T(4,128)S(1)}, f32[4,64]{1,0:T(4,128)}, u32[]{:S(2)}) copy-start(f32[4,64]{1,0:T(4,128)} %param.32) | copy-start | bytes 3076
  9.8 58.0 %copy-start.12 = (f32[4]{0:T(128)S(1)}, f32[4]{0:T(128)}, u32[]{:S(2)}) copy-start(f32[4]{0:T(128)} %param.36) | copy-start | bytes 52
  9.8 58.1 %copy-start.10 = (f32[256]{0:T(256)S(1)}, f32[256]{0:T(256)}, u32[]{:S(2)}) copy-start(f32[256]{0:T(256)} %param.29) | copy-start | bytes 3076
  9.8 58.1 %copy-start.11 = (f32[256]{0:T(256)S(1)}, f32[256]{0:T(256)}, u32[]{:S(2)}) copy-start(f32[256]{0:T(256)} %param.37) | copy-start | bytes 3076
  9.8 58.1 %copy-start.5 = (f32[512,4]{0,1:T(4,128)S(1)}, f32[512,4]{0,1:T(4,128)}, u32[]{:S(2)}) copy-start(f32[512,4]{0,1:T(4,128)} %param.35) | copy-start | bytes 24580
  9.8 58.7 %copy-start.6 = (f32[4,256]{1,0:T(4,128)S(1)}, f32[4,256]{1,0:T(4,128)}, u32[]{:S(2)}) copy-start(f32[4,256]{1,0:T(4,128)} %param.30) | copy-start | bytes 12292
  9.8 58.7 %copy-start.8 = (f32[4,64]{1,0:T(4,128)S(1)}, f32[4,64]{1,0:T(4,128)}, u32[]{:S(2)}) copy-start(f32[4,64]{1,0:T(4,128)} %param.31) | copy-start | bytes 3076
  51.3 37.7 %collective-permute-start.4 = (bf16[64,16,384]{2,1,0:T(8,128)(2,1)S(1)}, bf16[64,16,384]{2,1,0:T(8,128)(2,1)}, u32[]{:S(2)}, u32[]{:S(2)}) collective-permute-start(bf16[64,16,384]{2,1,0:T(8,128)(2,1)S(1)} %all_to_all.20.mine), channel_id=1, source_target_pairs={{0,4},{4,0},{1,5},{5,1},{2,6},{6,2},{3,7},{7,3},{8,12},{12,8},{9,1... | collective-permute-start | bytes 2359304 | tf_op jit(solution)/shard_map/ppermute | solution.py:313
  53.2 3.2 %collective-permute-start = (bf16[16,512]{1,0:T(8,128)(2,1)S(1)}, bf16[16,512]{1,0:T(8,128)(2,1)S(1)}, u32[]{:S(2)}, u32[]{:S(2)}) collective-permute-start(bf16[16,512]{1,0:T(8,128)(2,1)S(1)} %slice.3), channel_id=1, source_target_pairs={{0,4},{4,8},{8,12},{12,16},{16,20},{20,24},{24,28},{28,32},{32,36}... | collective-permute-start | bytes 49160 | tf_op jit(solution)/shard_map/ppermute | solution.py:315
  56.5 30.1 %copy-start.1 = (bf16[544,512]{1,0:T(8,128)(2,1)}, bf16[544,512]{1,0:T(8,128)(2,1)S(1)}, u32[]{:S(2)}) copy-start(bf16[544,512]{1,0:T(8,128)(2,1)S(1)} %pad_maximum_fusion.x0) | copy-start | bytes 1671172
  56.5 17.1 %collective-permute-start.1 = (bf16[544,512]{1,0:T(8,128)(2,1)S(1)}, bf16[544,512]{1,0:T(8,128)(2,1)S(1)}, u32[]{:S(2)}, u32[]{:S(2)}) collective-permute-start(bf16[544,512]{1,0:T(8,128)(2,1)S(1)} %pad_maximum_fusion.x0), channel_id=1, source_target_pairs={{0,3},{1,0},{2,1},{3,2},{4,7},{5,4},{6,5},{7,6},{8,11},{9,8},{10,9... | collective-permute-start | bytes 1671176 | tf_op jit(solution)/shard_map/ppermute | solution.py:321
  59.0 18.2 %collective-permute-start.2 = (bf16[544,512]{1,0:T(8,128)(2,1)S(1)}, bf16[544,512]{1,0:T(8,128)(2,1)S(1)}, u32[]{:S(2)}, u32[]{:S(2)}) collective-permute-start(bf16[544,512]{1,0:T(8,128)(2,1)S(1)} %pad_maximum_fusion.x0), channel_id=1, source_target_pairs={{0,1},{1,2},{2,3},{3,0},{4,5},{5,6},{6,7},{7,4},{8,9},{9,10},{10,1... | collective-permute-start | bytes 1671176 | tf_op jit(solution)/shard_map/ppermute | solution.py:321
  62.4 24.2 %collective-permute-start.3 = (bf16[544,512]{1,0:T(8,128)(2,1)S(1)}, bf16[544,512]{1,0:T(8,128)(2,1)}, u32[]{:S(2)}, u32[]{:S(2)}) collective-permute-start(bf16[544,512]{1,0:T(8,128)(2,1)S(1)} %pad_maximum_fusion.x0), channel_id=1, source_target_pairs={{0,2},{1,3},{2,0},{3,1},{4,6},{5,7},{6,4},{7,5},{8,10},{9,11},{10,... | collective-permute-start | bytes 1671176 | tf_op jit(solution)/shard_map/ppermute | solution.py:321
  73.6 3.5 %copy-start.2 = (bf16[544,512]{1,0:T(8,128)(2,1)}, bf16[544,512]{1,0:T(8,128)(2,1)S(1)}, u32[]{:S(2)}) copy-start(bf16[544,512]{1,0:T(8,128)(2,1)S(1)} %collective-permute-done.1.x3) | copy-start | bytes 1671172
  77.1 0.8 copy-start.4
  89.0 5.4 %copy-start = (bf16[4,528,512]{2,1,0:T(8,128)(2,1)}, bf16[4,528,512]{2,1,0:T(8,128)(2,1)S(1)}, u32[]{:S(2)}) copy-start(bf16[4,528,512]{2,1,0:T(8,128)(2,1)S(1)} %shard_map.191.normed) | copy-start | bytes 6488068
  114.6 18.7 %all-to-all-start.1 = ((bf16[8,80,256]{2,1,0:T(8,128)(2,1)}), bf16[8,80,256]{2,1,0:T(8,128)(2,1)S(1)}, u32[]{:S(2)}, u32[]{:S(2)}) async-start(bf16[8,80,256]{2,1,0:T(8,128)(2,1)} %broadcast_in_dim.55), calls=%async_computation.1 | async-start | bytes 655360 | tf_op jit(solution)/shard_map/all_to_all | solution.py:26
Sparse Core Ops, SparseCore 0:
  10.5 95.9 all-gather.2

commit v5 on v4

--- a/solution.py
+++ b/solution.py
@@ -51,15 +51,19 @@
     return silu(total).astype(BF16)
 
 
+def three_parts(row):
+    high = row.astype(BF16).astype(F32)
+    middle = (row - high).astype(BF16).astype(F32)
+    low = row - high - middle
+    at = lax.broadcasted_iota(jnp.int32, (PAY, row.shape[1]), 0)
+    parts = jnp.where(at == 0, high, jnp.where(at == 1, middle, jnp.where(at == 2, low, 0.0)))
+    return parts.astype(BF16)
+
+
 def write_payload(ref, state, log_row):
     rows = state.shape[0]
-    high = log_row.astype(BF16).astype(F32)
-    middle = (log_row - high).astype(BF16).astype(F32)
-    low = log_row - high - middle
-    at = lax.broadcasted_iota(jnp.int32, (PAY, log_row.shape[1]), 0)
-    tail = jnp.where(at == 0, high, jnp.where(at == 1, middle, jnp.where(at == 2, low, 0.0)))
     ref[:rows] = state.astype(BF16)
-    ref[rows:] = tail.astype(BF16)
+    ref[rows:] = three_parts(log_row)
 
 
 def read_payload(ref, k):
@@ -199,30 +203,41 @@
         local_out[here] = jnp.concatenate(results, axis=1) + params[24:25, :span] * values[here]
 
 
-def third_kernel(
-    planes, before, logs_before, reads, local_in, gate, cum, params, rows_out, squares_out
-):
+def third_kernel(planes, before, logs_before, reads, local_in, gate, cum, params, pool, out):
     _, _, earlier, _ = scan_payloads(planes, lax.axis_index("sp_0"))
     incoming = earlier * jnp.exp(logs_before[:1]) + before[...]
-    lanes = heads_of_lanes(local_in.shape[1])
+    length, span = local_in.shape
+    lanes = heads_of_lanes(span)
     decay = dot(jnp.exp(cum[...]), lanes, 0, 0, HIGH)
     far = dot(reads[:, :HEAD].astype(F32), incoming, precision=HIGH) * decay
     gated = (local_in[...] + far) * silu(gate[...].astype(F32))
-    ones = jnp.ones((8, gated.shape[1]), F32)
-    squares_out[...] = dot(ones, gated * gated, 1, 1, HIGH)
-    rows_out[...] = (gated * params[26:27, : gated.shape[1]]).astype(BF16)
-
-
-def out_kernel(pool, rows, squares, weight, out):
-    span = pool.shape[1]
-    mean = jnp.sum(squares[...], axis=0) / MIX_W
-    scale = jnp.transpose(lax.rsqrt(mean + EPSILON))[:, :1]
-    for d in range(out.shape[0]):
-        width = out.shape[2]
-        block = weight[d * width : (d + 1) * width]
-        terms = dot(pool[...], block[:, :span], 1, 1)
-        terms = terms + dot(rows[...], block[:, span:], 1, 1) * scale
-        out[d] = terms.astype(BF16)
+    ones = jnp.ones((8, span), F32)
+    squares = dot(ones, gated * gated, 1, 1, HIGH)
+    out[:length, :span] = pool[...]
+    out[:length, span:] = (gated * params[26:27, :span]).astype(BF16)
+    out[length:] = three_parts(squares[:1])
+
+
+def out_kernel(rows, weight, out):
+    length = out.shape[0]
+    span = rows.shape[2] // 2
+    count = rows.shape[0]
+    halves = weight.shape[0] // (count * span)
+    squares = jnp.zeros((1, length), F32)
+    for j in range(count):
+        parts = rows[j, length:].astype(F32)
+        squares = squares + jnp.sum(parts, axis=0, keepdims=True)
+    scale = lax.rsqrt(squares / MIX_W + EPSILON)
+    scale = jnp.transpose(jnp.broadcast_to(scale, (8, length)))[:, :1]
+    for half in range(halves):
+        pooled = jnp.zeros((length, span), F32)
+        states = jnp.zeros((length, span), F32)
+        for j in range(count):
+            first = (half * count + j) * span
+            block = weight[first : first + span]
+            pooled = pooled + dot(rows[j, :length, :span], block[:, :span], 1, 1)
+            states = states + dot(rows[j, :length, span:], block[:, span:], 1, 1)
+        out[:, half * span : (half + 1) * span] = (pooled + states * scale).astype(BF16)
 
 
 def whole(shape):
@@ -294,13 +309,23 @@
     state = key_weight.shape[1]
     heads = step_weight.shape[1]
     count = lax.axis_size("tp")
+    planes = lax.axis_size("sp_0")
+    half = planes // count
+    out_weights = lax.ppermute(
+        jnp.transpose(jnp.concatenate([out_pool_weight, out_state_weight], axis=0)),
+        ("sp_0", "tp"),
+        [
+            (z * count + x, (z % half * count + x) * count + z // half)
+            for z in range(planes)
+            for x in range(count)
+        ],
+    )
     fill = jnp.zeros((read_weight.shape[0], BLOCK - state), BF16)
     joined = jnp.concatenate(
         [
             pool_weight,
             gate_weight,
-            jnp.transpose(out_pool_weight),
-            jnp.transpose(out_state_weight),
+            out_weights,
             read_weight,
             fill,
         ],
@@ -388,26 +413,24 @@
         },
         far=range(9),
     )
-    gated, squares = call(
+    rows_here = call(
         third_kernel,
         "third",
-        (plane_pieces, before_row, logs_row, reads, inside, gate, cum, params),
-        (shape_of((length, mix), BF16), shape_of((8, length), F32)),
+        (plane_pieces, before_row, logs_row, reads, inside, gate, cum, params, pool_out),
+        (shape_of((length + PAY, 2 * mix), BF16),),
         10**7,
-        far=range(1, 8),
-    )
-    all_squares = sent_to_all(squares, "tp")
-    terms = call(
+        far=range(1, 9),
+    )[0]
+    all_rows = sent_to_all(rows_here, "tp")
+    return call(
         out_kernel,
         "out",
-        (pool_out, gated, all_squares, later_weights),
-        (shape_of((count, length, width), BF16),),
+        (all_rows, later_weights),
+        (shape_of((length, width), BF16),),
         2 * length * 2 * mix * D,
-        specs={3: pl.BlockSpec((D, 2 * mix), lambda *_: (0, 1))},
-        far=(0, 3),
+        specs={1: pl.BlockSpec((D, 2 * mix), lambda *_: (0, 1))},
+        far=(1,),
     )[0]
-    arrived = lax.all_to_all(terms, "tp", split_axis=0, concat_axis=0, tiled=True)
-    return arrived.astype(F32).sum(axis=0).astype(BF16)
 
 
 def solution(mesh):

time: 188 us -> 191 us (1.016)
  the two profiles are of different devices: /device:TPU:2 before, /device:TPU:1 now
where the time goes in v5:
time: 191 us
  blocking collectives  95.5 us (50%)
  Pallas kernels  24.3 us (13%)
  starting transfers between devices  24.1 us (13%)
  waiting for transfers between devices  23.9 us (13%)
  between operations  13.7 us (7%)
  local copies, waits for them, and re-layouts  7.5 us (4%)
    all_to_all x2, blocking collectives, sent_to_all(): return lax.all_to_all(copies, axis, split_axis=0, concat_axis=0, tiled=True)  77.3 us
    pallas_call x7, Pallas kernels, call(): pl.pallas_call(kernel, grid=(1,), in_specs=[specs.get(k, whole(a.shape))...  24.3 us
    all_gather x1, blocking collectives, local(): row_pieces = lax.all_gather(payload, ('sp_1', 'sp_2'))  18.2 us
    ppermute x3, waiting for transfers between devices, local(): pieces.append(lax.ppermute(sent, 'tp', pairs))  17.3 us
    ppermute x3, starting transfers between devices, local(): pieces.append(lax.ppermute(sent, 'tp', pairs))  9.74 us
    ppermute x1, starting transfers between devices, local(): other = lax.ppermute(mine, 'sp_2', [(0, 1), (1, 0)])  6.63 us
    all_to_all x1, waiting for transfers between devices, sent_to_all(): return lax.all_to_all(copies, axis, split_axis=0, concat_axis=0, tiled=True)  5.72 us
    all_to_all x1, starting transfers between devices, sent_to_all(): return lax.all_to_all(copies, axis, split_axis=0, concat_axis=0, tiled=True)  3.97 us
  transfers between devices with their start and end apart: 8, of which 5 were waited for; matrix products, arithmetic and copies ran while one was open for 3% of the time, Pallas kernels for 9%

profile of v5, /device:TPU:1, one launch (start us, length us, event | category | flops | bytes accessed | tf_op | source)
XLA Modules:
  0.0 190.6 jit_solution(1111617328742681523)
XLA Ops:
  6.5 0.7 maximum_bitcast_fusion
  7.3 0.7 collective-permute-start.5
  7.9 1.4 concatenate.23
  9.3 0.0 all-gather.3.cloned.1.call-update
  9.4 0.8 copy.21
  10.1 0.1 pad.44.clone
  10.2 0.8 maximum_maximum_fusion
  11.0 0.1 broadcast_in_dim.47
  11.1 0.0 copy-start.13
  11.1 0.0 copy-start.14
  11.1 0.0 copy-start.7
  11.1 0.0 copy-start.12
  11.1 0.0 copy-start.10
  11.2 0.0 copy-start.11
  11.2 0.0 copy-start.5
  11.2 0.0 copy-start.6
  11.2 0.0 copy-start.8
  11.2 47.7 %all_to_all.15.mine = bf16[64,16,384]{2,1,0:T(8,128)(2,1)S(1)} all-to-all(bf16[64,16,384]{2,1,0:T(8,128)(2,1)S(1)} %broadcast_in_dim.47), channel_id=1, replica_groups=mesh['sp_0'=8,'sp_1'=8,'sp_2'=2,'tp'=4] {'sp_0','sp_1'}, dimensions={0} | all-to-all | bytes 1572864 | tf_op jit(solution)/shard_map/all_to_all | solution.py:26
  58.9 6.6 %collective-permute-start.4 = (bf16[64,16,384]{2,1,0:T(8,128)(2,1)S(1)}, bf16[64,16,384]{2,1,0:T(8,128)(2,1)}, u32[]{:S(2)}, u32[]{:S(2)}) collective-permute-start(bf16[64,16,384]{2,1,0:T(8,128)(2,1)S(1)} %all_to_all.15.mine), channel_id=1, source_target_pairs={{0,4},{4,0},{1,5},{5,1},{2,6},{6,2},{3,7},{7,3},{8,12},{12,8},{9,1... | collective-permute-start | bytes 2359304 | tf_op jit(solution)/shard_map/ppermute | solution.py:338
  65.5 3.1 %collective-permute-start = (bf16[16,512]{1,0:T(8,128)(2,1)S(1)}, bf16[16,512]{1,0:T(8,128)(2,1)S(1)}, u32[]{:S(2)}, u32[]{:S(2)}) collective-permute-start(bf16[16,512]{1,0:T(8,128)(2,1)S(1)} %slice.3), channel_id=1, source_target_pairs={{0,4},{4,8},{8,12},{12,16},{16,20},{20,24},{24,28},{28,32},{32,36}... | collective-permute-start | bytes 49160 | tf_op jit(solution)/shard_map/ppermute | solution.py:340
  68.7 0.8 collective-permute-done
  69.6 2.9 %collective-permute-start.1 = (bf16[544,512]{1,0:T(8,128)(2,1)S(1)}, bf16[544,512]{1,0:T(8,128)(2,1)S(1)}, u32[]{:S(2)}, u32[]{:S(2)}) collective-permute-start(bf16[544,512]{1,0:T(8,128)(2,1)S(1)} %pad_maximum_fusion.x0), channel_id=1, source_target_pairs={{0,3},{1,0},{2,1},{3,2},{4,7},{5,4},{6,5},{7,6},{8,11},{9,8},{10,9... | collective-permute-start | bytes 1671176 | tf_op jit(solution)/shard_map/ppermute | solution.py:346
  72.5 3.2 %collective-permute-start.2 = (bf16[544,512]{1,0:T(8,128)(2,1)S(1)}, bf16[544,512]{1,0:T(8,128)(2,1)S(1)}, u32[]{:S(2)}, u32[]{:S(2)}) collective-permute-start(bf16[544,512]{1,0:T(8,128)(2,1)S(1)} %pad_maximum_fusion.x0), channel_id=1, source_target_pairs={{0,1},{1,2},{2,3},{3,0},{4,5},{5,6},{6,7},{7,4},{8,9},{9,10},{10,1... | collective-permute-start | bytes 1671176 | tf_op jit(solution)/shard_map/ppermute | solution.py:346
  75.6 3.7 %collective-permute-start.3 = (bf16[544,512]{1,0:T(8,128)(2,1)S(1)}, bf16[544,512]{1,0:T(8,128)(2,1)}, u32[]{:S(2)}, u32[]{:S(2)}) collective-permute-start(bf16[544,512]{1,0:T(8,128)(2,1)S(1)} %pad_maximum_fusion.x0), channel_id=1, source_target_pairs={{0,2},{1,3},{2,0},{3,1},{4,6},{5,7},{6,4},{7,5},{8,10},{9,11},{10,... | collective-permute-start | bytes 1671176 | tf_op jit(solution)/shard_map/ppermute | solution.py:346
  79.4 0.1 broadcast_in_dim.50
  79.5 0.1 broadcast_in_dim_reshape.3
  79.6 0.6 pad.36.extra
  80.3 0.1 broadcast_in_dim.49
  80.3 0.1 broadcast_in_dim.48
  80.4 2.4 %concatenate.21.params = f32[32,384]{1,0:T(8,128)} concatenate(f32[4,384]{1,0:T(4,128)S(1)} %select_maximum_fusion, f32[4,384]{1,0:T(4,128)S(1)} %pad.30, f32[8,384]{1,0:T(8,128)S(1)} %broadcast_in_dim.48, f32[8,384]{1,0:T(8,128)S(1)} %broadcast_in_dim.49, f32[1,384]{1,0:T(1,128)S(1)} %pad.33, f32[1,384]{1,0:T(1,128)S(1)} %pad.34, f32[1,384]{1,0:T(1,128)S(1)} %pad.35, ...), dimensions={0} | concatenate | bytes 98304 | tf_op jit(solution)/shard_map/concatenate | solution.py:360
  82.8 4.1 %collective-permute-done.1.x3 = bf16[544,512]{1,0:T(8,128)(2,1)S(1)} collective-permute-done((bf16[544,512]{1,0:T(8,128)(2,1)S(1)}, bf16[544,512]{1,0:T(8,128)(2,1)S(1)}, u32[]{:S(2)}, u32[]{:S(2)}) %collective-permute-start.1) | collective-permute-done | bytes 557088 | tf_op jit(solution)/shard_map/ppermute | solution.py:346
  86.9 1.0 shard_map.190.early
  87.9 2.3 %collective-permute-done.2.x1 = bf16[544,512]{1,0:T(8,128)(2,1)S(1)} collective-permute-done((bf16[544,512]{1,0:T(8,128)(2,1)S(1)}, bf16[544,512]{1,0:T(8,128)(2,1)S(1)}, u32[]{:S(2)}, u32[]{:S(2)}) %collective-permute-start.2) | collective-permute-done | bytes 557088 | tf_op jit(solution)/shard_map/ppermute | solution.py:346
  90.1 0.8 copy-done.4
  91.0 11.0 %collective-permute-done.3.x2 = bf16[544,512]{1,0:T(8,128)(2,1)} collective-permute-done((bf16[544,512]{1,0:T(8,128)(2,1)S(1)}, bf16[544,512]{1,0:T(8,128)(2,1)}, u32[]{:S(2)}, u32[]{:S(2)}) %collective-permute-start.3) | collective-permute-done | bytes 557088 | tf_op jit(solution)/shard_map/ppermute | solution.py:346
  102.0 2.4 %shard_map.191.normed = bf16[4,528,512]{2,1,0:T(8,128)(2,1)S(1)} custom-call(f32[528,1]{1,0:T(8,128)} %shard_map.190.early, bf16[544,512]{1,0:T(8,128)(2,1)} %copy-done.1, bf16[544,512]{1,0:T(8,128)(2,1)} %copy-done.4, bf16[544,512]{1,0:T(8,128)(2,1)} %collective-permute-done.3.x2, bf16[544,512]{1,0:T(8,128)(2,1)} %copy-done.2), custom_call_target="tpu_custom_call" | custom-call | flops 1000000 | bytes 2230336 | tf_op jit(solution)/shard_map/pallas_call | solution.py:257
  104.4 5.4 %shard_map.192 = (bf16[512,256]{1,0:T(8,128)(2,1)}, bf16[512,128]{1,0:T(8,128)(2,1)}, f32[8,512]{1,0:T(8,128)}, f32[8,512]{1,0:T(8,128)}, bf16[80,256]{1,0:T(8,128)(2,1)S(1)}) custom-call(bf16[4,528,512]{2,1,0:T(8,128)(2,1)S(1)} %shard_map.191.normed, bf16[64,16,384]{2,1,0:T(8,128)(2,1)S(1)} %all_to_all.15.mine, ...), custom_call_target="tpu_custom_call" | custom-call | flops 830472192 | bytes 3801088 | tf_op jit(solution)/shard_map/pallas_call | solution.py:257
  109.8 18.2 %all-gather = bf16[1280,256]{1,0:T(8,128)(2,1)S(1)} all-gather(bf16[80,256]{1,0:T(8,128)(2,1)S(1)} %get-tuple-element.17), channel_id=2, replica_groups=mesh['sp_0'=8,'sp_1'=8,'sp_2'=2,'tp'=4] {'sp_1','sp_2'}, dimensions={0}, use_global_device_ids=true | all-gather | bytes 696320 | tf_op jit(solution)/shard_map/all_gather | solution.py:390
  128.0 0.9 shard_map.193
  128.9 0.8 broadcast_in_dim.54
  129.6 4.0 %all-to-all-start.1 = ((bf16[8,80,256]{2,1,0:T(8,128)(2,1)}), bf16[8,80,256]{2,1,0:T(8,128)(2,1)S(1)}, u32[]{:S(2)}, u32[]{:S(2)}) async-start(bf16[8,80,256]{2,1,0:T(8,128)(2,1)} %broadcast_in_dim.54), calls=%async_computation.1 | async-start | bytes 655360 | tf_op jit(solution)/shard_map/all_to_all | solution.py:26
  133.6 0.0 all-gather.3.cloned.1.call-done.weight.weight_read
  133.6 8.0 %shard_map.194 = (bf16[512,256]{1,0:T(8,128)(2,1)}, bf16[512,256]{1,0:T(8,128)(2,1)}, bf16[512,128]{1,0:T(8,128)(2,1)}, f32[512,256]{1,0:T(8,128)}) custom-call(bf16[4,528,512]{2,1,0:T(8,128)(2,1)} %copy-done, bf16[2048,1152]{1,0:T(8,128)(2,1)} %all-gather.3.cloned.1.call-done.weight.weight_read, ...), custom_call_target="tpu_custom_call" | custom-call | flops 1384120320 | bytes 12206080 | tf_op jit(solution)/shard_map/pallas_call | solution.py:257
  141.6 5.7 %all-to-all-done.1.planes = bf16[8,80,256]{2,1,0:T(8,128)(2,1)S(1)} async-done(((bf16[8,80,256]{2,1,0:T(8,128)(2,1)}), bf16[8,80,256]{2,1,0:T(8,128)(2,1)S(1)}, u32[]{:S(2)}, u32[]{:S(2)}) %all-to-all-start.1) | async-done | bytes 327712 | tf_op jit(solution)/shard_map/all_to_all | solution.py:26
  147.3 2.9 %shard_map.195 = bf16[528,512]{1,0:T(8,128)(2,1)S(1)} custom-call(bf16[8,80,256]{2,1,0:T(8,128)(2,1)S(1)} %all-to-all-done.1.planes, f32[64,256]{1,0:T(8,128)} %get-tuple-element.19.before, f32[8,256]{1,0:T(8,128)} %get-tuple-element.20.logs_before, bf16[512,128]{1,0:T(8,128)(2,1)} %get-tuple-element.25.reads, f32[512,256]{1,0:T(8,128)} %get-tuple-element.26.local_in, ...), custom_call_target="tpu_custom_call" | custom-call | flops 10000000 | bytes 1646592 | tf_op jit(solution)/shard_map/pallas_call | solution.py:257
  150.3 0.2 broadcast_in_dim.56
  150.5 29.6 %all_to_all.16.rows = bf16[4,528,512]{2,1,0:T(8,128)(2,1)S(1)} all-to-all(bf16[4,528,512]{2,1,0:T(8,128)(2,1)S(1)} %broadcast_in_dim.56), channel_id=1, replica_groups=mesh['sp_0'=8,'sp_1'=8,'sp_2'=2,'tp'=4] {'tp'}, dimensions={0} | all-to-all | bytes 4325376 | tf_op jit(solution)/shard_map/all_to_all | solution.py:26
  180.1 3.7 %shard_map.196 = bf16[512,512]{1,0:T(8,128)(2,1)} custom-call(bf16[4,528,512]{2,1,0:T(8,128)(2,1)S(1)} %all_to_all.16.rows, bf16[2048,1152]{1,0:T(8,128)(2,1)} %all-gather.3.cloned.1.call-done.weight.weight_read), custom_call_target="tpu_custom_call" | custom-call | flops 1073741824 | bytes 6881280 | tf_op jit(solution)/shard_map/pallas_call | solution.py:257
  (37 shorter events, 0.1 us)
Async XLA Ops:
  6.5 127.1 %all-gather.3.cloned.1.call-start = ((), (), s32[]{:S(2)}) async-start(), calls=%async_computation.3 | async-start | bytes 4755456 | tf_op jit(solution)/shard_map/all_gather | solution.py:334
  7.3 0.7 collective-permute-start.5
  11.0 54.5 %copy-start.3 = (bf16[512,512]{1,0:T(8,128)(2,1)S(1)}, bf16[512,512]{1,0:T(8,128)(2,1)}, u32[]{:S(2)}) copy-start(bf16[512,512]{1,0:T(8,128)(2,1)} %param.20) | copy-start | bytes 1572868
  11.0 58.5 %copy-start.9 = (bf16[512]{0:T(512)(128)(2,1)S(1)}, bf16[512]{0:T(512)(128)(2,1)}, u32[]{:S(2)}) copy-start(bf16[512]{0:T(512)(128)(2,1)} %param.21) | copy-start | bytes 3076
  11.1 68.3 %copy-start.13 = (f32[4]{0:T(128)S(1)}, f32[4]{0:T(128)}, u32[]{:S(2)}) copy-start(f32[4]{0:T(128)} %param.34) | copy-start | bytes 52
  11.1 68.3 %copy-start.14 = (f32[4]{0:T(128)S(1)}, f32[4]{0:T(128)}, u32[]{:S(2)}) copy-start(f32[4]{0:T(128)} %param.33) | copy-start | bytes 52
  11.1 68.3 %copy-start.7 = (f32[4,64]{1,0:T(4,128)S(1)}, f32[4,64]{1,0:T(4,128)}, u32[]{:S(2)}) copy-start(f32[4,64]{1,0:T(4,128)} %param.32) | copy-start | bytes 3076
  11.1 68.3 %copy-start.12 = (f32[4]{0:T(128)S(1)}, f32[4]{0:T(128)}, u32[]{:S(2)}) copy-start(f32[4]{0:T(128)} %param.36) | copy-start | bytes 52
  11.1 68.5 %copy-start.10 = (f32[256]{0:T(256)S(1)}, f32[256]{0:T(256)}, u32[]{:S(2)}) copy-start(f32[256]{0:T(256)} %param.29) | copy-start | bytes 3076
  11.2 68.5 %copy-start.11 = (f32[256]{0:T(256)S(1)}, f32[256]{0:T(256)}, u32[]{:S(2)}) copy-start(f32[256]{0:T(256)} %param.37) | copy-start | bytes 3076
  11.2 68.5 %copy-start.5 = (f32[512,4]{0,1:T(4,128)S(1)}, f32[512,4]{0,1:T(4,128)}, u32[]{:S(2)}) copy-start(f32[512,4]{0,1:T(4,128)} %param.35) | copy-start | bytes 24580
  11.2 69.1 %copy-start.6 = (f32[4,256]{1,0:T(4,128)S(1)}, f32[4,256]{1,0:T(4,128)}, u32[]{:S(2)}) copy-start(f32[4,256]{1,0:T(4,128)} %param.30) | copy-start | bytes 12292
  11.2 69.1 %copy-start.8 = (f32[4,64]{1,0:T(4,128)S(1)}, f32[4,64]{1,0:T(4,128)}, u32[]{:S(2)}) copy-start(f32[4,64]{1,0:T(4,128)} %param.31) | copy-start | bytes 3076
  58.9 45.5 %collective-permute-start.4 = (bf16[64,16,384]{2,1,0:T(8,128)(2,1)S(1)}, bf16[64,16,384]{2,1,0:T(8,128)(2,1)}, u32[]{:S(2)}, u32[]{:S(2)}) collective-permute-start(bf16[64,16,384]{2,1,0:T(8,128)(2,1)S(1)} %all_to_all.15.mine), channel_id=1, source_target_pairs={{0,4},{4,0},{1,5},{5,1},{2,6},{6,2},{3,7},{7,3},{8,12},{12,8},{9,1... | collective-permute-start | bytes 2359304 | tf_op jit(solution)/shard_map/ppermute | solution.py:338
  65.5 4.0 %collective-permute-start = (bf16[16,512]{1,0:T(8,128)(2,1)S(1)}, bf16[16,512]{1,0:T(8,128)(2,1)S(1)}, u32[]{:S(2)}, u32[]{:S(2)}) collective-permute-start(bf16[16,512]{1,0:T(8,128)(2,1)S(1)} %slice.3), channel_id=1, source_target_pairs={{0,4},{4,8},{8,12},{12,16},{16,20},{20,24},{24,28},{28,32},{32,36}... | collective-permute-start | bytes 49160 | tf_op jit(solution)/shard_map/ppermute | solution.py:340
  69.6 32.4 %copy-start.1 = (bf16[544,512]{1,0:T(8,128)(2,1)}, bf16[544,512]{1,0:T(8,128)(2,1)S(1)}, u32[]{:S(2)}) copy-start(bf16[544,512]{1,0:T(8,128)(2,1)S(1)} %pad_maximum_fusion.x0) | copy-start | bytes 1671172
  69.6 17.3 %collective-permute-start.1 = (bf16[544,512]{1,0:T(8,128)(2,1)S(1)}, bf16[544,512]{1,0:T(8,128)(2,1)S(1)}, u32[]{:S(2)}, u32[]{:S(2)}) collective-permute-start(bf16[544,512]{1,0:T(8,128)(2,1)S(1)} %pad_maximum_fusion.x0), channel_id=1, source_target_pairs={{0,3},{1,0},{2,1},{3,2},{4,7},{5,4},{6,5},{7,6},{8,11},{9,8},{10,9... | collective-permute-start | bytes 1671176 | tf_op jit(solution)/shard_map/ppermute | solution.py:346
  72.5 17.7 %collective-permute-start.2 = (bf16[544,512]{1,0:T(8,128)(2,1)S(1)}, bf16[544,512]{1,0:T(8,128)(2,1)S(1)}, u32[]{:S(2)}, u32[]{:S(2)}) collective-permute-start(bf16[544,512]{1,0:T(8,128)(2,1)S(1)} %pad_maximum_fusion.x0), channel_id=1, source_target_pairs={{0,1},{1,2},{2,3},{3,0},{4,5},{5,6},{6,7},{7,4},{8,9},{9,10},{10,1... | collective-permute-start | bytes 1671176 | tf_op jit(solution)/shard_map/ppermute | solution.py:346
  75.6 26.3 %collective-permute-start.3 = (bf16[544,512]{1,0:T(8,128)(2,1)S(1)}, bf16[544,512]{1,0:T(8,128)(2,1)}, u32[]{:S(2)}, u32[]{:S(2)}) collective-permute-start(bf16[544,512]{1,0:T(8,128)(2,1)S(1)} %pad_maximum_fusion.x0), channel_id=1, source_target_pairs={{0,2},{1,3},{2,0},{3,1},{4,6},{5,7},{6,4},{7,5},{8,10},{9,11},{10,... | collective-permute-start | bytes 1671176 | tf_op jit(solution)/shard_map/ppermute | solution.py:346
  86.9 3.3 %copy-start.2 = (bf16[544,512]{1,0:T(8,128)(2,1)}, bf16[544,512]{1,0:T(8,128)(2,1)S(1)}, u32[]{:S(2)}) copy-start(bf16[544,512]{1,0:T(8,128)(2,1)S(1)} %collective-permute-done.1.x3) | copy-start | bytes 1671172
  90.1 0.8 copy-start.4
  104.4 5.4 %copy-start = (bf16[4,528,512]{2,1,0:T(8,128)(2,1)}, bf16[4,528,512]{2,1,0:T(8,128)(2,1)S(1)}, u32[]{:S(2)}) copy-start(bf16[4,528,512]{2,1,0:T(8,128)(2,1)S(1)} %shard_map.191.normed) | copy-start | bytes 6488068
  129.6 17.7 %all-to-all-start.1 = ((bf16[8,80,256]{2,1,0:T(8,128)(2,1)}), bf16[8,80,256]{2,1,0:T(8,128)(2,1)S(1)}, u32[]{:S(2)}, u32[]{:S(2)}) async-start(bf16[8,80,256]{2,1,0:T(8,128)(2,1)} %broadcast_in_dim.54), calls=%async_computation.1 | async-start | bytes 655360 | tf_op jit(solution)/shard_map/all_to_all | solution.py:26
Sparse Core Ops, SparseCore 0:
  10.5 105.1 all-gather.2

commit v6 on v4

--- a/solution.py
+++ b/solution.py
@@ -89,13 +89,9 @@
     return squares
 
 
-def early_kernel(x0, x3, out):
-    out[...] = squares_of((x0, x3), out.shape[0])
-
-
-def norm_kernel(early, x0, x1, x2, x3, normed):
+def norm_kernel(x0, x1, x2, x3, normed):
     total_rows = normed.shape[1]
-    scale = lax.rsqrt((early[...] + squares_of((x1, x2), total_rows)) / D + EPSILON)
+    scale = lax.rsqrt(squares_of((x0, x1, x2, x3), total_rows) / D + EPSILON)
     for k, piece in enumerate((x0, x1, x2, x3)):
         gain = piece[total_rows : total_rows + 1].astype(F32)
         normed[k] = (piece[:total_rows].astype(F32) * scale * gain).astype(BF16)
@@ -145,20 +141,58 @@
     write_payload(payload, total, logs)
 
 
+def inner_kernel(value, cum, step, factors, scaled):
+    length, span = scaled.shape
+    lanes = heads_of_lanes(span)
+    scaled[...] = (value[...].astype(F32) * dot(step[...], lanes, 0, 0, HIGH)).astype(BF16)
+    columns = jnp.transpose(cum[...])
+    lower = lax.broadcasted_iota(jnp.int32, (BLOCK, BLOCK), 0) >= lax.broadcasted_iota(
+        jnp.int32, (BLOCK, BLOCK), 1
+    )
+    at = 0
+    for i in range(length // BLOCK):
+        for h in range(span // HEAD):
+            for j in range(i + 1):
+                column = columns[i * BLOCK : (i + 1) * BLOCK, h : h + 1]
+                gap = column - cum[h : h + 1, j * BLOCK : (j + 1) * BLOCK]
+                if i == j:
+                    gap = jnp.where(lower, gap, -jnp.inf)
+                factors[at] = jnp.exp(gap)
+                at = at + 1
+
+
 def second_kernel(
-    normed, weight, weight_read, value, key, cum, step, params, mix_weight,
+    normed, weight, value, key, factors, scaled, params, mix_weight,
     pool_out, gate_out, read_out, local_out,
+    rows_here, weight_here, read_here, arrived,
 ):
     length, span = pool_out.shape
     place = lax.axis_index("tp")
-    total_rows = normed.shape[1]
-    acc = jnp.zeros((total_rows, weight.shape[1]), F32)
-    acc_read = jnp.zeros((total_rows, weight_read.shape[1]), F32)
-    width = normed.shape[2]
-    for k in range(normed.shape[0]):
+    count, total_rows, width = rows_here.shape
+    copies = []
+    for k in range(count):
         start = pl.multiple_of(((place - k) & 3) * width, width)
-        acc = acc + dot(normed[k], weight[pl.ds(start, width)])
-        acc_read = acc_read + dot(normed[k], weight_read[pl.ds(start, width)])
+        block = weight.at[pl.ds(start, width)]
+        copies.append(
+            [
+                pltpu.make_async_copy(normed.at[k], rows_here.at[k], arrived.at[k, 0]),
+                pltpu.make_async_copy(
+                    block.at[:, : 2 * span], weight_here.at[k], arrived.at[k, 1]
+                ),
+                pltpu.make_async_copy(
+                    block.at[:, 4 * span :], read_here.at[k], arrived.at[k, 2]
+                ),
+            ]
+        )
+        for copy in copies[k]:
+            copy.start()
+    acc = jnp.zeros((total_rows, 2 * span), F32)
+    acc_read = jnp.zeros((total_rows, BLOCK), F32)
+    for k in range(count):
+        for copy in copies[k]:
+            copy.wait()
+        acc = acc + dot(rows_here[k], weight_here[k])
+        acc_read = acc_read + dot(rows_here[k], read_here[k])
     gate_out[...] = acc[HALO:, span:].astype(BF16)
     running = acc[:, :span].astype(BF16).astype(F32)
     own = running[HALO:]
@@ -173,13 +207,7 @@
     pool_out[...] = (dot(pooled, mix_weight[...]) * params[25:26, :span]).astype(BF16)
     reads = convolved(acc_read.astype(BF16).astype(F32), params[4:8, :BLOCK], length)
     read_out[...] = reads
-    lanes = heads_of_lanes(span)
-    values = value[...].astype(F32)
-    scaled = (values * dot(step[...], lanes, 0, 0, HIGH)).astype(BF16)
-    columns = jnp.transpose(cum[...])
-    lower = lax.broadcasted_iota(jnp.int32, (BLOCK, BLOCK), 0) >= lax.broadcasted_iota(
-        jnp.int32, (BLOCK, BLOCK), 1
-    )
+    at = 0
     for i in range(length // BLOCK):
         here = slice(i * BLOCK, (i + 1) * BLOCK)
         products = [
@@ -189,14 +217,13 @@
         for h in range(span // HEAD):
             parts = []
             for j in range(i + 1):
-                gap = columns[here, h : h + 1] - cum[h : h + 1, j * BLOCK : (j + 1) * BLOCK]
-                if i == j:
-                    gap = jnp.where(lower, gap, -jnp.inf)
-                parts.append((products[j] * jnp.exp(gap)).astype(BF16))
+                parts.append((products[j] * factors[at]).astype(BF16))
+                at = at + 1
             left = jnp.concatenate(parts, axis=1)
-            right = scaled[: (i + 1) * BLOCK, h * HEAD : (h + 1) * HEAD]
-            results.append(dot(left, right))
-        local_out[here] = jnp.concatenate(results, axis=1) + params[24:25, :span] * values[here]
+            results.append(dot(left, scaled[: (i + 1) * BLOCK, h * HEAD : (h + 1) * HEAD]))
+        local_out[here] = jnp.concatenate(results, axis=1) + params[24:25, :span] * value[
+            here
+        ].astype(F32)
 
 
 def third_kernel(
@@ -213,9 +240,9 @@
     rows_out[...] = (gated * params[26:27, : gated.shape[1]]).astype(BF16)
 
 
-def out_kernel(pool, rows, squares, weight, out):
+def out_kernel(pool, rows, weight, s0, s1, s2, s3, out):
     span = pool.shape[1]
-    mean = jnp.sum(squares[...], axis=0) / MIX_W
+    mean = (s0[...] + s1[...] + s2[...] + s3[...]) / MIX_W
     scale = jnp.transpose(lax.rsqrt(mean + EPSILON))[:, :1]
     for d in range(out.shape[0]):
         width = out.shape[2]
@@ -229,7 +256,7 @@
     return pl.BlockSpec(shape, lambda *_: (0,) * len(shape))
 
 
-LIMITS = {"early": 8, "norm": 16, "first": 16, "row": 6, "second": 24, "third": 10, "out": 16}
+LIMITS = {"inner": 24, "norm": 16, "first": 16, "row": 6, "second": 24, "third": 10, "out": 16}
 
 
 def call(kernel, name, args, outs, flops, scratch=(), specs=None, far=()):
@@ -320,16 +347,13 @@
         pairs = [(k, (k + shift) % count) for k in range(count)]
         pieces.append(lax.ppermute(sent, "tp", pairs))
     rows = HALO + length
-    early = call(
-        early_kernel, "early", (pieces[0], pieces[-1]), (far_of((rows, 1), F32),), 10**6
-    )[0]
     normed = call(
         norm_kernel,
         "norm",
-        (early, *pieces),
+        pieces,
         (shape_of((count, rows, width), BF16),),
         10**6,
-        far=range(5),
+        far=range(4),
     )[0]
     lanes = mix + BLOCK
     params = jnp.concatenate(
@@ -371,10 +395,23 @@
         10**6,
     )
     plane_pieces = sent_to_all(payload, "sp_0")
+    blocks = length // BLOCK
+    factors, scaled = call(
+        inner_kernel,
+        "inner",
+        (value, cum, step),
+        (
+            far_of((heads * blocks * (blocks + 1) // 2, BLOCK, BLOCK), F32),
+            far_of((length, mix), BF16),
+        ),
+        10**7,
+        far=range(3),
+    )
+    anywhere = pl.BlockSpec(memory_space=pl.ANY)
     pool_out, gate, reads, inside = call(
         second_kernel,
         "second",
-        (normed, later_weights, later_weights, value, key, cum, step, params, pool_mix[0]),
+        (normed, later_weights, value, key, factors, scaled, params, pool_mix[0]),
         (
             far_of((length, mix), BF16),
             far_of((length, mix), BF16),
@@ -382,11 +419,14 @@
             far_of((length, mix), F32),
         ),
         2 * rows * D * (2 * mix + BLOCK),
-        specs={
-            1: pl.BlockSpec((D, 2 * mix), lambda *_: (0, 0)),
-            2: pl.BlockSpec((D, BLOCK), lambda *_: (0, 4 * mix // BLOCK)),
-        },
-        far=range(9),
+        [
+            pltpu.VMEM((count, rows, width), BF16),
+            pltpu.VMEM((count, width, 2 * mix), BF16),
+            pltpu.VMEM((count, width, BLOCK), BF16),
+            pltpu.SemaphoreType.DMA((count, 3)),
+        ],
+        specs={0: anywhere, 1: anywhere},
+        far=range(8),
     )
     gated, squares = call(
         third_kernel,
@@ -396,15 +436,18 @@
         10**7,
         far=range(1, 8),
     )
-    all_squares = sent_to_all(squares, "tp")
+    all_squares = [squares] + [
+        lax.ppermute(squares, "tp", [(k, (k + shift) % count) for k in range(count)])
+        for shift in range(1, count)
+    ]
     terms = call(
         out_kernel,
         "out",
-        (pool_out, gated, all_squares, later_weights),
+        (pool_out, gated, later_weights, *all_squares),
         (shape_of((count, length, width), BF16),),
         2 * length * 2 * mix * D,
-        specs={3: pl.BlockSpec((D, 2 * mix), lambda *_: (0, 1))},
-        far=(0, 3),
+        specs={2: pl.BlockSpec((D, 2 * mix), lambda *_: (0, 1))},
+        far=(0, 2),
     )[0]
     arrived = lax.all_to_all(terms, "tp", split_axis=0, concat_axis=0, tiled=True)
     return arrived.astype(F32).sum(axis=0).astype(BF16)

time: 188 us -> 192 us (1.021)
  blocking collectives: 99.7 us -> 88.7 us
  starting transfers between devices: 20.3 us -> 29 us
  Pallas kernels: 23.5 us -> 26.7 us
  waiting for transfers between devices: 20.3 us -> 23.2 us
    all_to_all x2 -> x1, blocking collectives: 53.1 us -> 41.3 us  [sent_to_all(): return lax.all_to_all(copies, axis, split_axis=0, concat_axis=0, tiled=True)]
    ppermute x0 -> x3, starting transfers between devices: none -> 9.54 us  [local(): lax.ppermute(squares, 'tp', [(k, (k + shift) % count) for k in range(coun...]
    ppermute x3, waiting for transfers between devices: 13.7 us -> 19 us  [local(): pieces.append(lax.ppermute(sent, 'tp', pairs))]
    all_to_all x1, waiting for transfers between devices: 5.76 us -> 1.61 us  [sent_to_all(): return lax.all_to_all(copies, axis, split_axis=0, concat_axis=0, tiled=True)]
    pallas_call x7, Pallas kernels: 23.5 us -> 26.7 us  [call(): pl.pallas_call(kernel, grid=(1,), in_specs=[specs.get(k, whole(a.shape))...]
  transfers between devices with their start and end apart: 7 -> 10, of which waited for: 5 -> 7; matrix products, arithmetic and copies ran while one was open for 3% -> 3% of each run, Pallas kernels for 9% -> 11%
where the time goes in v6:
time: 192 us; the launch traced here: 191 us
  blocking collectives  88.7 us (46%)
  starting transfers between devices  29 us (15%)
  Pallas kernels  26.7 us (14%)
  waiting for transfers between devices  23.2 us (12%)
  between operations  13.7 us (7%)
  local copies, waits for them, and re-layouts  7.45 us (4%)
  other arithmetic  2.08 us (1%)
    all_to_all x1, blocking collectives, sent_to_all(): return lax.all_to_all(copies, axis, split_axis=0, concat_axis=0, tiled=True)  41.3 us
    all_to_all x1, blocking collectives, local(): lax.all_to_all(terms, 'tp', split_axis=0, concat_axis=0, tiled=True)  29.4 us
    pallas_call x7, Pallas kernels, call(): pl.pallas_call(kernel, grid=(1,), in_specs=[specs.get(k, whole(a.shape))...  26.7 us
    ppermute x3, waiting for transfers between devices, local(): pieces.append(lax.ppermute(sent, 'tp', pairs))  19 us
    all_gather x1, blocking collectives, local(): row_pieces = lax.all_gather(payload, ('sp_1', 'sp_2'))  18.1 us
    ppermute x3, starting transfers between devices, local(): pieces.append(lax.ppermute(sent, 'tp', pairs))  10.5 us
    ppermute x3, starting transfers between devices, local(): lax.ppermute(squares, 'tp', [(k, (k + shift) % count) for k in range(coun...  9.54 us
    all_to_all x1, starting transfers between devices, sent_to_all(): return lax.all_to_all(copies, axis, split_axis=0, concat_axis=0, tiled=True)  4.59 us
  transfers between devices with their start and end apart: 10, of which 7 were waited for; matrix products, arithmetic and copies ran while one was open for 3% of the time, Pallas kernels for 11%

profile of v6, /device:TPU:2, one launch (start us, length us, event | category | flops | bytes accessed | tf_op | source)
XLA Modules:
  0.0 190.9 jit_solution(4351966608597803482)
XLA Ops:
  6.6 0.0 all-gather.3.cloned.1.call-start
  6.7 1.6 concatenate.16
  8.2 0.0 all-gather.3.cloned.1.call-update
  8.2 0.8 copy.21
  9.0 0.1 pad.42.clone
  9.1 0.8 maximum_maximum_fusion
  9.9 0.1 broadcast_in_dim.45
  10.0 41.3 %all_to_all.15.mine = bf16[64,16,384]{2,1,0:T(8,128)(2,1)S(1)} all-to-all(bf16[64,16,384]{2,1,0:T(8,128)(2,1)S(1)} %broadcast_in_dim.45), channel_id=1, replica_groups=mesh['sp_0'=8,'sp_1'=8,'sp_2'=2,'tp'=4] {'sp_0','sp_1'}, dimensions={0} | all-to-all | bytes 1572864 | tf_op jit(solution)/shard_map/all_to_all | solution.py:26
  51.3 1.9 %collective-permute-start.4 = (bf16[64,16,384]{2,1,0:T(8,128)(2,1)S(1)}, bf16[64,16,384]{2,1,0:T(8,128)(2,1)}, u32[]{:S(2)}, u32[]{:S(2)}) collective-permute-start(bf16[64,16,384]{2,1,0:T(8,128)(2,1)S(1)} %all_to_all.15.mine), channel_id=1, source_target_pairs={{0,4},{4,0},{1,5},{5,1},{2,6},{6,2},{3,7},{7,3},{8,12},{12,8},{9,1... | collective-permute-start | bytes 2359304 | tf_op jit(solution)/shard_map/ppermute | solution.py:340
  53.2 2.4 %collective-permute-start = (bf16[16,512]{1,0:T(8,128)(2,1)S(1)}, bf16[16,512]{1,0:T(8,128)(2,1)S(1)}, u32[]{:S(2)}, u32[]{:S(2)}) collective-permute-start(bf16[16,512]{1,0:T(8,128)(2,1)S(1)} %slice.3), channel_id=1, source_target_pairs={{0,4},{4,8},{8,12},{12,16},{16,20},{20,24},{24,28},{28,32},{32,36}... | collective-permute-start | bytes 49160 | tf_op jit(solution)/shard_map/ppermute | solution.py:342
  55.6 0.8 collective-permute-done
  56.5 0.0 copy-start.1
  56.5 3.4 %collective-permute-start.1 = (bf16[544,512]{1,0:T(8,128)(2,1)S(1)}, bf16[544,512]{1,0:T(8,128)(2,1)S(1)}, u32[]{:S(2)}, u32[]{:S(2)}) collective-permute-start(bf16[544,512]{1,0:T(8,128)(2,1)S(1)} %pad_maximum_fusion.x0), channel_id=1, source_target_pairs={{0,1},{1,2},{2,3},{3,0},{4,5},{5,6},{6,7},{7,4},{8,9},{9,10},{10,1... | collective-permute-start | bytes 1671176 | tf_op jit(solution)/shard_map/ppermute | solution.py:348
  59.9 3.0 %collective-permute-start.2 = (bf16[544,512]{1,0:T(8,128)(2,1)S(1)}, bf16[544,512]{1,0:T(8,128)(2,1)S(1)}, u32[]{:S(2)}, u32[]{:S(2)}) collective-permute-start(bf16[544,512]{1,0:T(8,128)(2,1)S(1)} %pad_maximum_fusion.x0), channel_id=1, source_target_pairs={{0,2},{1,3},{2,0},{3,1},{4,6},{5,7},{6,4},{7,5},{8,10},{9,11},{10,... | collective-permute-start | bytes 1671176 | tf_op jit(solution)/shard_map/ppermute | solution.py:348
  62.9 4.1 %collective-permute-start.3 = (bf16[544,512]{1,0:T(8,128)(2,1)S(1)}, bf16[544,512]{1,0:T(8,128)(2,1)}, u32[]{:S(2)}, u32[]{:S(2)}) collective-permute-start(bf16[544,512]{1,0:T(8,128)(2,1)S(1)} %pad_maximum_fusion.x0), channel_id=1, source_target_pairs={{0,3},{1,0},{2,1},{3,2},{4,7},{5,4},{6,5},{7,6},{8,11},{9,8},{10,9... | collective-permute-start | bytes 1671176 | tf_op jit(solution)/shard_map/ppermute | solution.py:348
  67.0 0.0 copy-done.13
  67.1 0.0 copy-done.7
  67.1 0.0 copy-done.12
  67.1 0.1 broadcast_in_dim.48
  67.2 0.1 broadcast_in_dim_reshape.3
  67.3 0.6 pad.36.extra
  67.9 0.1 broadcast_in_dim.47
  68.0 0.1 broadcast_in_dim.46
  68.1 2.4 %concatenate.19.params = f32[32,384]{1,0:T(8,128)} concatenate(f32[4,384]{1,0:T(4,128)S(1)} %select_maximum_fusion, f32[4,384]{1,0:T(4,128)S(1)} %pad.30, f32[8,384]{1,0:T(8,128)S(1)} %broadcast_in_dim.46, f32[8,384]{1,0:T(8,128)S(1)} %broadcast_in_dim.47, f32[1,384]{1,0:T(1,128)S(1)} %pad.33, f32[1,384]{1,0:T(1,128)S(1)} %pad.34, f32[1,384]{1,0:T(1,128)S(1)} %pad.35, ...), dimensions={0} | concatenate | bytes 98304 | tf_op jit(solution)/shard_map/concatenate | solution.py:359
  70.5 3.4 %collective-permute-done.1.x1 = bf16[544,512]{1,0:T(8,128)(2,1)S(1)} collective-permute-done((bf16[544,512]{1,0:T(8,128)(2,1)S(1)}, bf16[544,512]{1,0:T(8,128)(2,1)S(1)}, u32[]{:S(2)}, u32[]{:S(2)}) %collective-permute-start.1) | collective-permute-done | bytes 557088 | tf_op jit(solution)/shard_map/ppermute | solution.py:348
  73.9 5.0 %collective-permute-done.2.x2 = bf16[544,512]{1,0:T(8,128)(2,1)S(1)} collective-permute-done((bf16[544,512]{1,0:T(8,128)(2,1)S(1)}, bf16[544,512]{1,0:T(8,128)(2,1)S(1)}, u32[]{:S(2)}, u32[]{:S(2)}) %collective-permute-start.2) | collective-permute-done | bytes 557088 | tf_op jit(solution)/shard_map/ppermute | solution.py:348
  78.9 0.8 copy-done.4
  79.7 10.6 %collective-permute-done.3.x3 = bf16[544,512]{1,0:T(8,128)(2,1)} collective-permute-done((bf16[544,512]{1,0:T(8,128)(2,1)S(1)}, bf16[544,512]{1,0:T(8,128)(2,1)}, u32[]{:S(2)}, u32[]{:S(2)}) %collective-permute-start.3) | collective-permute-done | bytes 557088 | tf_op jit(solution)/shard_map/ppermute | solution.py:348
  90.3 2.5 %shard_map.190.normed = bf16[4,528,512]{2,1,0:T(8,128)(2,1)S(1)} custom-call(bf16[544,512]{1,0:T(8,128)(2,1)} %copy-done.1, bf16[544,512]{1,0:T(8,128)(2,1)} %copy-done.3, bf16[544,512]{1,0:T(8,128)(2,1)} %copy-done.4, bf16[544,512]{1,0:T(8,128)(2,1)} %collective-permute-done.3.x3), custom_call_target="tpu_custom_call" | custom-call | flops 1000000 | bytes 2228224 | tf_op jit(solution)/shard_map/pallas_call | solution.py:269
  92.8 0.0 collective-permute-done.4.other
  92.9 5.4 %shard_map.191 = (bf16[512,256]{1,0:T(8,128)(2,1)}, bf16[512,128]{1,0:T(8,128)(2,1)}, f32[8,512]{1,0:T(8,128)}, f32[8,512]{1,0:T(8,128)}, bf16[80,256]{1,0:T(8,128)(2,1)S(1)}) custom-call(bf16[4,528,512]{2,1,0:T(8,128)(2,1)S(1)} %shard_map.190.normed, bf16[64,16,384]{2,1,0:T(8,128)(2,1)S(1)} %all_to_all.15.mine, ...), custom_call_target="tpu_custom_call" | custom-call | flops 830472192 | bytes 3801088 | tf_op jit(solution)/shard_map/pallas_call | solution.py:269
  98.3 18.1 %all-gather = bf16[1280,256]{1,0:T(8,128)(2,1)S(1)} all-gather(bf16[80,256]{1,0:T(8,128)(2,1)S(1)} %get-tuple-element.28), channel_id=2, replica_groups=mesh['sp_0'=8,'sp_1'=8,'sp_2'=2,'tp'=4] {'sp_1','sp_2'}, dimensions={0}, use_global_device_ids=true | all-gather | bytes 696320 | tf_op jit(solution)/shard_map/all_gather | solution.py:389
  116.3 0.8 shard_map.194
  117.2 0.8 broadcast_in_dim.52
  117.9 4.6 %all-to-all-start.1 = ((bf16[8,80,256]{2,1,0:T(8,128)(2,1)}), bf16[8,80,256]{2,1,0:T(8,128)(2,1)S(1)}, u32[]{:S(2)}, u32[]{:S(2)}) async-start(bf16[8,80,256]{2,1,0:T(8,128)(2,1)} %broadcast_in_dim.52), calls=%async_computation.1 | async-start | bytes 655360 | tf_op jit(solution)/shard_map/all_to_all | solution.py:26
  122.5 3.3 %shard_map.192 = (f32[40,128,128]{2,1,0:T(8,128)}, bf16[512,256]{1,0:T(8,128)(2,1)}) custom-call(bf16[512,256]{1,0:T(8,128)(2,1)} %get-tuple-element.21.value, f32[8,512]{1,0:T(8,128)} %get-tuple-element.23.cum, f32[8,512]{1,0:T(8,128)} %get-tuple-element.24.step), custom_call_target="tpu_custom_call" | custom-call | flops 10000000 | bytes 294912 | tf_op jit(solution)/shard_map/pallas_call | solution.py:269
  125.8 8.9 %shard_map.193 = (bf16[512,256]{1,0:T(8,128)(2,1)}, bf16[512,256]{1,0:T(8,128)(2,1)}, bf16[512,128]{1,0:T(8,128)(2,1)}, f32[512,256]{1,0:T(8,128)}) custom-call(bf16[4,528,512]{2,1,0:T(8,128)(2,1)} %copy-done, bf16[2048,1152]{1,0:T(8,128)(2,1)} %all-gather.3.cloned.1.call-done.weight, bf16[512,256]{1,0:T(8,128)(2,1)} %get-tuple-element.21.value, ...), custom_call_target="tpu_custom_call" | custom-call | flops 1384120320 | bytes 10338304 | tf_op jit(solution)/shard_map/pallas_call | solution.py:269
  134.7 1.6 all-to-all-done.1.planes
  136.3 2.8 %shard_map.195 = (bf16[512,256]{1,0:T(8,128)(2,1)S(1)}, f32[8,512]{1,0:T(8,128)S(1)}) custom-call(bf16[8,80,256]{2,1,0:T(8,128)(2,1)S(1)} %all-to-all-done.1.planes, f32[64,256]{1,0:T(8,128)} %get-tuple-element.30.before, f32[8,256]{1,0:T(8,128)} %get-tuple-element.31.logs_before, bf16[512,128]{1,0:T(8,128)(2,1)} %get-tuple-element.32.reads, ...), custom_call_target="tpu_custom_call" | custom-call | flops 10000000 | bytes 1384448 | tf_op jit(solution)/shard_map/pallas_call | solution.py:269
  139.1 2.8 %collective-permute-start.5 = (f32[8,512]{1,0:T(8,128)S(1)}, f32[8,512]{1,0:T(8,128)S(1)}, u32[]{:S(2)}, u32[]{:S(2)}) collective-permute-start(f32[8,512]{1,0:T(8,128)S(1)} %get-tuple-element.36.s0), channel_id=1, source_target_pairs={{0,1},{1,2},{2,3},{3,0},{4,5},{5,6},{6,7},{7,4},{8,9},{9,10},{10,1... | collective-permute-start | bytes 49160 | tf_op jit(solution)/shard_map/ppermute | solution.py:440
  141.9 2.9 %collective-permute-start.6 = (f32[8,512]{1,0:T(8,128)S(1)}, f32[8,512]{1,0:T(8,128)S(1)}, u32[]{:S(2)}, u32[]{:S(2)}) collective-permute-start(f32[8,512]{1,0:T(8,128)S(1)} %get-tuple-element.36.s0), channel_id=1, source_target_pairs={{0,2},{1,3},{2,0},{3,1},{4,6},{5,7},{6,4},{7,5},{8,10},{9,11},{10,... | collective-permute-start | bytes 49160 | tf_op jit(solution)/shard_map/ppermute | solution.py:440
  144.8 3.8 %collective-permute-start.7 = (f32[8,512]{1,0:T(8,128)S(1)}, f32[8,512]{1,0:T(8,128)S(1)}, u32[]{:S(2)}, u32[]{:S(2)}) collective-permute-start(f32[8,512]{1,0:T(8,128)S(1)} %get-tuple-element.36.s0), channel_id=1, source_target_pairs={{0,3},{1,0},{2,1},{3,2},{4,7},{5,4},{6,5},{7,6},{8,11},{9,8},{10,9... | collective-permute-start | bytes 49160 | tf_op jit(solution)/shard_map/ppermute | solution.py:440
  148.6 0.0 collective-permute-done.5.s1
  148.7 0.5 collective-permute-done.6.s2
  149.1 1.3 collective-permute-done.7.s3
  150.4 3.0 %shard_map.196 = bf16[4,512,512]{2,1,0:T(8,128)(2,1)S(1)} custom-call(bf16[512,256]{1,0:T(8,128)(2,1)} %get-tuple-element.27.pool, bf16[512,256]{1,0:T(8,128)(2,1)S(1)} %get-tuple-element.35.rows, bf16[2048,1152]{1,0:T(8,128)(2,1)} %all-gather.3.cloned.1.call-done.weight, f32[8,512]{1,0:T(8,128)S(1)} %get-tuple-element.36.s0, ...), custom_call_target="tpu_custom_call" | custom-call | flops 1073741824 | bytes 5308416 | tf_op jit(solution)/shard_map/pallas_call | solution.py:269
  153.5 29.4 %all_to_all.16 = bf16[4,512,512]{2,1,0:T(8,128)(2,1)S(1)} all-to-all(bf16[4,512,512]{2,1,0:T(8,128)(2,1)S(1)} %shard_map.196), channel_id=1, replica_groups=mesh['sp_0'=8,'sp_1'=8,'sp_2'=2,'tp'=4] {'tp'}, dimensions={0} | all-to-all | bytes 4194304 | tf_op jit(solution)/shard_map/all_to_all | solution.py:452
  182.8 1.2 reduce_sum.12
  (40 shorter events, 0.1 us)
Async XLA Ops:
  6.5 46.7 %copy-start.2 = (bf16[512,512]{1,0:T(8,128)(2,1)S(1)}, bf16[512,512]{1,0:T(8,128)(2,1)}, u32[]{:S(2)}) copy-start(bf16[512,512]{1,0:T(8,128)(2,1)} %param.20) | copy-start | bytes 1572868
  6.5 49.9 %copy-start.9 = (bf16[512]{0:T(512)(128)(2,1)S(1)}, bf16[512]{0:T(512)(128)(2,1)}, u32[]{:S(2)}) copy-start(bf16[512]{0:T(512)(128)(2,1)} %param.21) | copy-start | bytes 3076
  6.5 60.5 %copy-start.13 = (f32[4]{0:T(128)S(1)}, f32[4]{0:T(128)}, u32[]{:S(2)}) copy-start(f32[4]{0:T(128)} %param.34) | copy-start | bytes 52
  6.5 60.5 %copy-start.14 = (f32[4]{0:T(128)S(1)}, f32[4]{0:T(128)}, u32[]{:S(2)}) copy-start(f32[4]{0:T(128)} %param.33) | copy-start | bytes 52
  6.5 60.5 %copy-start.7 = (f32[4,64]{1,0:T(4,128)S(1)}, f32[4,64]{1,0:T(4,128)}, u32[]{:S(2)}) copy-start(f32[4,64]{1,0:T(4,128)} %param.32) | copy-start | bytes 3076
  6.5 60.6 %copy-start.12 = (f32[4]{0:T(128)S(1)}, f32[4]{0:T(128)}, u32[]{:S(2)}) copy-start(f32[4]{0:T(128)} %param.36) | copy-start | bytes 52
  6.6 60.7 %copy-start.10 = (f32[256]{0:T(256)S(1)}, f32[256]{0:T(256)}, u32[]{:S(2)}) copy-start(f32[256]{0:T(256)} %param.29) | copy-start | bytes 3076
  6.6 60.7 %copy-start.11 = (f32[256]{0:T(256)S(1)}, f32[256]{0:T(256)}, u32[]{:S(2)}) copy-start(f32[256]{0:T(256)} %param.37) | copy-start | bytes 3076
  6.6 60.7 %copy-start.5 = (f32[512,4]{0,1:T(4,128)S(1)}, f32[512,4]{0,1:T(4,128)}, u32[]{:S(2)}) copy-start(f32[512,4]{0,1:T(4,128)} %param.35) | copy-start | bytes 24580
  6.6 61.3 %copy-start.6 = (f32[4,256]{1,0:T(4,128)S(1)}, f32[4,256]{1,0:T(4,128)}, u32[]{:S(2)}) copy-start(f32[4,256]{1,0:T(4,128)} %param.30) | copy-start | bytes 12292
  6.6 61.3 %copy-start.8 = (f32[4,64]{1,0:T(4,128)S(1)}, f32[4,64]{1,0:T(4,128)}, u32[]{:S(2)}) copy-start(f32[4,64]{1,0:T(4,128)} %param.31) | copy-start | bytes 3076
  6.6 119.2 %all-gather.3.cloned.1.call-start = ((), (), s32[]{:S(2)}) async-start(), calls=%async_computation.3 | async-start | bytes 4755456 | tf_op jit(solution)/shard_map/all_gather | solution.py:336
  51.3 41.5 %collective-permute-start.4 = (bf16[64,16,384]{2,1,0:T(8,128)(2,1)S(1)}, bf16[64,16,384]{2,1,0:T(8,128)(2,1)}, u32[]{:S(2)}, u32[]{:S(2)}) collective-permute-start(bf16[64,16,384]{2,1,0:T(8,128)(2,1)S(1)} %all_to_all.15.mine), channel_id=1, source_target_pairs={{0,4},{4,0},{1,5},{5,1},{2,6},{6,2},{3,7},{7,3},{8,12},{12,8},{9,1... | collective-permute-start | bytes 2359304 | tf_op jit(solution)/shard_map/ppermute | solution.py:340
  53.2 3.2 %collective-permute-start = (bf16[16,512]{1,0:T(8,128)(2,1)S(1)}, bf16[16,512]{1,0:T(8,128)(2,1)S(1)}, u32[]{:S(2)}, u32[]{:S(2)}) collective-permute-start(bf16[16,512]{1,0:T(8,128)(2,1)S(1)} %slice.3), channel_id=1, source_target_pairs={{0,4},{4,8},{8,12},{12,16},{16,20},{20,24},{24,28},{28,32},{32,36}... | collective-permute-start | bytes 49160 | tf_op jit(solution)/shard_map/ppermute | solution.py:342
  56.5 33.8 %copy-start.1 = (bf16[544,512]{1,0:T(8,128)(2,1)}, bf16[544,512]{1,0:T(8,128)(2,1)S(1)}, u32[]{:S(2)}) copy-start(bf16[544,512]{1,0:T(8,128)(2,1)S(1)} %pad_maximum_fusion.x0) | copy-start | bytes 1671172
  56.5 17.4 %collective-permute-start.1 = (bf16[544,512]{1,0:T(8,128)(2,1)S(1)}, bf16[544,512]{1,0:T(8,128)(2,1)S(1)}, u32[]{:S(2)}, u32[]{:S(2)}) collective-permute-start(bf16[544,512]{1,0:T(8,128)(2,1)S(1)} %pad_maximum_fusion.x0), channel_id=1, source_target_pairs={{0,1},{1,2},{2,3},{3,0},{4,5},{5,6},{6,7},{7,4},{8,9},{9,10},{10,1... | collective-permute-start | bytes 1671176 | tf_op jit(solution)/shard_map/ppermute | solution.py:348
  59.9 18.9 %collective-permute-start.2 = (bf16[544,512]{1,0:T(8,128)(2,1)S(1)}, bf16[544,512]{1,0:T(8,128)(2,1)S(1)}, u32[]{:S(2)}, u32[]{:S(2)}) collective-permute-start(bf16[544,512]{1,0:T(8,128)(2,1)S(1)} %pad_maximum_fusion.x0), channel_id=1, source_target_pairs={{0,2},{1,3},{2,0},{3,1},{4,6},{5,7},{6,4},{7,5},{8,10},{9,11},{10,... | collective-permute-start | bytes 1671176 | tf_op jit(solution)/shard_map/ppermute | solution.py:348
  62.9 27.4 %collective-permute-start.3 = (bf16[544,512]{1,0:T(8,128)(2,1)S(1)}, bf16[544,512]{1,0:T(8,128)(2,1)}, u32[]{:S(2)}, u32[]{:S(2)}) collective-permute-start(bf16[544,512]{1,0:T(8,128)(2,1)S(1)} %pad_maximum_fusion.x0), channel_id=1, source_target_pairs={{0,3},{1,0},{2,1},{3,2},{4,7},{5,4},{6,5},{7,6},{8,11},{9,8},{10,9... | collective-permute-start | bytes 1671176 | tf_op jit(solution)/shard_map/ppermute | solution.py:348
  73.9 5.0 %copy-start.3 = (bf16[544,512]{1,0:T(8,128)(2,1)}, bf16[544,512]{1,0:T(8,128)(2,1)S(1)}, u32[]{:S(2)}) copy-start(bf16[544,512]{1,0:T(8,128)(2,1)S(1)} %collective-permute-done.1.x1) | copy-start | bytes 1671172
  78.9 0.8 copy-start.4
  92.8 23.5 %copy-start = (bf16[4,528,512]{2,1,0:T(8,128)(2,1)}, bf16[4,528,512]{2,1,0:T(8,128)(2,1)S(1)}, u32[]{:S(2)}) copy-start(bf16[4,528,512]{2,1,0:T(8,128)(2,1)S(1)} %shard_map.190.normed) | copy-start | bytes 6488068
  117.9 18.4 %all-to-all-start.1 = ((bf16[8,80,256]{2,1,0:T(8,128)(2,1)}), bf16[8,80,256]{2,1,0:T(8,128)(2,1)S(1)}, u32[]{:S(2)}, u32[]{:S(2)}) async-start(bf16[8,80,256]{2,1,0:T(8,128)(2,1)} %broadcast_in_dim.52), calls=%async_computation.1 | async-start | bytes 655360 | tf_op jit(solution)/shard_map/all_to_all | solution.py:26
  139.1 9.6 %collective-permute-start.5 = (f32[8,512]{1,0:T(8,128)S(1)}, f32[8,512]{1,0:T(8,128)S(1)}, u32[]{:S(2)}, u32[]{:S(2)}) collective-permute-start(f32[8,512]{1,0:T(8,128)S(1)} %get-tuple-element.36.s0), channel_id=1, source_target_pairs={{0,1},{1,2},{2,3},{3,0},{4,5},{5,6},{6,7},{7,4},{8,9},{9,10},{10,1... | collective-permute-start | bytes 49160 | tf_op jit(solution)/shard_map/ppermute | solution.py:440
  141.9 7.2 %collective-permute-start.6 = (f32[8,512]{1,0:T(8,128)S(1)}, f32[8,512]{1,0:T(8,128)S(1)}, u32[]{:S(2)}, u32[]{:S(2)}) collective-permute-start(f32[8,512]{1,0:T(8,128)S(1)} %get-tuple-element.36.s0), channel_id=1, source_target_pairs={{0,2},{1,3},{2,0},{3,1},{4,6},{5,7},{6,4},{7,5},{8,10},{9,11},{10,... | collective-permute-start | bytes 49160 | tf_op jit(solution)/shard_map/ppermute | solution.py:440
  144.8 5.6 %collective-permute-start.7 = (f32[8,512]{1,0:T(8,128)S(1)}, f32[8,512]{1,0:T(8,128)S(1)}, u32[]{:S(2)}, u32[]{:S(2)}) collective-permute-start(f32[8,512]{1,0:T(8,128)S(1)} %get-tuple-element.36.s0), channel_id=1, source_target_pairs={{0,3},{1,0},{2,1},{3,2},{4,7},{5,4},{6,5},{7,6},{8,11},{9,8},{10,9... | collective-permute-start | bytes 49160 | tf_op jit(solution)/shard_map/ppermute | solution.py:440
Sparse Core Ops, SparseCore 0:
  10.6 95.6 all-gather.2

commit v7 on v6

--- a/solution.py
+++ b/solution.py
@@ -161,40 +161,36 @@
                 at = at + 1
 
 
-def second_kernel(
-    normed, weight, value, key, factors, scaled, params, mix_weight,
-    pool_out, gate_out, read_out, local_out,
-    rows_here, weight_here, read_here, arrived,
-):
-    length, span = pool_out.shape
+def block_products(normed, weight, rows_here, weight_here, arrived, lanes):
     place = lax.axis_index("tp")
     count, total_rows, width = rows_here.shape
     copies = []
     for k in range(count):
         start = pl.multiple_of(((place - k) & 3) * width, width)
         block = weight.at[pl.ds(start, width)]
-        copies.append(
-            [
-                pltpu.make_async_copy(normed.at[k], rows_here.at[k], arrived.at[k, 0]),
+        copies.append([pltpu.make_async_copy(normed.at[k], rows_here.at[k], arrived.at[k, 0])])
+        for n, (first, size) in enumerate(lanes):
+            copies[k].append(
                 pltpu.make_async_copy(
-                    block.at[:, : 2 * span], weight_here.at[k], arrived.at[k, 1]
-                ),
-                pltpu.make_async_copy(
-                    block.at[:, 4 * span :], read_here.at[k], arrived.at[k, 2]
-                ),
-            ]
-        )
+                    block.at[:, first : first + size], weight_here[n].at[k], arrived.at[k, n + 1]
+                )
+            )
         for copy in copies[k]:
             copy.start()
-    acc = jnp.zeros((total_rows, 2 * span), F32)
-    acc_read = jnp.zeros((total_rows, BLOCK), F32)
+    sums = [jnp.zeros((total_rows, size), F32) for _, size in lanes]
     for k in range(count):
         for copy in copies[k]:
             copy.wait()
-        acc = acc + dot(rows_here[k], weight_here[k])
-        acc_read = acc_read + dot(rows_here[k], read_here[k])
-    gate_out[...] = acc[HALO:, span:].astype(BF16)
-    running = acc[:, :span].astype(BF16).astype(F32)
+        for n in range(len(lanes)):
+            sums[n] = sums[n] + dot(rows_here[k], weight_here[n][k])
+    return sums
+
+
+def pool_kernel(normed, weight, params, mix_weight, pool_out, rows_here, weight_here, arrived):
+    length, span = pool_out.shape
+    place = lax.axis_index("tp")
+    acc = block_products(normed, weight, rows_here, [weight_here], arrived, [(0, span)])[0]
+    running = acc.astype(BF16).astype(F32)
     own = running[HALO:]
     chosen = own
     for level in range(POOL_GROUPS):
@@ -205,8 +201,24 @@
     counts = jnp.minimum(position, 2 << place).astype(F32)
     pooled = (chosen / counts - own).astype(BF16)
     pool_out[...] = (dot(pooled, mix_weight[...]) * params[25:26, :span]).astype(BF16)
+
+
+def second_kernel(
+    normed, weight, value, key, factors_far, scaled, params,
+    gate_out, read_out, local_out,
+    rows_here, gate_here, read_here, factors, arrived, factors_arrived,
+):
+    length, span = gate_out.shape
+    fetch = pltpu.make_async_copy(factors_far, factors, factors_arrived)
+    fetch.start()
+    lanes = [(span, span), (4 * span, BLOCK)]
+    acc, acc_read = block_products(
+        normed, weight, rows_here, [gate_here, read_here], arrived, lanes
+    )
+    gate_out[...] = acc[HALO:].astype(BF16)
     reads = convolved(acc_read.astype(BF16).astype(F32), params[4:8, :BLOCK], length)
     read_out[...] = reads
+    fetch.wait()
     at = 0
     for i in range(length // BLOCK):
         here = slice(i * BLOCK, (i + 1) * BLOCK)
@@ -236,14 +248,14 @@
     far = dot(reads[:, :HEAD].astype(F32), incoming, precision=HIGH) * decay
     gated = (local_in[...] + far) * silu(gate[...].astype(F32))
     ones = jnp.ones((8, gated.shape[1]), F32)
-    squares_out[...] = dot(ones, gated * gated, 1, 1, HIGH)
+    squares_out[...] = dot(ones, gated * gated, 1, 1, HIGH)[:1]
     rows_out[...] = (gated * params[26:27, : gated.shape[1]]).astype(BF16)
 
 
-def out_kernel(pool, rows, weight, s0, s1, s2, s3, out):
+def out_kernel(pool, rows, weight, squares, out):
     span = pool.shape[1]
-    mean = (s0[...] + s1[...] + s2[...] + s3[...]) / MIX_W
-    scale = jnp.transpose(lax.rsqrt(mean + EPSILON))[:, :1]
+    scale = lax.rsqrt(jnp.sum(squares[...], axis=0) / MIX_W + EPSILON)
+    scale = jnp.transpose(jnp.broadcast_to(scale, (8, scale.shape[1])))[:, :1]
     for d in range(out.shape[0]):
         width = out.shape[2]
         block = weight[d * width : (d + 1) * width]
@@ -256,7 +268,7 @@
     return pl.BlockSpec(shape, lambda *_: (0,) * len(shape))
 
 
-LIMITS = {"inner": 24, "norm": 16, "first": 16, "row": 6, "second": 24, "third": 10, "out": 16}
+LIMITS = {"pool": 16, "inner": 24, "norm": 16, "first": 16, "row": 6, "second": 24, "third": 10, "out": 16}
 
 
 def call(kernel, name, args, outs, flops, scratch=(), specs=None, far=()):
@@ -408,42 +420,54 @@
         far=range(3),
     )
     anywhere = pl.BlockSpec(memory_space=pl.ANY)
-    pool_out, gate, reads, inside = call(
+    gate, reads, inside = call(
         second_kernel,
         "second",
-        (normed, later_weights, value, key, factors, scaled, params, pool_mix[0]),
+        (normed, later_weights, value, key, factors, scaled, params),
         (
-            far_of((length, mix), BF16),
             far_of((length, mix), BF16),
             far_of((length, BLOCK), BF16),
             far_of((length, mix), F32),
         ),
-        2 * rows * D * (2 * mix + BLOCK),
+        2 * rows * D * (mix + BLOCK),
         [
             pltpu.VMEM((count, rows, width), BF16),
-            pltpu.VMEM((count, width, 2 * mix), BF16),
+            pltpu.VMEM((count, width, mix), BF16),
             pltpu.VMEM((count, width, BLOCK), BF16),
+            pltpu.VMEM(factors.shape, F32),
             pltpu.SemaphoreType.DMA((count, 3)),
+            pltpu.SemaphoreType.DMA,
+        ],
+        specs={0: anywhere, 1: anywhere, 4: anywhere},
+        far=range(7),
+    )
+    pool_out = call(
+        pool_kernel,
+        "pool",
+        (normed, later_weights, params, pool_mix[0]),
+        (far_of((length, mix), BF16),),
+        2 * rows * D * mix,
+        [
+            pltpu.VMEM((count, rows, width), BF16),
+            pltpu.VMEM((count, width, mix), BF16),
+            pltpu.SemaphoreType.DMA((count, 2)),
         ],
         specs={0: anywhere, 1: anywhere},
-        far=range(8),
-    )
+        far=range(4),
+    )[0]
     gated, squares = call(
         third_kernel,
         "third",
         (plane_pieces, before_row, logs_row, reads, inside, gate, cum, params),
-        (shape_of((length, mix), BF16), shape_of((8, length), F32)),
+        (shape_of((length, mix), BF16), shape_of((1, length), F32)),
         10**7,
         far=range(1, 8),
     )
-    all_squares = [squares] + [
-        lax.ppermute(squares, "tp", [(k, (k + shift) % count) for k in range(count)])
-        for shift in range(1, count)
-    ]
+    all_squares = sent_to_all(squares, "tp")
     terms = call(
         out_kernel,
         "out",
-        (pool_out, gated, later_weights, *all_squares),
+        (pool_out, gated, later_weights, all_squares),
         (shape_of((count, length, width), BF16),),
         2 * length * 2 * mix * D,
         specs={2: pl.BlockSpec((D, 2 * mix), lambda *_: (0, 1))},

time: 192 us -> 190 us (0.990)
  starting transfers between devices: 29 us -> 23.7 us
  Pallas kernels: 26.7 us -> 29.2 us
    ppermute x3 -> x0, starting transfers between devices: 9.54 us -> none  [local(): lax.ppermute(squares, 'tp', [(k, (k + shift) % count) for k in range(coun...]
    all_to_all x1 -> x2, starting transfers between devices: 4.59 us -> 8.85 us  [sent_to_all(): return lax.all_to_all(copies, axis, split_axis=0, concat_axis=0, tiled=True)]
    pallas_call x7 -> x8, Pallas kernels: 26.7 us -> 29.2 us  [call(): pl.pallas_call(kernel, grid=(1,), in_specs=[specs.get(k, whole(a.shape))...]
    all_to_all x1 -> x2, waiting for transfers between devices: 1.61 us -> 3.93 us  [sent_to_all(): return lax.all_to_all(copies, axis, split_axis=0, concat_axis=0, tiled=True)]
  transfers between devices with their start and end apart: 10 -> 8, of which waited for: 7 -> 5; matrix products, arithmetic and copies ran while one was open for 3% -> 3% of each run, Pallas kernels for 11% -> 12%
where the time goes in v7:
time: 190 us; the launch traced here: 189 us
  blocking collectives  88.5 us (47%)
  Pallas kernels  29.2 us (15%)
  waiting for transfers between devices  23.8 us (13%)
  starting transfers between devices  23.7 us (12%)
  between operations  13.7 us (7%)
  local copies, waits for them, and re-layouts  8.08 us (4%)
  other arithmetic  2.08 us (1%)
    all_to_all x1, blocking collectives, sent_to_all(): return lax.all_to_all(copies, axis, split_axis=0, concat_axis=0, tiled=True)  41.3 us
    pallas_call x8, Pallas kernels, call(): pl.pallas_call(kernel, grid=(1,), in_specs=[specs.get(k, whole(a.shape))...  29.2 us
    all_to_all x1, blocking collectives, local(): lax.all_to_all(terms, 'tp', split_axis=0, concat_axis=0, tiled=True)  29.1 us
    ppermute x3, waiting for transfers between devices, local(): pieces.append(lax.ppermute(sent, 'tp', pairs))  19 us
    all_gather x1, blocking collectives, local(): row_pieces = lax.all_gather(payload, ('sp_1', 'sp_2'))  18.1 us
    ppermute x3, starting transfers between devices, local(): pieces.append(lax.ppermute(sent, 'tp', pairs))  10.5 us
    all_to_all x2, starting transfers between devices, sent_to_all(): return lax.all_to_all(copies, axis, split_axis=0, concat_axis=0, tiled=True)  8.85 us
    all_to_all x2, waiting for transfers between devices, sent_to_all(): return lax.all_to_all(copies, axis, split_axis=0, concat_axis=0, tiled=True)  3.93 us
  transfers between devices with their start and end apart: 8, of which 5 were waited for; matrix products, arithmetic and copies ran while one was open for 3% of the time, Pallas kernels for 12%

profile of v7, /device:TPU:2, one launch (start us, length us, event | category | flops | bytes accessed | tf_op | source)
XLA Modules:
  0.0 189.0 jit_solution(555528731562736387)
XLA Ops:
  6.6 0.0 all-gather.3.cloned.1.call-start
  6.7 1.6 concatenate.16
  8.2 0.0 all-gather.3.cloned.1.call-update
  8.2 0.8 copy.21
  9.0 0.1 pad.40.clone
  9.1 0.8 maximum_maximum_fusion
  9.9 0.1 broadcast_in_dim.54
  10.0 41.3 %all_to_all.20.mine = bf16[64,16,384]{2,1,0:T(8,128)(2,1)S(1)} all-to-all(bf16[64,16,384]{2,1,0:T(8,128)(2,1)S(1)} %broadcast_in_dim.54), channel_id=1, replica_groups=mesh['sp_0'=8,'sp_1'=8,'sp_2'=2,'tp'=4] {'sp_0','sp_1'}, dimensions={0} | all-to-all | bytes 1572864 | tf_op jit(solution)/shard_map/all_to_all | solution.py:26
  51.3 1.9 %collective-permute-start.4 = (bf16[64,16,384]{2,1,0:T(8,128)(2,1)S(1)}, bf16[64,16,384]{2,1,0:T(8,128)(2,1)}, u32[]{:S(2)}, u32[]{:S(2)}) collective-permute-start(bf16[64,16,384]{2,1,0:T(8,128)(2,1)S(1)} %all_to_all.20.mine), channel_id=1, source_target_pairs={{0,4},{4,0},{1,5},{5,1},{2,6},{6,2},{3,7},{7,3},{8,12},{12,8},{9,1... | collective-permute-start | bytes 2359304 | tf_op jit(solution)/shard_map/ppermute | solution.py:352
  53.2 2.4 %collective-permute-start = (bf16[16,512]{1,0:T(8,128)(2,1)S(1)}, bf16[16,512]{1,0:T(8,128)(2,1)S(1)}, u32[]{:S(2)}, u32[]{:S(2)}) collective-permute-start(bf16[16,512]{1,0:T(8,128)(2,1)S(1)} %slice.3), channel_id=1, source_target_pairs={{0,4},{4,8},{8,12},{12,16},{16,20},{20,24},{24,28},{28,32},{32,36}... | collective-permute-start | bytes 49160 | tf_op jit(solution)/shard_map/ppermute | solution.py:354
  55.6 0.8 collective-permute-done
  56.5 0.0 copy-start.1
  56.5 3.4 %collective-permute-start.1 = (bf16[544,512]{1,0:T(8,128)(2,1)S(1)}, bf16[544,512]{1,0:T(8,128)(2,1)S(1)}, u32[]{:S(2)}, u32[]{:S(2)}) collective-permute-start(bf16[544,512]{1,0:T(8,128)(2,1)S(1)} %pad_maximum_fusion.x0), channel_id=1, source_target_pairs={{0,1},{1,2},{2,3},{3,0},{4,5},{5,6},{6,7},{7,4},{8,9},{9,10},{10,1... | collective-permute-start | bytes 1671176 | tf_op jit(solution)/shard_map/ppermute | solution.py:360
  59.9 3.0 %collective-permute-start.2 = (bf16[544,512]{1,0:T(8,128)(2,1)S(1)}, bf16[544,512]{1,0:T(8,128)(2,1)S(1)}, u32[]{:S(2)}, u32[]{:S(2)}) collective-permute-start(bf16[544,512]{1,0:T(8,128)(2,1)S(1)} %pad_maximum_fusion.x0), channel_id=1, source_target_pairs={{0,2},{1,3},{2,0},{3,1},{4,6},{5,7},{6,4},{7,5},{8,10},{9,11},{10,... | collective-permute-start | bytes 1671176 | tf_op jit(solution)/shard_map/ppermute | solution.py:360
  62.9 4.1 %collective-permute-start.3 = (bf16[544,512]{1,0:T(8,128)(2,1)S(1)}, bf16[544,512]{1,0:T(8,128)(2,1)}, u32[]{:S(2)}, u32[]{:S(2)}) collective-permute-start(bf16[544,512]{1,0:T(8,128)(2,1)S(1)} %pad_maximum_fusion.x0), channel_id=1, source_target_pairs={{0,3},{1,0},{2,1},{3,2},{4,7},{5,4},{6,5},{7,6},{8,11},{9,8},{10,9... | collective-permute-start | bytes 1671176 | tf_op jit(solution)/shard_map/ppermute | solution.py:360
  67.0 0.0 copy-done.13
  67.1 0.0 copy-done.7
  67.1 0.0 copy-done.12
  67.1 0.1 broadcast_in_dim.49
  67.2 0.1 broadcast_in_dim_reshape.3
  67.3 0.6 pad.36.extra
  67.9 0.0 copy-done.6
  67.9 0.1 broadcast_in_dim.48
  68.0 0.1 broadcast_in_dim.47
  68.1 2.4 %concatenate.18.params = f32[32,384]{1,0:T(8,128)} concatenate(f32[4,384]{1,0:T(4,128)S(1)} %select_maximum_fusion, f32[4,384]{1,0:T(4,128)S(1)} %pad.30, f32[8,384]{1,0:T(8,128)S(1)} %broadcast_in_dim.47, f32[8,384]{1,0:T(8,128)S(1)} %broadcast_in_dim.48, f32[1,384]{1,0:T(1,128)S(1)} %pad.33, f32[1,384]{1,0:T(1,128)S(1)} %pad.34, f32[1,384]{1,0:T(1,128)S(1)} %pad.35, ...), dimensions={0} | concatenate | bytes 98304 | tf_op jit(solution)/shard_map/concatenate | solution.py:371
  70.5 3.4 %collective-permute-done.1.x1 = bf16[544,512]{1,0:T(8,128)(2,1)S(1)} collective-permute-done((bf16[544,512]{1,0:T(8,128)(2,1)S(1)}, bf16[544,512]{1,0:T(8,128)(2,1)S(1)}, u32[]{:S(2)}, u32[]{:S(2)}) %collective-permute-start.1) | collective-permute-done | bytes 557088 | tf_op jit(solution)/shard_map/ppermute | solution.py:360
  73.9 5.0 %collective-permute-done.2.x2 = bf16[544,512]{1,0:T(8,128)(2,1)S(1)} collective-permute-done((bf16[544,512]{1,0:T(8,128)(2,1)S(1)}, bf16[544,512]{1,0:T(8,128)(2,1)S(1)}, u32[]{:S(2)}, u32[]{:S(2)}) %collective-permute-start.2) | collective-permute-done | bytes 557088 | tf_op jit(solution)/shard_map/ppermute | solution.py:360
  78.9 0.0 copy-done.3
  78.9 0.8 copy-done.4
  79.7 10.6 %collective-permute-done.3.x3 = bf16[544,512]{1,0:T(8,128)(2,1)} collective-permute-done((bf16[544,512]{1,0:T(8,128)(2,1)S(1)}, bf16[544,512]{1,0:T(8,128)(2,1)}, u32[]{:S(2)}, u32[]{:S(2)}) %collective-permute-start.3) | collective-permute-done | bytes 557088 | tf_op jit(solution)/shard_map/ppermute | solution.py:360
  90.3 2.5 %shard_map.190.normed = bf16[4,528,512]{2,1,0:T(8,128)(2,1)S(1)} custom-call(bf16[544,512]{1,0:T(8,128)(2,1)} %copy-done.1, bf16[544,512]{1,0:T(8,128)(2,1)} %copy-done.3, bf16[544,512]{1,0:T(8,128)(2,1)} %copy-done.4, bf16[544,512]{1,0:T(8,128)(2,1)} %collective-permute-done.3.x3), custom_call_target="tpu_custom_call" | custom-call | flops 1000000 | bytes 2228224 | tf_op jit(solution)/shard_map/pallas_call | solution.py:281
  92.8 0.0 collective-permute-done.4.other
  92.9 5.4 %shard_map.192 = (bf16[512,256]{1,0:T(8,128)(2,1)}, bf16[512,128]{1,0:T(8,128)(2,1)}, f32[8,512]{1,0:T(8,128)}, f32[8,512]{1,0:T(8,128)}, bf16[80,256]{1,0:T(8,128)(2,1)S(1)}) custom-call(bf16[4,528,512]{2,1,0:T(8,128)(2,1)S(1)} %shard_map.190.normed, bf16[64,16,384]{2,1,0:T(8,128)(2,1)S(1)} %all_to_all.20.mine, ...), custom_call_target="tpu_custom_call" | custom-call | flops 830472192 | bytes 3801088 | tf_op jit(solution)/shard_map/pallas_call | solution.py:281
  98.3 18.1 %all-gather = bf16[1280,256]{1,0:T(8,128)(2,1)S(1)} all-gather(bf16[80,256]{1,0:T(8,128)(2,1)S(1)} %get-tuple-element.20), channel_id=2, replica_groups=mesh['sp_0'=8,'sp_1'=8,'sp_2'=2,'tp'=4] {'sp_1','sp_2'}, dimensions={0}, use_global_device_ids=true | all-gather | bytes 696320 | tf_op jit(solution)/shard_map/all_gather | solution.py:401
  116.3 0.8 shard_map.193
  117.1 0.7 broadcast_in_dim.55
  117.9 4.6 %all-to-all-start.1 = ((bf16[8,80,256]{2,1,0:T(8,128)(2,1)}), bf16[8,80,256]{2,1,0:T(8,128)(2,1)S(1)}, u32[]{:S(2)}, u32[]{:S(2)}) async-start(bf16[8,80,256]{2,1,0:T(8,128)(2,1)} %broadcast_in_dim.55), calls=%async_computation.1 | async-start | bytes 655360 | tf_op jit(solution)/shard_map/all_to_all | solution.py:26
  122.5 3.3 %shard_map.194 = (f32[40,128,128]{2,1,0:T(8,128)}, bf16[512,256]{1,0:T(8,128)(2,1)}) custom-call(bf16[512,256]{1,0:T(8,128)(2,1)} %get-tuple-element.24.value, f32[8,512]{1,0:T(8,128)} %get-tuple-element.26.cum, f32[8,512]{1,0:T(8,128)} %get-tuple-element.27.step), custom_call_target="tpu_custom_call" | custom-call | flops 10000000 | bytes 294912 | tf_op jit(solution)/shard_map/pallas_call | solution.py:281
  125.8 6.6 %shard_map.195 = (bf16[512,256]{1,0:T(8,128)(2,1)}, bf16[512,128]{1,0:T(8,128)(2,1)}, f32[512,256]{1,0:T(8,128)}) custom-call(bf16[4,528,512]{2,1,0:T(8,128)(2,1)} %copy-done, bf16[2048,1152]{1,0:T(8,128)(2,1)} %all-gather.3.cloned.1.call-done.weight, bf16[512,256]{1,0:T(8,128)(2,1)} %get-tuple-element.24.value, bf16[512,128]{1,0:T(8,128)(2,1)} %get-tuple-element.25.key, ...), custom_call_target="tpu_custom_call" | custom-call | flops 830472192 | bytes 10207232 | tf_op jit(solution)/shard_map/pallas_call | solution.py:281
  132.4 3.9 %all-to-all-done.1.planes = bf16[8,80,256]{2,1,0:T(8,128)(2,1)S(1)} async-done(((bf16[8,80,256]{2,1,0:T(8,128)(2,1)}), bf16[8,80,256]{2,1,0:T(8,128)(2,1)S(1)}, u32[]{:S(2)}, u32[]{:S(2)}) %all-to-all-start.1) | async-done | bytes 327712 | tf_op jit(solution)/shard_map/all_to_all | solution.py:26
  136.3 2.8 %shard_map.196 = (bf16[512,256]{1,0:T(8,128)(2,1)S(1)}, f32[1,512]{1,0:T(1,128)S(1)}) custom-call(bf16[8,80,256]{2,1,0:T(8,128)(2,1)S(1)} %all-to-all-done.1.planes, f32[64,256]{1,0:T(8,128)} %get-tuple-element.22.before, f32[8,256]{1,0:T(8,128)} %get-tuple-element.23.logs_before, bf16[512,128]{1,0:T(8,128)(2,1)} %get-tuple-element.30.reads, ...), custom_call_target="tpu_custom_call" | custom-call | flops 10000000 | bytes 1384448 | tf_op jit(solution)/shard_map/pallas_call | solution.py:281
  139.1 0.6 broadcast_in_dim.56
  139.7 4.2 %all-to-all-start.2 = ((f32[4,1,512]{2,1,0:T(1,128)}), f32[4,1,512]{2,1,0:T(1,128)S(1)}, u32[]{:S(2)}, u32[]{:S(2)}) async-start(f32[4,1,512]{2,1,0:T(1,128)} %broadcast_in_dim.56), calls=%async_computation.2 | async-start | bytes 16384 | tf_op jit(solution)/shard_map/all_to_all | solution.py:26
  144.0 4.9 %shard_map.191.pool = bf16[512,256]{1,0:T(8,128)(2,1)} custom-call(bf16[4,528,512]{2,1,0:T(8,128)(2,1)} %copy-done, bf16[2048,1152]{1,0:T(8,128)(2,1)} %all-gather.3.cloned.1.call-done.weight, f32[32,384]{1,0:T(8,128)} %concatenate.18.params, bf16[256,256]{1,0:T(8,128)(2,1)} %bitcast.10), custom_call_target="tpu_custom_call" | custom-call | flops 553648128 | bytes 7061504 | tf_op jit(solution)/shard_map/pallas_call | solution.py:281
  148.8 0.0 all-to-all-done.2.squares
  148.8 3.0 %shard_map.197 = bf16[4,512,512]{2,1,0:T(8,128)(2,1)S(1)} custom-call(bf16[512,256]{1,0:T(8,128)(2,1)} %shard_map.191.pool, bf16[512,256]{1,0:T(8,128)(2,1)S(1)} %get-tuple-element.33.rows, bf16[2048,1152]{1,0:T(8,128)(2,1)} %all-gather.3.cloned.1.call-done.weight, f32[4,1,512]{2,1,0:T(1,128)S(1)} %all-to-all-done.2.squares), custom_call_target="tpu_custom_call" | custom-call | flops 1073741824 | bytes 5251072 | tf_op jit(solution)/shard_map/pallas_call | solution.py:281
  151.9 29.1 %all_to_all.21 = bf16[4,512,512]{2,1,0:T(8,128)(2,1)S(1)} all-to-all(bf16[4,512,512]{2,1,0:T(8,128)(2,1)S(1)} %shard_map.197), channel_id=1, replica_groups=mesh['sp_0'=8,'sp_1'=8,'sp_2'=2,'tp'=4] {'tp'}, dimensions={0} | all-to-all | bytes 4194304 | tf_op jit(solution)/shard_map/all_to_all | solution.py:476
  181.0 1.2 reduce_sum.12
  (38 shorter events, 0.1 us)
Async XLA Ops:
  6.5 46.7 %copy-start.2 = (bf16[512,512]{1,0:T(8,128)(2,1)S(1)}, bf16[512,512]{1,0:T(8,128)(2,1)}, u32[]{:S(2)}) copy-start(bf16[512,512]{1,0:T(8,128)(2,1)} %param.20) | copy-start | bytes 1572868
  6.5 49.9 %copy-start.9 = (bf16[512]{0:T(512)(128)(2,1)S(1)}, bf16[512]{0:T(512)(128)(2,1)}, u32[]{:S(2)}) copy-start(bf16[512]{0:T(512)(128)(2,1)} %param.21) | copy-start | bytes 3076
  6.5 60.5 %copy-start.13 = (f32[4]{0:T(128)S(1)}, f32[4]{0:T(128)}, u32[]{:S(2)}) copy-start(f32[4]{0:T(128)} %param.34) | copy-start | bytes 52
  6.5 60.5 %copy-start.14 = (f32[4]{0:T(128)S(1)}, f32[4]{0:T(128)}, u32[]{:S(2)}) copy-start(f32[4]{0:T(128)} %param.33) | copy-start | bytes 52
  6.5 60.5 %copy-start.7 = (f32[4,64]{1,0:T(4,128)S(1)}, f32[4,64]{1,0:T(4,128)}, u32[]{:S(2)}) copy-start(f32[4,64]{1,0:T(4,128)} %param.32) | copy-start | bytes 3076
  6.5 60.6 %copy-start.12 = (f32[4]{0:T(128)S(1)}, f32[4]{0:T(128)}, u32[]{:S(2)}) copy-start(f32[4]{0:T(128)} %param.36) | copy-start | bytes 52
  6.6 60.7 %copy-start.10 = (f32[256]{0:T(256)S(1)}, f32[256]{0:T(256)}, u32[]{:S(2)}) copy-start(f32[256]{0:T(256)} %param.29) | copy-start | bytes 3076
  6.6 60.7 %copy-start.11 = (f32[256]{0:T(256)S(1)}, f32[256]{0:T(256)}, u32[]{:S(2)}) copy-start(f32[256]{0:T(256)} %param.37) | copy-start | bytes 3076
  6.6 60.7 %copy-start.5 = (f32[512,4]{0,1:T(4,128)S(1)}, f32[512,4]{0,1:T(4,128)}, u32[]{:S(2)}) copy-start(f32[512,4]{0,1:T(4,128)} %param.35) | copy-start | bytes 24580
  6.6 61.3 %copy-start.6 = (f32[4,256]{1,0:T(4,128)S(1)}, f32[4,256]{1,0:T(4,128)}, u32[]{:S(2)}) copy-start(f32[4,256]{1,0:T(4,128)} %param.30) | copy-start | bytes 12292
  6.6 61.3 %copy-start.8 = (f32[4,64]{1,0:T(4,128)S(1)}, f32[4,64]{1,0:T(4,128)}, u32[]{:S(2)}) copy-start(f32[4,64]{1,0:T(4,128)} %param.31) | copy-start | bytes 3076
  6.6 119.2 %all-gather.3.cloned.1.call-start = ((), (), s32[]{:S(2)}) async-start(), calls=%async_computation.4 | async-start | bytes 4755456 | tf_op jit(solution)/shard_map/all_gather | solution.py:348
  51.3 41.5 %collective-permute-start.4 = (bf16[64,16,384]{2,1,0:T(8,128)(2,1)S(1)}, bf16[64,16,384]{2,1,0:T(8,128)(2,1)}, u32[]{:S(2)}, u32[]{:S(2)}) collective-permute-start(bf16[64,16,384]{2,1,0:T(8,128)(2,1)S(1)} %all_to_all.20.mine), channel_id=1, source_target_pairs={{0,4},{4,0},{1,5},{5,1},{2,6},{6,2},{3,7},{7,3},{8,12},{12,8},{9,1... | collective-permute-start | bytes 2359304 | tf_op jit(solution)/shard_map/ppermute | solution.py:352
  53.2 3.2 %collective-permute-start = (bf16[16,512]{1,0:T(8,128)(2,1)S(1)}, bf16[16,512]{1,0:T(8,128)(2,1)S(1)}, u32[]{:S(2)}, u32[]{:S(2)}) collective-permute-start(bf16[16,512]{1,0:T(8,128)(2,1)S(1)} %slice.3), channel_id=1, source_target_pairs={{0,4},{4,8},{8,12},{12,16},{16,20},{20,24},{24,28},{28,32},{32,36}... | collective-permute-start | bytes 49160 | tf_op jit(solution)/shard_map/ppermute | solution.py:354
  56.5 33.8 %copy-start.1 = (bf16[544,512]{1,0:T(8,128)(2,1)}, bf16[544,512]{1,0:T(8,128)(2,1)S(1)}, u32[]{:S(2)}) copy-start(bf16[544,512]{1,0:T(8,128)(2,1)S(1)} %pad_maximum_fusion.x0) | copy-start | bytes 1671172
  56.5 17.4 %collective-permute-start.1 = (bf16[544,512]{1,0:T(8,128)(2,1)S(1)}, bf16[544,512]{1,0:T(8,128)(2,1)S(1)}, u32[]{:S(2)}, u32[]{:S(2)}) collective-permute-start(bf16[544,512]{1,0:T(8,128)(2,1)S(1)} %pad_maximum_fusion.x0), channel_id=1, source_target_pairs={{0,1},{1,2},{2,3},{3,0},{4,5},{5,6},{6,7},{7,4},{8,9},{9,10},{10,1... | collective-permute-start | bytes 1671176 | tf_op jit(solution)/shard_map/ppermute | solution.py:360
  59.9 18.9 %collective-permute-start.2 = (bf16[544,512]{1,0:T(8,128)(2,1)S(1)}, bf16[544,512]{1,0:T(8,128)(2,1)S(1)}, u32[]{:S(2)}, u32[]{:S(2)}) collective-permute-start(bf16[544,512]{1,0:T(8,128)(2,1)S(1)} %pad_maximum_fusion.x0), channel_id=1, source_target_pairs={{0,2},{1,3},{2,0},{3,1},{4,6},{5,7},{6,4},{7,5},{8,10},{9,11},{10,... | collective-permute-start | bytes 1671176 | tf_op jit(solution)/shard_map/ppermute | solution.py:360
  62.9 27.4 %collective-permute-start.3 = (bf16[544,512]{1,0:T(8,128)(2,1)S(1)}, bf16[544,512]{1,0:T(8,128)(2,1)}, u32[]{:S(2)}, u32[]{:S(2)}) collective-permute-start(bf16[544,512]{1,0:T(8,128)(2,1)S(1)} %pad_maximum_fusion.x0), channel_id=1, source_target_pairs={{0,3},{1,0},{2,1},{3,2},{4,7},{5,4},{6,5},{7,6},{8,11},{9,8},{10,9... | collective-permute-start | bytes 1671176 | tf_op jit(solution)/shard_map/ppermute | solution.py:360
  73.9 5.0 %copy-start.3 = (bf16[544,512]{1,0:T(8,128)(2,1)}, bf16[544,512]{1,0:T(8,128)(2,1)S(1)}, u32[]{:S(2)}) copy-start(bf16[544,512]{1,0:T(8,128)(2,1)S(1)} %collective-permute-done.1.x1) | copy-start | bytes 1671172
  78.9 0.8 copy-start.4
  92.8 23.5 %copy-start = (bf16[4,528,512]{2,1,0:T(8,128)(2,1)}, bf16[4,528,512]{2,1,0:T(8,128)(2,1)S(1)}, u32[]{:S(2)}) copy-start(bf16[4,528,512]{2,1,0:T(8,128)(2,1)S(1)} %shard_map.190.normed) | copy-start | bytes 6488068
  117.9 18.4 %all-to-all-start.1 = ((bf16[8,80,256]{2,1,0:T(8,128)(2,1)}), bf16[8,80,256]{2,1,0:T(8,128)(2,1)S(1)}, u32[]{:S(2)}, u32[]{:S(2)}) async-start(bf16[8,80,256]{2,1,0:T(8,128)(2,1)} %broadcast_in_dim.55), calls=%async_computation.1 | async-start | bytes 655360 | tf_op jit(solution)/shard_map/all_to_all | solution.py:26
  139.7 9.1 %all-to-all-start.2 = ((f32[4,1,512]{2,1,0:T(1,128)}), f32[4,1,512]{2,1,0:T(1,128)S(1)}, u32[]{:S(2)}, u32[]{:S(2)}) async-start(f32[4,1,512]{2,1,0:T(1,128)} %broadcast_in_dim.56), calls=%async_computation.2 | async-start | bytes 16384 | tf_op jit(solution)/shard_map/all_to_all | solution.py:26
Sparse Core Ops, SparseCore 0:
  10.6 95.6 all-gather.2

commit v8 on v7

--- a/solution.py
+++ b/solution.py
@@ -204,20 +204,24 @@
 
 
 def second_kernel(
-    normed, weight, value, key, factors_far, scaled, params,
-    gate_out, read_out, local_out,
+    normed, weight, value, key, factors_far, scaled, params, planes, before, logs_before, cum,
+    rows_out, squares_out,
     rows_here, gate_here, read_here, factors, arrived, factors_arrived,
 ):
-    length, span = gate_out.shape
+    length, span = rows_out.shape
     fetch = pltpu.make_async_copy(factors_far, factors, factors_arrived)
     fetch.start()
     lanes = [(span, span), (4 * span, BLOCK)]
     acc, acc_read = block_products(
         normed, weight, rows_here, [gate_here, read_here], arrived, lanes
     )
-    gate_out[...] = acc[HALO:].astype(BF16)
+    gate = silu(acc[HALO:].astype(BF16).astype(F32))
     reads = convolved(acc_read.astype(BF16).astype(F32), params[4:8, :BLOCK], length)
-    read_out[...] = reads
+    _, _, earlier, _ = scan_payloads(planes, lax.axis_index("sp_0"))
+    incoming = earlier * jnp.exp(logs_before[:1]) + before[...]
+    decay = dot(jnp.exp(cum[...]), heads_of_lanes(span), 0, 0, HIGH)
+    far = dot(reads[:, :HEAD].astype(F32), incoming, precision=HIGH) * decay
+    ones = jnp.ones((8, span), F32)
     fetch.wait()
     at = 0
     for i in range(length // BLOCK):
@@ -233,34 +237,31 @@
                 at = at + 1
             left = jnp.concatenate(parts, axis=1)
             results.append(dot(left, scaled[: (i + 1) * BLOCK, h * HEAD : (h + 1) * HEAD]))
-        local_out[here] = jnp.concatenate(results, axis=1) + params[24:25, :span] * value[
-            here
-        ].astype(F32)
-
-
-def third_kernel(
-    planes, before, logs_before, reads, local_in, gate, cum, params, rows_out, squares_out
-):
-    _, _, earlier, _ = scan_payloads(planes, lax.axis_index("sp_0"))
-    incoming = earlier * jnp.exp(logs_before[:1]) + before[...]
-    lanes = heads_of_lanes(local_in.shape[1])
-    decay = dot(jnp.exp(cum[...]), lanes, 0, 0, HIGH)
-    far = dot(reads[:, :HEAD].astype(F32), incoming, precision=HIGH) * decay
-    gated = (local_in[...] + far) * silu(gate[...].astype(F32))
-    ones = jnp.ones((8, gated.shape[1]), F32)
-    squares_out[...] = dot(ones, gated * gated, 1, 1, HIGH)[:1]
-    rows_out[...] = (gated * params[26:27, : gated.shape[1]]).astype(BF16)
-
-
-def out_kernel(pool, rows, weight, squares, out):
+        near = jnp.concatenate(results, axis=1) + params[24:25, :span] * value[here].astype(F32)
+        gated = (near + far[here]) * gate[here]
+        squares_out[:, here] = dot(ones, gated * gated, 1, 1, HIGH)[:1]
+        rows_out[here] = (gated * params[26:27, :span]).astype(BF16)
+
+
+def out_kernel(pool, rows, weight, squares, out, weight_here, arrived):
     span = pool.shape[1]
+    count, _, width = out.shape
+    copies = [
+        pltpu.make_async_copy(
+            weight.at[pl.ds(d * width, width), pl.ds(2 * span, 2 * span)],
+            weight_here.at[d],
+            arrived.at[d],
+        )
+        for d in range(count)
+    ]
+    for copy in copies:
+        copy.start()
     scale = lax.rsqrt(jnp.sum(squares[...], axis=0) / MIX_W + EPSILON)
     scale = jnp.transpose(jnp.broadcast_to(scale, (8, scale.shape[1])))[:, :1]
-    for d in range(out.shape[0]):
-        width = out.shape[2]
-        block = weight[d * width : (d + 1) * width]
-        terms = dot(pool[...], block[:, :span], 1, 1)
-        terms = terms + dot(rows[...], block[:, span:], 1, 1) * scale
+    for d in range(count):
+        copies[d].wait()
+        terms = dot(pool[...], weight_here[d, :, :span], 1, 1)
+        terms = terms + dot(rows[...], weight_here[d, :, span:], 1, 1) * scale
         out[d] = terms.astype(BF16)
 
 
@@ -268,7 +269,7 @@
     return pl.BlockSpec(shape, lambda *_: (0,) * len(shape))
 
 
-LIMITS = {"pool": 16, "inner": 24, "norm": 16, "first": 16, "row": 6, "second": 24, "third": 10, "out": 16}
+LIMITS = {"pool": 16, "inner": 24, "norm": 16, "first": 16, "row": 6, "second": 28, "out": 16}
 
 
 def call(kernel, name, args, outs, flops, scratch=(), specs=None, far=()):
@@ -420,15 +421,14 @@
         far=range(3),
     )
     anywhere = pl.BlockSpec(memory_space=pl.ANY)
-    gate, reads, inside = call(
+    gated, squares = call(
         second_kernel,
         "second",
-        (normed, later_weights, value, key, factors, scaled, params),
         (
-            far_of((length, mix), BF16),
-            far_of((length, BLOCK), BF16),
-            far_of((length, mix), F32),
+            normed, later_weights, value, key, factors, scaled, params,
+            plane_pieces, before_row, logs_row, cum,
         ),
+        (shape_of((length, mix), BF16), shape_of((1, length), F32)),
         2 * rows * D * (mix + BLOCK),
         [
             pltpu.VMEM((count, rows, width), BF16),
@@ -439,7 +439,7 @@
             pltpu.SemaphoreType.DMA,
         ],
         specs={0: anywhere, 1: anywhere, 4: anywhere},
-        far=range(7),
+        far=(0, 1, 2, 3, 4, 5, 6, 8, 9, 10),
     )
     pool_out = call(
         pool_kernel,
@@ -455,14 +455,6 @@
         specs={0: anywhere, 1: anywhere},
         far=range(4),
     )[0]
-    gated, squares = call(
-        third_kernel,
-        "third",
-        (plane_pieces, before_row, logs_row, reads, inside, gate, cum, params),
-        (shape_of((length, mix), BF16), shape_of((1, length), F32)),
-        10**7,
-        far=range(1, 8),
-    )
     all_squares = sent_to_all(squares, "tp")
     terms = call(
         out_kernel,
@@ -470,7 +462,11 @@
         (pool_out, gated, later_weights, all_squares),
         (shape_of((count, length, width), BF16),),
         2 * length * 2 * mix * D,
-        specs={2: pl.BlockSpec((D, 2 * mix), lambda *_: (0, 1))},
+        [
+            pltpu.VMEM((count, width, 2 * mix), BF16),
+            pltpu.SemaphoreType.DMA((count,)),
+        ],
+        specs={2: anywhere},
         far=(0, 2),
     )[0]
     arrived = lax.all_to_all(terms, "tp", split_axis=0, concat_axis=0, tiled=True)

time: 190 us -> 195 us (1.026)
  waiting for transfers between devices: 23.8 us -> 30.4 us
    all_to_all x2, waiting for transfers between devices: 3.93 us -> 10.5 us  [sent_to_all(): return lax.all_to_all(copies, axis, split_axis=0, concat_axis=0, tiled=True)]
    pallas_call x8 -> x7, Pallas kernels: 29.2 us -> 28.3 us  [call(): pl.pallas_call(kernel, grid=(1,), in_specs=[specs.get(k, whole(a.shape))...]
  transfers between devices with their start and end apart: 8 -> 8, of which waited for: 5 -> 5; matrix products, arithmetic and copies ran while one was open for 3% -> 3% of each run, Pallas kernels for 12% -> 9%
where the time goes in v8:
time: 195 us
  blocking collectives  88.5 us (45%)
  waiting for transfers between devices  30.4 us (16%)
  Pallas kernels  28.3 us (15%)
  starting transfers between devices  23.6 us (12%)
  between operations  13.7 us (7%)
  local copies, waits for them, and re-layouts  8.06 us (4%)
  other arithmetic  2.08 us (1%)
    all_to_all x1, blocking collectives, sent_to_all(): return lax.all_to_all(copies, axis, split_axis=0, concat_axis=0, tiled=True)  41.3 us
    all_to_all x1, blocking collectives, local(): lax.all_to_all(terms, 'tp', split_axis=0, concat_axis=0, tiled=True)  29.1 us
    pallas_call x7, Pallas kernels, call(): pl.pallas_call(kernel, grid=(1,), in_specs=[specs.get(k, whole(a.shape))...  28.3 us
    ppermute x3, waiting for transfers between devices, local(): pieces.append(lax.ppermute(sent, 'tp', pairs))  19 us
    all_gather x1, blocking collectives, local(): row_pieces = lax.all_gather(payload, ('sp_1', 'sp_2'))  18 us
    all_to_all x2, waiting for transfers between devices, sent_to_all(): return lax.all_to_all(copies, axis, split_axis=0, concat_axis=0, tiled=True)  10.5 us
    ppermute x3, starting transfers between devices, local(): pieces.append(lax.ppermute(sent, 'tp', pairs))  10.5 us
    all_to_all x2, starting transfers between devices, sent_to_all(): return lax.all_to_all(copies, axis, split_axis=0, concat_axis=0, tiled=True)  8.84 us
  transfers between devices with their start and end apart: 8, of which 5 were waited for; matrix products, arithmetic and copies ran while one was open for 3% of the time, Pallas kernels for 9%

profile of v8, /device:TPU:2, one launch (start us, length us, event | category | flops | bytes accessed | tf_op | source)
XLA Modules:
  0.0 194.7 jit_solution(8059143980353371413)
XLA Ops:
  6.5 0.0 copy-start.12
  6.6 0.0 copy-start.10
  6.6 0.0 all-gather.3.cloned.1.call-start
  6.7 1.6 concatenate.16
  8.2 0.0 all-gather.3.cloned.1.call-update
  8.2 0.8 copy.21
  9.0 0.1 pad.40.clone
  9.1 0.8 maximum_maximum_fusion
  9.9 0.1 broadcast_in_dim.54
  10.0 41.3 %all_to_all.20.mine = bf16[64,16,384]{2,1,0:T(8,128)(2,1)S(1)} all-to-all(bf16[64,16,384]{2,1,0:T(8,128)(2,1)S(1)} %broadcast_in_dim.54), channel_id=1, replica_groups=mesh['sp_0'=8,'sp_1'=8,'sp_2'=2,'tp'=4] {'sp_0','sp_1'}, dimensions={0} | all-to-all | bytes 1572864 | tf_op jit(solution)/shard_map/all_to_all | solution.py:26
  51.3 1.9 collective-permute-start.4
  53.2 0.0 copy-done.2
  53.2 2.4 %collective-permute-start = (bf16[16,512]{1,0:T(8,128)(2,1)S(1)}, bf16[16,512]{1,0:T(8,128)(2,1)S(1)}, u32[]{:S(2)}, u32[]{:S(2)}) collective-permute-start(bf16[16,512]{1,0:T(8,128)(2,1)S(1)} %slice.3), channel_id=1, source_target_pairs={{0,4},{4,8},{8,12},{12,16},{16,20},{20,24},{24,28},{28,32},{32,36}... | collective-permute-start | bytes 49160 | tf_op jit(solution)/shard_map/ppermute | solution.py:355
  55.6 0.8 collective-permute-done
  56.5 3.4 %collective-permute-start.1 = (bf16[544,512]{1,0:T(8,128)(2,1)S(1)}, bf16[544,512]{1,0:T(8,128)(2,1)S(1)}, u32[]{:S(2)}, u32[]{:S(2)}) collective-permute-start(bf16[544,512]{1,0:T(8,128)(2,1)S(1)} %pad_maximum_fusion.x0), channel_id=1, source_target_pairs={{0,1},{1,2},{2,3},{3,0},{4,5},{5,6},{6,7},{7,4},{8,9},{9,10},{10,1... | collective-permute-start | bytes 1671176 | tf_op jit(solution)/shard_map/ppermute | solution.py:361
  59.9 3.0 %collective-permute-start.2 = (bf16[544,512]{1,0:T(8,128)(2,1)S(1)}, bf16[544,512]{1,0:T(8,128)(2,1)S(1)}, u32[]{:S(2)}, u32[]{:S(2)}) collective-permute-start(bf16[544,512]{1,0:T(8,128)(2,1)S(1)} %pad_maximum_fusion.x0), channel_id=1, source_target_pairs={{0,2},{1,3},{2,0},{3,1},{4,6},{5,7},{6,4},{7,5},{8,10},{9,11},{10,... | collective-permute-start | bytes 1671176 | tf_op jit(solution)/shard_map/ppermute | solution.py:361
  62.9 4.1 %collective-permute-start.3 = (bf16[544,512]{1,0:T(8,128)(2,1)S(1)}, bf16[544,512]{1,0:T(8,128)(2,1)}, u32[]{:S(2)}, u32[]{:S(2)}) collective-permute-start(bf16[544,512]{1,0:T(8,128)(2,1)S(1)} %pad_maximum_fusion.x0), channel_id=1, source_target_pairs={{0,3},{1,0},{2,1},{3,2},{4,7},{5,4},{6,5},{7,6},{8,11},{9,8},{10,9... | collective-permute-start | bytes 1671176 | tf_op jit(solution)/shard_map/ppermute | solution.py:361
  67.0 0.0 copy-done.13
  67.1 0.0 copy-done.7
  67.1 0.0 copy-done.12
  67.1 0.1 broadcast_in_dim.49
  67.2 0.1 broadcast_in_dim_reshape.3
  67.3 0.0 copy-done.10
  67.3 0.6 pad.36.extra
  67.9 0.1 broadcast_in_dim.48
  68.0 0.1 broadcast_in_dim.47
  68.1 2.4 %concatenate.18.params = f32[32,384]{1,0:T(8,128)} concatenate(f32[4,384]{1,0:T(4,128)S(1)} %select_maximum_fusion, f32[4,384]{1,0:T(4,128)S(1)} %pad.30, f32[8,384]{1,0:T(8,128)S(1)} %broadcast_in_dim.47, f32[8,384]{1,0:T(8,128)S(1)} %broadcast_in_dim.48, f32[1,384]{1,0:T(1,128)S(1)} %pad.33, f32[1,384]{1,0:T(1,128)S(1)} %pad.34, f32[1,384]{1,0:T(1,128)S(1)} %pad.35, ...), dimensions={0} | concatenate | bytes 98304 | tf_op jit(solution)/shard_map/concatenate | solution.py:372
  70.5 3.4 %collective-permute-done.1.x1 = bf16[544,512]{1,0:T(8,128)(2,1)S(1)} collective-permute-done((bf16[544,512]{1,0:T(8,128)(2,1)S(1)}, bf16[544,512]{1,0:T(8,128)(2,1)S(1)}, u32[]{:S(2)}, u32[]{:S(2)}) %collective-permute-start.1) | collective-permute-done | bytes 557088 | tf_op jit(solution)/shard_map/ppermute | solution.py:361
  73.9 5.0 %collective-permute-done.2.x2 = bf16[544,512]{1,0:T(8,128)(2,1)S(1)} collective-permute-done((bf16[544,512]{1,0:T(8,128)(2,1)S(1)}, bf16[544,512]{1,0:T(8,128)(2,1)S(1)}, u32[]{:S(2)}, u32[]{:S(2)}) %collective-permute-start.2) | collective-permute-done | bytes 557088 | tf_op jit(solution)/shard_map/ppermute | solution.py:361
  78.9 0.8 copy-done.4
  79.7 10.6 %collective-permute-done.3.x3 = bf16[544,512]{1,0:T(8,128)(2,1)} collective-permute-done((bf16[544,512]{1,0:T(8,128)(2,1)S(1)}, bf16[544,512]{1,0:T(8,128)(2,1)}, u32[]{:S(2)}, u32[]{:S(2)}) %collective-permute-start.3) | collective-permute-done | bytes 557088 | tf_op jit(solution)/shard_map/ppermute | solution.py:361
  90.3 2.5 %shard_map.190.normed = bf16[4,528,512]{2,1,0:T(8,128)(2,1)S(1)} custom-call(bf16[544,512]{1,0:T(8,128)(2,1)} %copy-done.1, bf16[544,512]{1,0:T(8,128)(2,1)} %copy-done.3, bf16[544,512]{1,0:T(8,128)(2,1)} %copy-done.4, bf16[544,512]{1,0:T(8,128)(2,1)} %collective-permute-done.3.x3), custom_call_target="tpu_custom_call" | custom-call | flops 1000000 | bytes 2228224 | tf_op jit(solution)/shard_map/pallas_call | solution.py:282
  92.8 0.0 collective-permute-done.4.other
  92.9 5.4 %shard_map.192 = (bf16[512,256]{1,0:T(8,128)(2,1)}, bf16[512,128]{1,0:T(8,128)(2,1)}, f32[8,512]{1,0:T(8,128)}, f32[8,512]{1,0:T(8,128)}, bf16[80,256]{1,0:T(8,128)(2,1)S(1)}) custom-call(bf16[4,528,512]{2,1,0:T(8,128)(2,1)S(1)} %shard_map.190.normed, bf16[64,16,384]{2,1,0:T(8,128)(2,1)S(1)} %all_to_all.20.mine, ...), custom_call_target="tpu_custom_call" | custom-call | flops 830472192 | bytes 3801088 | tf_op jit(solution)/shard_map/pallas_call | solution.py:282
  98.3 18.0 %all-gather = bf16[1280,256]{1,0:T(8,128)(2,1)S(1)} all-gather(bf16[80,256]{1,0:T(8,128)(2,1)S(1)} %get-tuple-element.23), channel_id=2, replica_groups=mesh['sp_0'=8,'sp_1'=8,'sp_2'=2,'tp'=4] {'sp_1','sp_2'}, dimensions={0}, use_global_device_ids=true | all-gather | bytes 696320 | tf_op jit(solution)/shard_map/all_gather | solution.py:402
  116.3 0.8 shard_map.194
  117.1 0.7 broadcast_in_dim.55
  117.9 4.6 %all-to-all-start.1 = ((bf16[8,80,256]{2,1,0:T(8,128)(2,1)}), bf16[8,80,256]{2,1,0:T(8,128)(2,1)S(1)}, u32[]{:S(2)}, u32[]{:S(2)}) async-start(bf16[8,80,256]{2,1,0:T(8,128)(2,1)} %broadcast_in_dim.55), calls=%async_computation.1 | async-start | bytes 655360 | tf_op jit(solution)/shard_map/all_to_all | solution.py:26
  122.5 3.3 %shard_map.193 = (f32[40,128,128]{2,1,0:T(8,128)}, bf16[512,256]{1,0:T(8,128)(2,1)}) custom-call(bf16[512,256]{1,0:T(8,128)(2,1)} %get-tuple-element.17.value, f32[8,512]{1,0:T(8,128)} %get-tuple-element.19.cum, f32[8,512]{1,0:T(8,128)} %get-tuple-element.20.step), custom_call_target="tpu_custom_call" | custom-call | flops 10000000 | bytes 294912 | tf_op jit(solution)/shard_map/pallas_call | solution.py:282
  125.8 10.5 %all-to-all-done.1.planes = bf16[8,80,256]{2,1,0:T(8,128)(2,1)S(1)} async-done(((bf16[8,80,256]{2,1,0:T(8,128)(2,1)}), bf16[8,80,256]{2,1,0:T(8,128)(2,1)S(1)}, u32[]{:S(2)}, u32[]{:S(2)}) %all-to-all-start.1) | async-done | bytes 327712 | tf_op jit(solution)/shard_map/all_to_all | solution.py:26
  136.3 7.5 %shard_map.195 = (bf16[512,256]{1,0:T(8,128)(2,1)S(1)}, f32[1,512]{1,0:T(1,128)S(1)}) custom-call(bf16[4,528,512]{2,1,0:T(8,128)(2,1)} %copy-done, bf16[2048,1152]{1,0:T(8,128)(2,1)} %all-gather.3.cloned.1.call-done.weight, bf16[512,256]{1,0:T(8,128)(2,1)} %get-tuple-element.17.value, bf16[512,128]{1,0:T(8,128)(2,1)} %get-tuple-element.18.key, ...), custom_call_target="tpu_custom_call" | custom-call | flops 830472192 | bytes 10625024 | tf_op jit(solution)/shard_map/pallas_call | solution.py:282
  143.8 0.6 broadcast_in_dim.56
  144.4 4.2 %all-to-all-start.2 = ((f32[4,1,512]{2,1,0:T(1,128)}), f32[4,1,512]{2,1,0:T(1,128)S(1)}, u32[]{:S(2)}, u32[]{:S(2)}) async-start(f32[4,1,512]{2,1,0:T(1,128)} %broadcast_in_dim.56), calls=%async_computation.2 | async-start | bytes 16384 | tf_op jit(solution)/shard_map/all_to_all | solution.py:26
  148.7 4.9 %shard_map.191.pool = bf16[512,256]{1,0:T(8,128)(2,1)} custom-call(bf16[4,528,512]{2,1,0:T(8,128)(2,1)} %copy-done, bf16[2048,1152]{1,0:T(8,128)(2,1)} %all-gather.3.cloned.1.call-done.weight, f32[32,384]{1,0:T(8,128)} %concatenate.18.params, bf16[256,256]{1,0:T(8,128)(2,1)} %bitcast.10), custom_call_target="tpu_custom_call" | custom-call | flops 553648128 | bytes 7061504 | tf_op jit(solution)/shard_map/pallas_call | solution.py:282
  153.5 0.0 all-to-all-done.2.squares
  153.5 3.9 %shard_map.196 = bf16[4,512,512]{2,1,0:T(8,128)(2,1)S(1)} custom-call(bf16[512,256]{1,0:T(8,128)(2,1)} %shard_map.191.pool, bf16[512,256]{1,0:T(8,128)(2,1)S(1)} %get-tuple-element.27.rows, bf16[2048,1152]{1,0:T(8,128)(2,1)} %all-gather.3.cloned.1.call-done.weight, f32[4,1,512]{2,1,0:T(1,128)S(1)} %all-to-all-done.2.squares), custom_call_target="tpu_custom_call" | custom-call | flops 1073741824 | bytes 5251072 | tf_op jit(solution)/shard_map/pallas_call | solution.py:282
  157.5 29.1 %all_to_all.21 = bf16[4,512,512]{2,1,0:T(8,128)(2,1)S(1)} all-to-all(bf16[4,512,512]{2,1,0:T(8,128)(2,1)S(1)} %shard_map.196), channel_id=1, replica_groups=mesh['sp_0'=8,'sp_1'=8,'sp_2'=2,'tp'=4] {'tp'}, dimensions={0} | all-to-all | bytes 4194304 | tf_op jit(solution)/shard_map/all_to_all | solution.py:472
  186.6 1.2 reduce_sum.12
  (37 shorter events, 0.1 us)
Async XLA Ops:
  6.5 46.7 %copy-start.2 = (bf16[512,512]{1,0:T(8,128)(2,1)S(1)}, bf16[512,512]{1,0:T(8,128)(2,1)}, u32[]{:S(2)}) copy-start(bf16[512,512]{1,0:T(8,128)(2,1)} %param.20) | copy-start | bytes 1572868
  6.5 49.9 %copy-start.9 = (bf16[512]{0:T(512)(128)(2,1)S(1)}, bf16[512]{0:T(512)(128)(2,1)}, u32[]{:S(2)}) copy-start(bf16[512]{0:T(512)(128)(2,1)} %param.21) | copy-start | bytes 3076
  6.5 60.5 %copy-start.13 = (f32[4]{0:T(128)S(1)}, f32[4]{0:T(128)}, u32[]{:S(2)}) copy-start(f32[4]{0:T(128)} %param.34) | copy-start | bytes 52
  6.5 60.5 %copy-start.14 = (f32[4]{0:T(128)S(1)}, f32[4]{0:T(128)}, u32[]{:S(2)}) copy-start(f32[4]{0:T(128)} %param.33) | copy-start | bytes 52
  6.5 60.5 %copy-start.7 = (f32[4,64]{1,0:T(4,128)S(1)}, f32[4,64]{1,0:T(4,128)}, u32[]{:S(2)}) copy-start(f32[4,64]{1,0:T(4,128)} %param.32) | copy-start | bytes 3076
  6.5 60.5 %copy-start.12 = (f32[4]{0:T(128)S(1)}, f32[4]{0:T(128)}, u32[]{:S(2)}) copy-start(f32[4]{0:T(128)} %param.36) | copy-start | bytes 52
  6.6 60.7 %copy-start.10 = (f32[256]{0:T(256)S(1)}, f32[256]{0:T(256)}, u32[]{:S(2)}) copy-start(f32[256]{0:T(256)} %param.29) | copy-start | bytes 3076
  6.6 60.7 %copy-start.11 = (f32[256]{0:T(256)S(1)}, f32[256]{0:T(256)}, u32[]{:S(2)}) copy-start(f32[256]{0:T(256)} %param.37) | copy-start | bytes 3076
  6.6 60.7 %copy-start.5 = (f32[512,4]{0,1:T(4,128)S(1)}, f32[512,4]{0,1:T(4,128)}, u32[]{:S(2)}) copy-start(f32[512,4]{0,1:T(4,128)} %param.35) | copy-start | bytes 24580
  6.6 61.3 %copy-start.6 = (f32[4,256]{1,0:T(4,128)S(1)}, f32[4,256]{1,0:T(4,128)}, u32[]{:S(2)}) copy-start(f32[4,256]{1,0:T(4,128)} %param.30) | copy-start | bytes 12292
  6.6 61.3 %copy-start.8 = (f32[4,64]{1,0:T(4,128)S(1)}, f32[4,64]{1,0:T(4,128)}, u32[]{:S(2)}) copy-start(f32[4,64]{1,0:T(4,128)} %param.31) | copy-start | bytes 3076
  6.6 129.7 %all-gather.3.cloned.1.call-start = ((), (), s32[]{:S(2)}) async-start(), calls=%async_computation.4 | async-start | bytes 4755456 | tf_op jit(solution)/shard_map/all_gather | solution.py:349
  51.3 41.5 %collective-permute-start.4 = (bf16[64,16,384]{2,1,0:T(8,128)(2,1)S(1)}, bf16[64,16,384]{2,1,0:T(8,128)(2,1)}, u32[]{:S(2)}, u32[]{:S(2)}) collective-permute-start(bf16[64,16,384]{2,1,0:T(8,128)(2,1)S(1)} %all_to_all.20.mine), channel_id=1, source_target_pairs={{0,4},{4,0},{1,5},{5,1},{2,6},{6,2},{3,7},{7,3},{8,12},{12,8},{9,1... | collective-permute-start | bytes 2359304 | tf_op jit(solution)/shard_map/ppermute | solution.py:353
  53.2 3.2 %collective-permute-start = (bf16[16,512]{1,0:T(8,128)(2,1)S(1)}, bf16[16,512]{1,0:T(8,128)(2,1)S(1)}, u32[]{:S(2)}, u32[]{:S(2)}) collective-permute-start(bf16[16,512]{1,0:T(8,128)(2,1)S(1)} %slice.3), channel_id=1, source_target_pairs={{0,4},{4,8},{8,12},{12,16},{16,20},{20,24},{24,28},{28,32},{32,36}... | collective-permute-start | bytes 49160 | tf_op jit(solution)/shard_map/ppermute | solution.py:355
  56.5 33.8 %copy-start.1 = (bf16[544,512]{1,0:T(8,128)(2,1)}, bf16[544,512]{1,0:T(8,128)(2,1)S(1)}, u32[]{:S(2)}) copy-start(bf16[544,512]{1,0:T(8,128)(2,1)S(1)} %pad_maximum_fusion.x0) | copy-start | bytes 1671172
  56.5 17.4 %collective-permute-start.1 = (bf16[544,512]{1,0:T(8,128)(2,1)S(1)}, bf16[544,512]{1,0:T(8,128)(2,1)S(1)}, u32[]{:S(2)}, u32[]{:S(2)}) collective-permute-start(bf16[544,512]{1,0:T(8,128)(2,1)S(1)} %pad_maximum_fusion.x0), channel_id=1, source_target_pairs={{0,1},{1,2},{2,3},{3,0},{4,5},{5,6},{6,7},{7,4},{8,9},{9,10},{10,1... | collective-permute-start | bytes 1671176 | tf_op jit(solution)/shard_map/ppermute | solution.py:361
  59.9 18.9 %collective-permute-start.2 = (bf16[544,512]{1,0:T(8,128)(2,1)S(1)}, bf16[544,512]{1,0:T(8,128)(2,1)S(1)}, u32[]{:S(2)}, u32[]{:S(2)}) collective-permute-start(bf16[544,512]{1,0:T(8,128)(2,1)S(1)} %pad_maximum_fusion.x0), channel_id=1, source_target_pairs={{0,2},{1,3},{2,0},{3,1},{4,6},{5,7},{6,4},{7,5},{8,10},{9,11},{10,... | collective-permute-start | bytes 1671176 | tf_op jit(solution)/shard_map/ppermute | solution.py:361
  62.9 27.4 %collective-permute-start.3 = (bf16[544,512]{1,0:T(8,128)(2,1)S(1)}, bf16[544,512]{1,0:T(8,128)(2,1)}, u32[]{:S(2)}, u32[]{:S(2)}) collective-permute-start(bf16[544,512]{1,0:T(8,128)(2,1)S(1)} %pad_maximum_fusion.x0), channel_id=1, source_target_pairs={{0,3},{1,0},{2,1},{3,2},{4,7},{5,4},{6,5},{7,6},{8,11},{9,8},{10,9... | collective-permute-start | bytes 1671176 | tf_op jit(solution)/shard_map/ppermute | solution.py:361
  73.9 5.0 %copy-start.3 = (bf16[544,512]{1,0:T(8,128)(2,1)}, bf16[544,512]{1,0:T(8,128)(2,1)S(1)}, u32[]{:S(2)}) copy-start(bf16[544,512]{1,0:T(8,128)(2,1)S(1)} %collective-permute-done.1.x1) | copy-start | bytes 1671172
  78.9 0.8 copy-start.4
  92.8 23.5 %copy-start = (bf16[4,528,512]{2,1,0:T(8,128)(2,1)}, bf16[4,528,512]{2,1,0:T(8,128)(2,1)S(1)}, u32[]{:S(2)}) copy-start(bf16[4,528,512]{2,1,0:T(8,128)(2,1)S(1)} %shard_map.190.normed) | copy-start | bytes 6488068
  117.9 18.4 %all-to-all-start.1 = ((bf16[8,80,256]{2,1,0:T(8,128)(2,1)}), bf16[8,80,256]{2,1,0:T(8,128)(2,1)S(1)}, u32[]{:S(2)}, u32[]{:S(2)}) async-start(bf16[8,80,256]{2,1,0:T(8,128)(2,1)} %broadcast_in_dim.55), calls=%async_computation.1 | async-start | bytes 655360 | tf_op jit(solution)/shard_map/all_to_all | solution.py:26
  144.4 9.1 %all-to-all-start.2 = ((f32[4,1,512]{2,1,0:T(1,128)}), f32[4,1,512]{2,1,0:T(1,128)S(1)}, u32[]{:S(2)}, u32[]{:S(2)}) async-start(f32[4,1,512]{2,1,0:T(1,128)} %broadcast_in_dim.56), calls=%async_computation.2 | async-start | bytes 16384 | tf_op jit(solution)/shard_map/all_to_all | solution.py:26
Sparse Core Ops, SparseCore 0:
  10.6 95.6 all-gather.2

commit v9 on v8

--- a/solution.py
+++ b/solution.py
@@ -161,7 +161,7 @@
                 at = at + 1
 
 
-def block_products(normed, weight, rows_here, weight_here, arrived, lanes):
+def block_products(normed, weight, rows_here, weight_here, arrived, lanes, later=()):
     place = lax.axis_index("tp")
     count, total_rows, width = rows_here.shape
     copies = []
@@ -177,6 +177,8 @@
             )
         for copy in copies[k]:
             copy.start()
+    for copy in later:
+        copy.start()
     sums = [jnp.zeros((total_rows, size), F32) for _, size in lanes]
     for k in range(count):
         for copy in copies[k]:
@@ -210,10 +212,9 @@
 ):
     length, span = rows_out.shape
     fetch = pltpu.make_async_copy(factors_far, factors, factors_arrived)
-    fetch.start()
     lanes = [(span, span), (4 * span, BLOCK)]
     acc, acc_read = block_products(
-        normed, weight, rows_here, [gate_here, read_here], arrived, lanes
+        normed, weight, rows_here, [gate_here, read_here], arrived, lanes, [fetch]
     )
     gate = silu(acc[HALO:].astype(BF16).astype(F32))
     reads = convolved(acc_read.astype(BF16).astype(F32), params[4:8, :BLOCK], length)
@@ -243,25 +244,15 @@
         rows_out[here] = (gated * params[26:27, :span]).astype(BF16)
 
 
-def out_kernel(pool, rows, weight, squares, out, weight_here, arrived):
+def out_kernel(pool, rows, weight, squares, out):
     span = pool.shape[1]
-    count, _, width = out.shape
-    copies = [
-        pltpu.make_async_copy(
-            weight.at[pl.ds(d * width, width), pl.ds(2 * span, 2 * span)],
-            weight_here.at[d],
-            arrived.at[d],
-        )
-        for d in range(count)
-    ]
-    for copy in copies:
-        copy.start()
     scale = lax.rsqrt(jnp.sum(squares[...], axis=0) / MIX_W + EPSILON)
     scale = jnp.transpose(jnp.broadcast_to(scale, (8, scale.shape[1])))[:, :1]
-    for d in range(count):
-        copies[d].wait()
-        terms = dot(pool[...], weight_here[d, :, :span], 1, 1)
-        terms = terms + dot(rows[...], weight_here[d, :, span:], 1, 1) * scale
+    for d in range(out.shape[0]):
+        width = out.shape[2]
+        block = weight[d * width : (d + 1) * width]
+        terms = dot(pool[...], block[:, :span], 1, 1)
+        terms = terms + dot(rows[...], block[:, span:], 1, 1) * scale
         out[d] = terms.astype(BF16)
 
 
@@ -462,11 +453,7 @@
         (pool_out, gated, later_weights, all_squares),
         (shape_of((count, length, width), BF16),),
         2 * length * 2 * mix * D,
-        [
-            pltpu.VMEM((count, width, 2 * mix), BF16),
-            pltpu.SemaphoreType.DMA((count,)),
-        ],
-        specs={2: anywhere},
+        specs={2: pl.BlockSpec((D, 2 * mix), lambda *_: (0, 1))},
         far=(0, 2),
     )[0]
     arrived = lax.all_to_all(terms, "tp", split_axis=0, concat_axis=0, tiled=True)

time: 195 us -> 194 us (level)
  no operation moved by 1% of the time
where the time goes in v9:
time: 194 us
  blocking collectives  88.5 us (46%)
  waiting for transfers between devices  30.4 us (16%)
  Pallas kernels  27.2 us (14%)
  starting transfers between devices  23.7 us (12%)
  between operations  13.7 us (7%)
  local copies, waits for them, and re-layouts  8.06 us (4%)
  other arithmetic  2.08 us (1%)
    all_to_all x1, blocking collectives, sent_to_all(): return lax.all_to_all(copies, axis, split_axis=0, concat_axis=0, tiled=True)  41.3 us
    all_to_all x1, blocking collectives, local(): lax.all_to_all(terms, 'tp', split_axis=0, concat_axis=0, tiled=True)  29.1 us
    pallas_call x7, Pallas kernels, call(): pl.pallas_call(kernel, grid=(1,), in_specs=[specs.get(k, whole(a.shape))...  27.2 us
    ppermute x3, waiting for transfers between devices, local(): pieces.append(lax.ppermute(sent, 'tp', pairs))  19 us
    all_gather x1, blocking collectives, local(): row_pieces = lax.all_gather(payload, ('sp_1', 'sp_2'))  18 us
    all_to_all x2, waiting for transfers between devices, sent_to_all(): return lax.all_to_all(copies, axis, split_axis=0, concat_axis=0, tiled=True)  10.5 us
    ppermute x3, starting transfers between devices, local(): pieces.append(lax.ppermute(sent, 'tp', pairs))  10.5 us
    all_to_all x2, starting transfers between devices, sent_to_all(): return lax.all_to_all(copies, axis, split_axis=0, concat_axis=0, tiled=True)  8.86 us
  transfers between devices with their start and end apart: 8, of which 5 were waited for; matrix products, arithmetic and copies ran while one was open for 3% of the time, Pallas kernels for 9%

profile of v9, /device:TPU:2, one launch (start us, length us, event | category | flops | bytes accessed | tf_op | source)
XLA Modules:
  0.0 193.6 jit_solution(832019786660711541)
XLA Ops:
  6.5 0.0 copy-start.12
  6.6 0.0 copy-start.10
  6.6 0.0 all-gather.3.cloned.1.call-start
  6.7 1.6 concatenate.16
  8.2 0.0 all-gather.3.cloned.1.call-update
  8.2 0.8 copy.21
  9.0 0.1 pad.40.clone
  9.1 0.8 maximum_maximum_fusion
  9.9 0.1 broadcast_in_dim.54
  10.0 41.3 %all_to_all.20.mine = bf16[64,16,384]{2,1,0:T(8,128)(2,1)S(1)} all-to-all(bf16[64,16,384]{2,1,0:T(8,128)(2,1)S(1)} %broadcast_in_dim.54), channel_id=1, replica_groups=mesh['sp_0'=8,'sp_1'=8,'sp_2'=2,'tp'=4] {'sp_0','sp_1'}, dimensions={0} | all-to-all | bytes 1572864 | tf_op jit(solution)/shard_map/all_to_all | solution.py:26
  51.3 1.9 collective-permute-start.4
  53.2 0.0 copy-done.2
  53.2 2.4 %collective-permute-start = (bf16[16,512]{1,0:T(8,128)(2,1)S(1)}, bf16[16,512]{1,0:T(8,128)(2,1)S(1)}, u32[]{:S(2)}, u32[]{:S(2)}) collective-permute-start(bf16[16,512]{1,0:T(8,128)(2,1)S(1)} %slice.3), channel_id=1, source_target_pairs={{0,4},{4,8},{8,12},{12,16},{16,20},{20,24},{24,28},{28,32},{32,36}... | collective-permute-start | bytes 49160 | tf_op jit(solution)/shard_map/ppermute | solution.py:346
  55.6 0.8 collective-permute-done
  56.5 3.4 %collective-permute-start.1 = (bf16[544,512]{1,0:T(8,128)(2,1)S(1)}, bf16[544,512]{1,0:T(8,128)(2,1)S(1)}, u32[]{:S(2)}, u32[]{:S(2)}) collective-permute-start(bf16[544,512]{1,0:T(8,128)(2,1)S(1)} %pad_maximum_fusion.x0), channel_id=1, source_target_pairs={{0,1},{1,2},{2,3},{3,0},{4,5},{5,6},{6,7},{7,4},{8,9},{9,10},{10,1... | collective-permute-start | bytes 1671176 | tf_op jit(solution)/shard_map/ppermute | solution.py:352
  59.9 3.0 %collective-permute-start.2 = (bf16[544,512]{1,0:T(8,128)(2,1)S(1)}, bf16[544,512]{1,0:T(8,128)(2,1)S(1)}, u32[]{:S(2)}, u32[]{:S(2)}) collective-permute-start(bf16[544,512]{1,0:T(8,128)(2,1)S(1)} %pad_maximum_fusion.x0), channel_id=1, source_target_pairs={{0,2},{1,3},{2,0},{3,1},{4,6},{5,7},{6,4},{7,5},{8,10},{9,11},{10,... | collective-permute-start | bytes 1671176 | tf_op jit(solution)/shard_map/ppermute | solution.py:352
  62.9 4.1 %collective-permute-start.3 = (bf16[544,512]{1,0:T(8,128)(2,1)S(1)}, bf16[544,512]{1,0:T(8,128)(2,1)}, u32[]{:S(2)}, u32[]{:S(2)}) collective-permute-start(bf16[544,512]{1,0:T(8,128)(2,1)S(1)} %pad_maximum_fusion.x0), channel_id=1, source_target_pairs={{0,3},{1,0},{2,1},{3,2},{4,7},{5,4},{6,5},{7,6},{8,11},{9,8},{10,9... | collective-permute-start | bytes 1671176 | tf_op jit(solution)/shard_map/ppermute | solution.py:352
  67.0 0.0 copy-done.13
  67.1 0.0 copy-done.7
  67.1 0.0 copy-done.12
  67.1 0.1 broadcast_in_dim.49
  67.2 0.1 broadcast_in_dim_reshape.3
  67.3 0.0 copy-done.10
  67.3 0.6 pad.36.extra
  67.9 0.1 broadcast_in_dim.48
  68.0 0.1 broadcast_in_dim.47
  68.1 2.4 %concatenate.18.params = f32[32,384]{1,0:T(8,128)} concatenate(f32[4,384]{1,0:T(4,128)S(1)} %select_maximum_fusion, f32[4,384]{1,0:T(4,128)S(1)} %pad.30, f32[8,384]{1,0:T(8,128)S(1)} %broadcast_in_dim.47, f32[8,384]{1,0:T(8,128)S(1)} %broadcast_in_dim.48, f32[1,384]{1,0:T(1,128)S(1)} %pad.33, f32[1,384]{1,0:T(1,128)S(1)} %pad.34, f32[1,384]{1,0:T(1,128)S(1)} %pad.35, ...), dimensions={0} | concatenate | bytes 98304 | tf_op jit(solution)/shard_map/concatenate | solution.py:363
  70.5 3.4 %collective-permute-done.1.x1 = bf16[544,512]{1,0:T(8,128)(2,1)S(1)} collective-permute-done((bf16[544,512]{1,0:T(8,128)(2,1)S(1)}, bf16[544,512]{1,0:T(8,128)(2,1)S(1)}, u32[]{:S(2)}, u32[]{:S(2)}) %collective-permute-start.1) | collective-permute-done | bytes 557088 | tf_op jit(solution)/shard_map/ppermute | solution.py:352
  73.9 5.0 %collective-permute-done.2.x2 = bf16[544,512]{1,0:T(8,128)(2,1)S(1)} collective-permute-done((bf16[544,512]{1,0:T(8,128)(2,1)S(1)}, bf16[544,512]{1,0:T(8,128)(2,1)S(1)}, u32[]{:S(2)}, u32[]{:S(2)}) %collective-permute-start.2) | collective-permute-done | bytes 557088 | tf_op jit(solution)/shard_map/ppermute | solution.py:352
  78.9 0.8 copy-done.4
  79.7 10.6 %collective-permute-done.3.x3 = bf16[544,512]{1,0:T(8,128)(2,1)} collective-permute-done((bf16[544,512]{1,0:T(8,128)(2,1)S(1)}, bf16[544,512]{1,0:T(8,128)(2,1)}, u32[]{:S(2)}, u32[]{:S(2)}) %collective-permute-start.3) | collective-permute-done | bytes 557088 | tf_op jit(solution)/shard_map/ppermute | solution.py:352
  90.3 2.5 %shard_map.190.normed = bf16[4,528,512]{2,1,0:T(8,128)(2,1)S(1)} custom-call(bf16[544,512]{1,0:T(8,128)(2,1)} %copy-done.1, bf16[544,512]{1,0:T(8,128)(2,1)} %copy-done.3, bf16[544,512]{1,0:T(8,128)(2,1)} %copy-done.4, bf16[544,512]{1,0:T(8,128)(2,1)} %collective-permute-done.3.x3), custom_call_target="tpu_custom_call" | custom-call | flops 1000000 | bytes 2228224 | tf_op jit(solution)/shard_map/pallas_call | solution.py:273
  92.8 0.0 collective-permute-done.4.other
  92.9 5.4 %shard_map.192 = (bf16[512,256]{1,0:T(8,128)(2,1)}, bf16[512,128]{1,0:T(8,128)(2,1)}, f32[8,512]{1,0:T(8,128)}, f32[8,512]{1,0:T(8,128)}, bf16[80,256]{1,0:T(8,128)(2,1)S(1)}) custom-call(bf16[4,528,512]{2,1,0:T(8,128)(2,1)S(1)} %shard_map.190.normed, bf16[64,16,384]{2,1,0:T(8,128)(2,1)S(1)} %all_to_all.20.mine, ...), custom_call_target="tpu_custom_call" | custom-call | flops 830472192 | bytes 3801088 | tf_op jit(solution)/shard_map/pallas_call | solution.py:273
  98.3 18.0 %all-gather = bf16[1280,256]{1,0:T(8,128)(2,1)S(1)} all-gather(bf16[80,256]{1,0:T(8,128)(2,1)S(1)} %get-tuple-element.23), channel_id=2, replica_groups=mesh['sp_0'=8,'sp_1'=8,'sp_2'=2,'tp'=4] {'sp_1','sp_2'}, dimensions={0}, use_global_device_ids=true | all-gather | bytes 696320 | tf_op jit(solution)/shard_map/all_gather | solution.py:393
  116.3 0.8 shard_map.194
  117.1 0.7 broadcast_in_dim.55
  117.9 4.6 %all-to-all-start.1 = ((bf16[8,80,256]{2,1,0:T(8,128)(2,1)}), bf16[8,80,256]{2,1,0:T(8,128)(2,1)S(1)}, u32[]{:S(2)}, u32[]{:S(2)}) async-start(bf16[8,80,256]{2,1,0:T(8,128)(2,1)} %broadcast_in_dim.55), calls=%async_computation.1 | async-start | bytes 655360 | tf_op jit(solution)/shard_map/all_to_all | solution.py:26
  122.5 3.3 %shard_map.193 = (f32[40,128,128]{2,1,0:T(8,128)}, bf16[512,256]{1,0:T(8,128)(2,1)}) custom-call(bf16[512,256]{1,0:T(8,128)(2,1)} %get-tuple-element.17.value, f32[8,512]{1,0:T(8,128)} %get-tuple-element.19.cum, f32[8,512]{1,0:T(8,128)} %get-tuple-element.20.step), custom_call_target="tpu_custom_call" | custom-call | flops 10000000 | bytes 294912 | tf_op jit(solution)/shard_map/pallas_call | solution.py:273
  125.8 10.5 %all-to-all-done.1.planes = bf16[8,80,256]{2,1,0:T(8,128)(2,1)S(1)} async-done(((bf16[8,80,256]{2,1,0:T(8,128)(2,1)}), bf16[8,80,256]{2,1,0:T(8,128)(2,1)S(1)}, u32[]{:S(2)}, u32[]{:S(2)}) %all-to-all-start.1) | async-done | bytes 327712 | tf_op jit(solution)/shard_map/all_to_all | solution.py:26
  136.3 7.3 %shard_map.195 = (bf16[512,256]{1,0:T(8,128)(2,1)S(1)}, f32[1,512]{1,0:T(1,128)S(1)}) custom-call(bf16[4,528,512]{2,1,0:T(8,128)(2,1)} %copy-done, bf16[2048,1152]{1,0:T(8,128)(2,1)} %all-gather.3.cloned.1.call-done.weight, bf16[512,256]{1,0:T(8,128)(2,1)} %get-tuple-element.17.value, bf16[512,128]{1,0:T(8,128)(2,1)} %get-tuple-element.18.key, ...), custom_call_target="tpu_custom_call" | custom-call | flops 830472192 | bytes 10625024 | tf_op jit(solution)/shard_map/pallas_call | solution.py:273
  143.6 0.6 broadcast_in_dim.56
  144.2 4.3 %all-to-all-start.2 = ((f32[4,1,512]{2,1,0:T(1,128)}), f32[4,1,512]{2,1,0:T(1,128)S(1)}, u32[]{:S(2)}, u32[]{:S(2)}) async-start(f32[4,1,512]{2,1,0:T(1,128)} %broadcast_in_dim.56), calls=%async_computation.2 | async-start | bytes 16384 | tf_op jit(solution)/shard_map/all_to_all | solution.py:26
  148.5 4.9 %shard_map.191.pool = bf16[512,256]{1,0:T(8,128)(2,1)} custom-call(bf16[4,528,512]{2,1,0:T(8,128)(2,1)} %copy-done, bf16[2048,1152]{1,0:T(8,128)(2,1)} %all-gather.3.cloned.1.call-done.weight, f32[32,384]{1,0:T(8,128)} %concatenate.18.params, bf16[256,256]{1,0:T(8,128)(2,1)} %bitcast.10), custom_call_target="tpu_custom_call" | custom-call | flops 553648128 | bytes 7061504 | tf_op jit(solution)/shard_map/pallas_call | solution.py:273
  153.3 0.0 all-to-all-done.2.squares
  153.3 3.0 %shard_map.196 = bf16[4,512,512]{2,1,0:T(8,128)(2,1)S(1)} custom-call(bf16[512,256]{1,0:T(8,128)(2,1)} %shard_map.191.pool, bf16[512,256]{1,0:T(8,128)(2,1)S(1)} %get-tuple-element.27.rows, bf16[2048,1152]{1,0:T(8,128)(2,1)} %all-gather.3.cloned.1.call-done.weight, f32[4,1,512]{2,1,0:T(1,128)S(1)} %all-to-all-done.2.squares), custom_call_target="tpu_custom_call" | custom-call | flops 1073741824 | bytes 5251072 | tf_op jit(solution)/shard_map/pallas_call | solution.py:273
  156.4 29.1 %all_to_all.21 = bf16[4,512,512]{2,1,0:T(8,128)(2,1)S(1)} all-to-all(bf16[4,512,512]{2,1,0:T(8,128)(2,1)S(1)} %shard_map.196), channel_id=1, replica_groups=mesh['sp_0'=8,'sp_1'=8,'sp_2'=2,'tp'=4] {'tp'}, dimensions={0} | all-to-all | bytes 4194304 | tf_op jit(solution)/shard_map/all_to_all | solution.py:459
  185.5 1.2 reduce_sum.12
  (37 shorter events, 0.1 us)
Async XLA Ops:
  6.5 46.7 %copy-start.2 = (bf16[512,512]{1,0:T(8,128)(2,1)S(1)}, bf16[512,512]{1,0:T(8,128)(2,1)}, u32[]{:S(2)}) copy-start(bf16[512,512]{1,0:T(8,128)(2,1)} %param.20) | copy-start | bytes 1572868
  6.5 49.9 %copy-start.9 = (bf16[512]{0:T(512)(128)(2,1)S(1)}, bf16[512]{0:T(512)(128)(2,1)}, u32[]{:S(2)}) copy-start(bf16[512]{0:T(512)(128)(2,1)} %param.21) | copy-start | bytes 3076
  6.5 60.5 %copy-start.13 = (f32[4]{0:T(128)S(1)}, f32[4]{0:T(128)}, u32[]{:S(2)}) copy-start(f32[4]{0:T(128)} %param.34) | copy-start | bytes 52
  6.5 60.5 %copy-start.14 = (f32[4]{0:T(128)S(1)}, f32[4]{0:T(128)}, u32[]{:S(2)}) copy-start(f32[4]{0:T(128)} %param.33) | copy-start | bytes 52
  6.5 60.5 %copy-start.7 = (f32[4,64]{1,0:T(4,128)S(1)}, f32[4,64]{1,0:T(4,128)}, u32[]{:S(2)}) copy-start(f32[4,64]{1,0:T(4,128)} %param.32) | copy-start | bytes 3076
  6.5 60.5 %copy-start.12 = (f32[4]{0:T(128)S(1)}, f32[4]{0:T(128)}, u32[]{:S(2)}) copy-start(f32[4]{0:T(128)} %param.36) | copy-start | bytes 52
  6.6 60.7 %copy-start.10 = (f32[256]{0:T(256)S(1)}, f32[256]{0:T(256)}, u32[]{:S(2)}) copy-start(f32[256]{0:T(256)} %param.29) | copy-start | bytes 3076
  6.6 60.7 %copy-start.11 = (f32[256]{0:T(256)S(1)}, f32[256]{0:T(256)}, u32[]{:S(2)}) copy-start(f32[256]{0:T(256)} %param.37) | copy-start | bytes 3076
  6.6 60.7 %copy-start.5 = (f32[512,4]{0,1:T(4,128)S(1)}, f32[512,4]{0,1:T(4,128)}, u32[]{:S(2)}) copy-start(f32[512,4]{0,1:T(4,128)} %param.35) | copy-start | bytes 24580
  6.6 61.3 %copy-start.6 = (f32[4,256]{1,0:T(4,128)S(1)}, f32[4,256]{1,0:T(4,128)}, u32[]{:S(2)}) copy-start(f32[4,256]{1,0:T(4,128)} %param.30) | copy-start | bytes 12292
  6.6 61.3 %copy-start.8 = (f32[4,64]{1,0:T(4,128)S(1)}, f32[4,64]{1,0:T(4,128)}, u32[]{:S(2)}) copy-start(f32[4,64]{1,0:T(4,128)} %param.31) | copy-start | bytes 3076
  6.6 129.7 %all-gather.3.cloned.1.call-start = ((), (), s32[]{:S(2)}) async-start(), calls=%async_computation.4 | async-start | bytes 4755456 | tf_op jit(solution)/shard_map/all_gather | solution.py:340
  51.3 41.5 %collective-permute-start.4 = (bf16[64,16,384]{2,1,0:T(8,128)(2,1)S(1)}, bf16[64,16,384]{2,1,0:T(8,128)(2,1)}, u32[]{:S(2)}, u32[]{:S(2)}) collective-permute-start(bf16[64,16,384]{2,1,0:T(8,128)(2,1)S(1)} %all_to_all.20.mine), channel_id=1, source_target_pairs={{0,4},{4,0},{1,5},{5,1},{2,6},{6,2},{3,7},{7,3},{8,12},{12,8},{9,1... | collective-permute-start | bytes 2359304 | tf_op jit(solution)/shard_map/ppermute | solution.py:344
  53.2 3.2 %collective-permute-start = (bf16[16,512]{1,0:T(8,128)(2,1)S(1)}, bf16[16,512]{1,0:T(8,128)(2,1)S(1)}, u32[]{:S(2)}, u32[]{:S(2)}) collective-permute-start(bf16[16,512]{1,0:T(8,128)(2,1)S(1)} %slice.3), channel_id=1, source_target_pairs={{0,4},{4,8},{8,12},{12,16},{16,20},{20,24},{24,28},{28,32},{32,36}... | collective-permute-start | bytes 49160 | tf_op jit(solution)/shard_map/ppermute | solution.py:346
  56.5 33.8 %copy-start.1 = (bf16[544,512]{1,0:T(8,128)(2,1)}, bf16[544,512]{1,0:T(8,128)(2,1)S(1)}, u32[]{:S(2)}) copy-start(bf16[544,512]{1,0:T(8,128)(2,1)S(1)} %pad_maximum_fusion.x0) | copy-start | bytes 1671172
  56.5 17.4 %collective-permute-start.1 = (bf16[544,512]{1,0:T(8,128)(2,1)S(1)}, bf16[544,512]{1,0:T(8,128)(2,1)S(1)}, u32[]{:S(2)}, u32[]{:S(2)}) collective-permute-start(bf16[544,512]{1,0:T(8,128)(2,1)S(1)} %pad_maximum_fusion.x0), channel_id=1, source_target_pairs={{0,1},{1,2},{2,3},{3,0},{4,5},{5,6},{6,7},{7,4},{8,9},{9,10},{10,1... | collective-permute-start | bytes 1671176 | tf_op jit(solution)/shard_map/ppermute | solution.py:352
  59.9 18.9 %collective-permute-start.2 = (bf16[544,512]{1,0:T(8,128)(2,1)S(1)}, bf16[544,512]{1,0:T(8,128)(2,1)S(1)}, u32[]{:S(2)}, u32[]{:S(2)}) collective-permute-start(bf16[544,512]{1,0:T(8,128)(2,1)S(1)} %pad_maximum_fusion.x0), channel_id=1, source_target_pairs={{0,2},{1,3},{2,0},{3,1},{4,6},{5,7},{6,4},{7,5},{8,10},{9,11},{10,... | collective-permute-start | bytes 1671176 | tf_op jit(solution)/shard_map/ppermute | solution.py:352
  62.9 27.4 %collective-permute-start.3 = (bf16[544,512]{1,0:T(8,128)(2,1)S(1)}, bf16[544,512]{1,0:T(8,128)(2,1)}, u32[]{:S(2)}, u32[]{:S(2)}) collective-permute-start(bf16[544,512]{1,0:T(8,128)(2,1)S(1)} %pad_maximum_fusion.x0), channel_id=1, source_target_pairs={{0,3},{1,0},{2,1},{3,2},{4,7},{5,4},{6,5},{7,6},{8,11},{9,8},{10,9... | collective-permute-start | bytes 1671176 | tf_op jit(solution)/shard_map/ppermute | solution.py:352
  73.9 5.0 %copy-start.3 = (bf16[544,512]{1,0:T(8,128)(2,1)}, bf16[544,512]{1,0:T(8,128)(2,1)S(1)}, u32[]{:S(2)}) copy-start(bf16[544,512]{1,0:T(8,128)(2,1)S(1)} %collective-permute-done.1.x1) | copy-start | bytes 1671172
  78.9 0.8 copy-start.4
  92.8 23.5 %copy-start = (bf16[4,528,512]{2,1,0:T(8,128)(2,1)}, bf16[4,528,512]{2,1,0:T(8,128)(2,1)S(1)}, u32[]{:S(2)}) copy-start(bf16[4,528,512]{2,1,0:T(8,128)(2,1)S(1)} %shard_map.190.normed) | copy-start | bytes 6488068
  117.9 18.4 %all-to-all-start.1 = ((bf16[8,80,256]{2,1,0:T(8,128)(2,1)}), bf16[8,80,256]{2,1,0:T(8,128)(2,1)S(1)}, u32[]{:S(2)}, u32[]{:S(2)}) async-start(bf16[8,80,256]{2,1,0:T(8,128)(2,1)} %broadcast_in_dim.55), calls=%async_computation.1 | async-start | bytes 655360 | tf_op jit(solution)/shard_map/all_to_all | solution.py:26
  144.2 9.1 %all-to-all-start.2 = ((f32[4,1,512]{2,1,0:T(1,128)}), f32[4,1,512]{2,1,0:T(1,128)S(1)}, u32[]{:S(2)}, u32[]{:S(2)}) async-start(f32[4,1,512]{2,1,0:T(1,128)} %broadcast_in_dim.56), calls=%async_computation.2 | async-start | bytes 16384 | tf_op jit(solution)/shard_map/all_to_all | solution.py:26
Sparse Core Ops, SparseCore 0:
  10.6 95.6 all-gather.2

commit v10 on v9

--- a/solution.py
+++ b/solution.py
@@ -8,7 +8,6 @@
 
 
 D = 2048
-POOL_GROUPS = 4
 HEAD = 64
 MIX_W = 1024
 HALO = 16
@@ -192,13 +191,12 @@
     length, span = pool_out.shape
     place = lax.axis_index("tp")
     acc = block_products(normed, weight, rows_here, [weight_here], arrived, [(0, span)])[0]
-    running = acc.astype(BF16).astype(F32)
-    own = running[HALO:]
-    chosen = own
-    for level in range(POOL_GROUPS):
-        stride = 2**level
-        running = running[stride:] + running[:-stride]
-        chosen = jnp.where(place == level, running[running.shape[0] - length :], chosen)
+    values = acc.astype(BF16)
+    own = values[HALO:].astype(F32)
+    shape = (length, values.shape[0])
+    back = HALO + lax.broadcasted_iota(jnp.int32, shape, 0) - lax.broadcasted_iota(jnp.int32, shape, 1)
+    band = jnp.where((back >= 0) & (back < (2 << place)), 1.0, 0.0).astype(BF16)
+    chosen = dot(band, values)
     position = lax.axis_index(SP) * length + lax.broadcasted_iota(jnp.int32, (length, 1), 0) + 1
     counts = jnp.minimum(position, 2 << place).astype(F32)
     pooled = (chosen / counts - own).astype(BF16)

time: 194 us -> 194 us (level)
  no operation moved by 1% of the time
where the time goes in v10:
time: 194 us
  blocking collectives  88.5 us (46%)
  waiting for transfers between devices  30.4 us (16%)
  Pallas kernels  27.2 us (14%)
  starting transfers between devices  23.7 us (12%)
  between operations  13.7 us (7%)
  local copies, waits for them, and re-layouts  8.06 us (4%)
  other arithmetic  2.08 us (1%)
    all_to_all x1, blocking collectives, sent_to_all(): return lax.all_to_all(copies, axis, split_axis=0, concat_axis=0, tiled=True)  41.3 us
    all_to_all x1, blocking collectives, local(): lax.all_to_all(terms, 'tp', split_axis=0, concat_axis=0, tiled=True)  29.1 us
    pallas_call x7, Pallas kernels, call(): pl.pallas_call(kernel, grid=(1,), in_specs=[specs.get(k, whole(a.shape))...  27.2 us
    ppermute x3, waiting for transfers between devices, local(): pieces.append(lax.ppermute(sent, 'tp', pairs))  19 us
    all_gather x1, blocking collectives, local(): row_pieces = lax.all_gather(payload, ('sp_1', 'sp_2'))  18 us
    all_to_all x2, waiting for transfers between devices, sent_to_all(): return lax.all_to_all(copies, axis, split_axis=0, concat_axis=0, tiled=True)  10.5 us
    ppermute x3, starting transfers between devices, local(): pieces.append(lax.ppermute(sent, 'tp', pairs))  10.5 us
    all_to_all x2, starting transfers between devices, sent_to_all(): return lax.all_to_all(copies, axis, split_axis=0, concat_axis=0, tiled=True)  8.86 us
  transfers between devices with their start and end apart: 8, of which 5 were waited for; matrix products, arithmetic and copies ran while one was open for 3% of the time, Pallas kernels for 9%

profile of v10, /device:TPU:2, one launch (start us, length us, event | category | flops | bytes accessed | tf_op | source)
XLA Modules:
  0.0 193.5 jit_solution(11541341724009139942)
XLA Ops:
  6.5 0.0 copy-start.12
  6.6 0.0 copy-start.10
  6.6 0.0 all-gather.3.cloned.1.call-start
  6.7 1.6 concatenate.16
  8.2 0.0 all-gather.3.cloned.1.call-update
  8.2 0.8 copy.21
  9.0 0.1 pad.40.clone
  9.1 0.8 maximum_maximum_fusion
  9.9 0.1 broadcast_in_dim.54
  10.0 41.3 %all_to_all.20.mine = bf16[64,16,384]{2,1,0:T(8,128)(2,1)S(1)} all-to-all(bf16[64,16,384]{2,1,0:T(8,128)(2,1)S(1)} %broadcast_in_dim.54), channel_id=1, replica_groups=mesh['sp_0'=8,'sp_1'=8,'sp_2'=2,'tp'=4] {'sp_0','sp_1'}, dimensions={0} | all-to-all | bytes 1572864 | tf_op jit(solution)/shard_map/all_to_all | solution.py:25
  51.3 1.9 collective-permute-start.4
  53.2 0.0 copy-done.2
  53.2 2.4 %collective-permute-start = (bf16[16,512]{1,0:T(8,128)(2,1)S(1)}, bf16[16,512]{1,0:T(8,128)(2,1)S(1)}, u32[]{:S(2)}, u32[]{:S(2)}) collective-permute-start(bf16[16,512]{1,0:T(8,128)(2,1)S(1)} %slice.3), channel_id=1, source_target_pairs={{0,4},{4,8},{8,12},{12,16},{16,20},{20,24},{24,28},{28,32},{32,36}... | collective-permute-start | bytes 49160 | tf_op jit(solution)/shard_map/ppermute | solution.py:344
  55.6 0.8 collective-permute-done
  56.5 3.4 %collective-permute-start.1 = (bf16[544,512]{1,0:T(8,128)(2,1)S(1)}, bf16[544,512]{1,0:T(8,128)(2,1)S(1)}, u32[]{:S(2)}, u32[]{:S(2)}) collective-permute-start(bf16[544,512]{1,0:T(8,128)(2,1)S(1)} %pad_maximum_fusion.x0), channel_id=1, source_target_pairs={{0,1},{1,2},{2,3},{3,0},{4,5},{5,6},{6,7},{7,4},{8,9},{9,10},{10,1... | collective-permute-start | bytes 1671176 | tf_op jit(solution)/shard_map/ppermute | solution.py:350
  59.9 3.0 %collective-permute-start.2 = (bf16[544,512]{1,0:T(8,128)(2,1)S(1)}, bf16[544,512]{1,0:T(8,128)(2,1)S(1)}, u32[]{:S(2)}, u32[]{:S(2)}) collective-permute-start(bf16[544,512]{1,0:T(8,128)(2,1)S(1)} %pad_maximum_fusion.x0), channel_id=1, source_target_pairs={{0,2},{1,3},{2,0},{3,1},{4,6},{5,7},{6,4},{7,5},{8,10},{9,11},{10,... | collective-permute-start | bytes 1671176 | tf_op jit(solution)/shard_map/ppermute | solution.py:350
  62.9 4.1 %collective-permute-start.3 = (bf16[544,512]{1,0:T(8,128)(2,1)S(1)}, bf16[544,512]{1,0:T(8,128)(2,1)}, u32[]{:S(2)}, u32[]{:S(2)}) collective-permute-start(bf16[544,512]{1,0:T(8,128)(2,1)S(1)} %pad_maximum_fusion.x0), channel_id=1, source_target_pairs={{0,3},{1,0},{2,1},{3,2},{4,7},{5,4},{6,5},{7,6},{8,11},{9,8},{10,9... | collective-permute-start | bytes 1671176 | tf_op jit(solution)/shard_map/ppermute | solution.py:350
  67.0 0.0 copy-done.13
  67.1 0.0 copy-done.7
  67.1 0.0 copy-done.12
  67.1 0.1 broadcast_in_dim.49
  67.2 0.1 broadcast_in_dim_reshape.3
  67.3 0.0 copy-done.10
  67.3 0.6 pad.36.extra
  67.9 0.1 broadcast_in_dim.48
  68.0 0.1 broadcast_in_dim.47
  68.1 2.4 %concatenate.18.params = f32[32,384]{1,0:T(8,128)} concatenate(f32[4,384]{1,0:T(4,128)S(1)} %select_maximum_fusion, f32[4,384]{1,0:T(4,128)S(1)} %pad.30, f32[8,384]{1,0:T(8,128)S(1)} %broadcast_in_dim.47, f32[8,384]{1,0:T(8,128)S(1)} %broadcast_in_dim.48, f32[1,384]{1,0:T(1,128)S(1)} %pad.33, f32[1,384]{1,0:T(1,128)S(1)} %pad.34, f32[1,384]{1,0:T(1,128)S(1)} %pad.35, ...), dimensions={0} | concatenate | bytes 98304 | tf_op jit(solution)/shard_map/concatenate | solution.py:361
  70.5 3.4 %collective-permute-done.1.x1 = bf16[544,512]{1,0:T(8,128)(2,1)S(1)} collective-permute-done((bf16[544,512]{1,0:T(8,128)(2,1)S(1)}, bf16[544,512]{1,0:T(8,128)(2,1)S(1)}, u32[]{:S(2)}, u32[]{:S(2)}) %collective-permute-start.1) | collective-permute-done | bytes 557088 | tf_op jit(solution)/shard_map/ppermute | solution.py:350
  73.9 5.0 %collective-permute-done.2.x2 = bf16[544,512]{1,0:T(8,128)(2,1)S(1)} collective-permute-done((bf16[544,512]{1,0:T(8,128)(2,1)S(1)}, bf16[544,512]{1,0:T(8,128)(2,1)S(1)}, u32[]{:S(2)}, u32[]{:S(2)}) %collective-permute-start.2) | collective-permute-done | bytes 557088 | tf_op jit(solution)/shard_map/ppermute | solution.py:350
  78.9 0.8 copy-done.4
  79.7 10.6 %collective-permute-done.3.x3 = bf16[544,512]{1,0:T(8,128)(2,1)} collective-permute-done((bf16[544,512]{1,0:T(8,128)(2,1)S(1)}, bf16[544,512]{1,0:T(8,128)(2,1)}, u32[]{:S(2)}, u32[]{:S(2)}) %collective-permute-start.3) | collective-permute-done | bytes 557088 | tf_op jit(solution)/shard_map/ppermute | solution.py:350
  90.3 2.5 %shard_map.190.normed = bf16[4,528,512]{2,1,0:T(8,128)(2,1)S(1)} custom-call(bf16[544,512]{1,0:T(8,128)(2,1)} %copy-done.1, bf16[544,512]{1,0:T(8,128)(2,1)} %copy-done.3, bf16[544,512]{1,0:T(8,128)(2,1)} %copy-done.4, bf16[544,512]{1,0:T(8,128)(2,1)} %collective-permute-done.3.x3), custom_call_target="tpu_custom_call" | custom-call | flops 1000000 | bytes 2228224 | tf_op jit(solution)/shard_map/pallas_call | solution.py:271
  92.8 0.0 collective-permute-done.4.other
  92.9 5.4 %shard_map.192 = (bf16[512,256]{1,0:T(8,128)(2,1)}, bf16[512,128]{1,0:T(8,128)(2,1)}, f32[8,512]{1,0:T(8,128)}, f32[8,512]{1,0:T(8,128)}, bf16[80,256]{1,0:T(8,128)(2,1)S(1)}) custom-call(bf16[4,528,512]{2,1,0:T(8,128)(2,1)S(1)} %shard_map.190.normed, bf16[64,16,384]{2,1,0:T(8,128)(2,1)S(1)} %all_to_all.20.mine, ...), custom_call_target="tpu_custom_call" | custom-call | flops 830472192 | bytes 3801088 | tf_op jit(solution)/shard_map/pallas_call | solution.py:271
  98.3 18.0 %all-gather = bf16[1280,256]{1,0:T(8,128)(2,1)S(1)} all-gather(bf16[80,256]{1,0:T(8,128)(2,1)S(1)} %get-tuple-element.23), channel_id=2, replica_groups=mesh['sp_0'=8,'sp_1'=8,'sp_2'=2,'tp'=4] {'sp_1','sp_2'}, dimensions={0}, use_global_device_ids=true | all-gather | bytes 696320 | tf_op jit(solution)/shard_map/all_gather | solution.py:391
  116.3 0.8 shard_map.194
  117.1 0.7 broadcast_in_dim.55
  117.9 4.6 %all-to-all-start.1 = ((bf16[8,80,256]{2,1,0:T(8,128)(2,1)}), bf16[8,80,256]{2,1,0:T(8,128)(2,1)S(1)}, u32[]{:S(2)}, u32[]{:S(2)}) async-start(bf16[8,80,256]{2,1,0:T(8,128)(2,1)} %broadcast_in_dim.55), calls=%async_computation.1 | async-start | bytes 655360 | tf_op jit(solution)/shard_map/all_to_all | solution.py:25
  122.5 3.3 %shard_map.193 = (f32[40,128,128]{2,1,0:T(8,128)}, bf16[512,256]{1,0:T(8,128)(2,1)}) custom-call(bf16[512,256]{1,0:T(8,128)(2,1)} %get-tuple-element.17.value, f32[8,512]{1,0:T(8,128)} %get-tuple-element.19.cum, f32[8,512]{1,0:T(8,128)} %get-tuple-element.20.step), custom_call_target="tpu_custom_call" | custom-call | flops 10000000 | bytes 294912 | tf_op jit(solution)/shard_map/pallas_call | solution.py:271
  125.8 10.5 %all-to-all-done.1.planes = bf16[8,80,256]{2,1,0:T(8,128)(2,1)S(1)} async-done(((bf16[8,80,256]{2,1,0:T(8,128)(2,1)}), bf16[8,80,256]{2,1,0:T(8,128)(2,1)S(1)}, u32[]{:S(2)}, u32[]{:S(2)}) %all-to-all-start.1) | async-done | bytes 327712 | tf_op jit(solution)/shard_map/all_to_all | solution.py:25
  136.3 7.3 %shard_map.195 = (bf16[512,256]{1,0:T(8,128)(2,1)S(1)}, f32[1,512]{1,0:T(1,128)S(1)}) custom-call(bf16[4,528,512]{2,1,0:T(8,128)(2,1)} %copy-done, bf16[2048,1152]{1,0:T(8,128)(2,1)} %all-gather.3.cloned.1.call-done.weight, bf16[512,256]{1,0:T(8,128)(2,1)} %get-tuple-element.17.value, bf16[512,128]{1,0:T(8,128)(2,1)} %get-tuple-element.18.key, ...), custom_call_target="tpu_custom_call" | custom-call | flops 830472192 | bytes 10625024 | tf_op jit(solution)/shard_map/pallas_call | solution.py:271
  143.6 0.6 broadcast_in_dim.56
  144.2 4.3 %all-to-all-start.2 = ((f32[4,1,512]{2,1,0:T(1,128)}), f32[4,1,512]{2,1,0:T(1,128)S(1)}, u32[]{:S(2)}, u32[]{:S(2)}) async-start(f32[4,1,512]{2,1,0:T(1,128)} %broadcast_in_dim.56), calls=%async_computation.2 | async-start | bytes 16384 | tf_op jit(solution)/shard_map/all_to_all | solution.py:25
  148.5 4.8 %shard_map.191.pool = bf16[512,256]{1,0:T(8,128)(2,1)} custom-call(bf16[4,528,512]{2,1,0:T(8,128)(2,1)} %copy-done, bf16[2048,1152]{1,0:T(8,128)(2,1)} %all-gather.3.cloned.1.call-done.weight, f32[32,384]{1,0:T(8,128)} %concatenate.18.params, bf16[256,256]{1,0:T(8,128)(2,1)} %bitcast.10), custom_call_target="tpu_custom_call" | custom-call | flops 553648128 | bytes 7061504 | tf_op jit(solution)/shard_map/pallas_call | solution.py:271
  153.3 0.0 all-to-all-done.2.squares
  153.3 3.0 %shard_map.196 = bf16[4,512,512]{2,1,0:T(8,128)(2,1)S(1)} custom-call(bf16[512,256]{1,0:T(8,128)(2,1)} %shard_map.191.pool, bf16[512,256]{1,0:T(8,128)(2,1)S(1)} %get-tuple-element.27.rows, bf16[2048,1152]{1,0:T(8,128)(2,1)} %all-gather.3.cloned.1.call-done.weight, f32[4,1,512]{2,1,0:T(1,128)S(1)} %all-to-all-done.2.squares), custom_call_target="tpu_custom_call" | custom-call | flops 1073741824 | bytes 5251072 | tf_op jit(solution)/shard_map/pallas_call | solution.py:271
  156.3 29.1 %all_to_all.21 = bf16[4,512,512]{2,1,0:T(8,128)(2,1)S(1)} all-to-all(bf16[4,512,512]{2,1,0:T(8,128)(2,1)S(1)} %shard_map.196), channel_id=1, replica_groups=mesh['sp_0'=8,'sp_1'=8,'sp_2'=2,'tp'=4] {'tp'}, dimensions={0} | all-to-all | bytes 4194304 | tf_op jit(solution)/shard_map/all_to_all | solution.py:457
  185.5 1.2 reduce_sum.12
  (37 shorter events, 0.1 us)
Async XLA Ops:
  6.5 46.7 %copy-start.2 = (bf16[512,512]{1,0:T(8,128)(2,1)S(1)}, bf16[512,512]{1,0:T(8,128)(2,1)}, u32[]{:S(2)}) copy-start(bf16[512,512]{1,0:T(8,128)(2,1)} %param.20) | copy-start | bytes 1572868
  6.5 49.9 %copy-start.9 = (bf16[512]{0:T(512)(128)(2,1)S(1)}, bf16[512]{0:T(512)(128)(2,1)}, u32[]{:S(2)}) copy-start(bf16[512]{0:T(512)(128)(2,1)} %param.21) | copy-start | bytes 3076
  6.5 60.5 %copy-start.13 = (f32[4]{0:T(128)S(1)}, f32[4]{0:T(128)}, u32[]{:S(2)}) copy-start(f32[4]{0:T(128)} %param.34) | copy-start | bytes 52
  6.5 60.5 %copy-start.14 = (f32[4]{0:T(128)S(1)}, f32[4]{0:T(128)}, u32[]{:S(2)}) copy-start(f32[4]{0:T(128)} %param.33) | copy-start | bytes 52
  6.5 60.5 %copy-start.7 = (f32[4,64]{1,0:T(4,128)S(1)}, f32[4,64]{1,0:T(4,128)}, u32[]{:S(2)}) copy-start(f32[4,64]{1,0:T(4,128)} %param.32) | copy-start | bytes 3076
  6.5 60.5 %copy-start.12 = (f32[4]{0:T(128)S(1)}, f32[4]{0:T(128)}, u32[]{:S(2)}) copy-start(f32[4]{0:T(128)} %param.36) | copy-start | bytes 52
  6.6 60.7 %copy-start.10 = (f32[256]{0:T(256)S(1)}, f32[256]{0:T(256)}, u32[]{:S(2)}) copy-start(f32[256]{0:T(256)} %param.29) | copy-start | bytes 3076
  6.6 60.7 %copy-start.11 = (f32[256]{0:T(256)S(1)}, f32[256]{0:T(256)}, u32[]{:S(2)}) copy-start(f32[256]{0:T(256)} %param.37) | copy-start | bytes 3076
  6.6 60.7 %copy-start.5 = (f32[512,4]{0,1:T(4,128)S(1)}, f32[512,4]{0,1:T(4,128)}, u32[]{:S(2)}) copy-start(f32[512,4]{0,1:T(4,128)} %param.35) | copy-start | bytes 24580
  6.6 61.3 %copy-start.6 = (f32[4,256]{1,0:T(4,128)S(1)}, f32[4,256]{1,0:T(4,128)}, u32[]{:S(2)}) copy-start(f32[4,256]{1,0:T(4,128)} %param.30) | copy-start | bytes 12292
  6.6 61.3 %copy-start.8 = (f32[4,64]{1,0:T(4,128)S(1)}, f32[4,64]{1,0:T(4,128)}, u32[]{:S(2)}) copy-start(f32[4,64]{1,0:T(4,128)} %param.31) | copy-start | bytes 3076
  6.6 129.7 %all-gather.3.cloned.1.call-start = ((), (), s32[]{:S(2)}) async-start(), calls=%async_computation.4 | async-start | bytes 4755456 | tf_op jit(solution)/shard_map/all_gather | solution.py:338
  51.3 41.5 %collective-permute-start.4 = (bf16[64,16,384]{2,1,0:T(8,128)(2,1)S(1)}, bf16[64,16,384]{2,1,0:T(8,128)(2,1)}, u32[]{:S(2)}, u32[]{:S(2)}) collective-permute-start(bf16[64,16,384]{2,1,0:T(8,128)(2,1)S(1)} %all_to_all.20.mine), channel_id=1, source_target_pairs={{0,4},{4,0},{1,5},{5,1},{2,6},{6,2},{3,7},{7,3},{8,12},{12,8},{9,1... | collective-permute-start | bytes 2359304 | tf_op jit(solution)/shard_map/ppermute | solution.py:342
  53.2 3.2 %collective-permute-start = (bf16[16,512]{1,0:T(8,128)(2,1)S(1)}, bf16[16,512]{1,0:T(8,128)(2,1)S(1)}, u32[]{:S(2)}, u32[]{:S(2)}) collective-permute-start(bf16[16,512]{1,0:T(8,128)(2,1)S(1)} %slice.3), channel_id=1, source_target_pairs={{0,4},{4,8},{8,12},{12,16},{16,20},{20,24},{24,28},{28,32},{32,36}... | collective-permute-start | bytes 49160 | tf_op jit(solution)/shard_map/ppermute | solution.py:344
  56.5 33.8 %copy-start.1 = (bf16[544,512]{1,0:T(8,128)(2,1)}, bf16[544,512]{1,0:T(8,128)(2,1)S(1)}, u32[]{:S(2)}) copy-start(bf16[544,512]{1,0:T(8,128)(2,1)S(1)} %pad_maximum_fusion.x0) | copy-start | bytes 1671172
  56.5 17.4 %collective-permute-start.1 = (bf16[544,512]{1,0:T(8,128)(2,1)S(1)}, bf16[544,512]{1,0:T(8,128)(2,1)S(1)}, u32[]{:S(2)}, u32[]{:S(2)}) collective-permute-start(bf16[544,512]{1,0:T(8,128)(2,1)S(1)} %pad_maximum_fusion.x0), channel_id=1, source_target_pairs={{0,1},{1,2},{2,3},{3,0},{4,5},{5,6},{6,7},{7,4},{8,9},{9,10},{10,1... | collective-permute-start | bytes 1671176 | tf_op jit(solution)/shard_map/ppermute | solution.py:350
  59.9 18.9 %collective-permute-start.2 = (bf16[544,512]{1,0:T(8,128)(2,1)S(1)}, bf16[544,512]{1,0:T(8,128)(2,1)S(1)}, u32[]{:S(2)}, u32[]{:S(2)}) collective-permute-start(bf16[544,512]{1,0:T(8,128)(2,1)S(1)} %pad_maximum_fusion.x0), channel_id=1, source_target_pairs={{0,2},{1,3},{2,0},{3,1},{4,6},{5,7},{6,4},{7,5},{8,10},{9,11},{10,... | collective-permute-start | bytes 1671176 | tf_op jit(solution)/shard_map/ppermute | solution.py:350
  62.9 27.4 %collective-permute-start.3 = (bf16[544,512]{1,0:T(8,128)(2,1)S(1)}, bf16[544,512]{1,0:T(8,128)(2,1)}, u32[]{:S(2)}, u32[]{:S(2)}) collective-permute-start(bf16[544,512]{1,0:T(8,128)(2,1)S(1)} %pad_maximum_fusion.x0), channel_id=1, source_target_pairs={{0,3},{1,0},{2,1},{3,2},{4,7},{5,4},{6,5},{7,6},{8,11},{9,8},{10,9... | collective-permute-start | bytes 1671176 | tf_op jit(solution)/shard_map/ppermute | solution.py:350
  73.9 5.0 %copy-start.3 = (bf16[544,512]{1,0:T(8,128)(2,1)}, bf16[544,512]{1,0:T(8,128)(2,1)S(1)}, u32[]{:S(2)}) copy-start(bf16[544,512]{1,0:T(8,128)(2,1)S(1)} %collective-permute-done.1.x1) | copy-start | bytes 1671172
  78.9 0.8 copy-start.4
  92.8 23.5 %copy-start = (bf16[4,528,512]{2,1,0:T(8,128)(2,1)}, bf16[4,528,512]{2,1,0:T(8,128)(2,1)S(1)}, u32[]{:S(2)}) copy-start(bf16[4,528,512]{2,1,0:T(8,128)(2,1)S(1)} %shard_map.190.normed) | copy-start | bytes 6488068
  117.9 18.4 %all-to-all-start.1 = ((bf16[8,80,256]{2,1,0:T(8,128)(2,1)}), bf16[8,80,256]{2,1,0:T(8,128)(2,1)S(1)}, u32[]{:S(2)}, u32[]{:S(2)}) async-start(bf16[8,80,256]{2,1,0:T(8,128)(2,1)} %broadcast_in_dim.55), calls=%async_computation.1 | async-start | bytes 655360 | tf_op jit(solution)/shard_map/all_to_all | solution.py:25
  144.2 9.1 %all-to-all-start.2 = ((f32[4,1,512]{2,1,0:T(1,128)}), f32[4,1,512]{2,1,0:T(1,128)S(1)}, u32[]{:S(2)}, u32[]{:S(2)}) async-start(f32[4,1,512]{2,1,0:T(1,128)} %broadcast_in_dim.56), calls=%async_computation.2 | async-start | bytes 16384 | tf_op jit(solution)/shard_map/all_to_all | solution.py:25
Sparse Core Ops, SparseCore 0:
  10.6 95.6 all-gather.2

commit v11 on v10

--- a/solution.py
+++ b/solution.py
@@ -156,7 +156,7 @@
                 gap = column - cum[h : h + 1, j * BLOCK : (j + 1) * BLOCK]
                 if i == j:
                     gap = jnp.where(lower, gap, -jnp.inf)
-                factors[at] = jnp.exp(gap)
+                factors[at] = jnp.exp(gap).astype(BF16)
                 at = at + 1
 
 
@@ -232,7 +232,7 @@
         for h in range(span // HEAD):
             parts = []
             for j in range(i + 1):
-                parts.append((products[j] * factors[at]).astype(BF16))
+                parts.append((products[j] * factors[at].astype(F32)).astype(BF16))
                 at = at + 1
             left = jnp.concatenate(parts, axis=1)
             results.append(dot(left, scaled[: (i + 1) * BLOCK, h * HEAD : (h + 1) * HEAD]))
@@ -403,7 +403,7 @@
         "inner",
         (value, cum, step),
         (
-            far_of((heads * blocks * (blocks + 1) // 2, BLOCK, BLOCK), F32),
+            far_of((heads * blocks * (blocks + 1) // 2, BLOCK, BLOCK), BF16),
             far_of((length, mix), BF16),
         ),
         10**7,
@@ -423,7 +423,7 @@
             pltpu.VMEM((count, rows, width), BF16),
             pltpu.VMEM((count, width, mix), BF16),
             pltpu.VMEM((count, width, BLOCK), BF16),
-            pltpu.VMEM(factors.shape, F32),
+            pltpu.VMEM(factors.shape, BF16),
             pltpu.SemaphoreType.DMA((count, 3)),
             pltpu.SemaphoreType.DMA,
         ],

time: 194 us -> 194 us (level)
  no operation moved by 1% of the time
where the time goes in v11:
time: 194 us
  blocking collectives  88.7 us (46%)
  waiting for transfers between devices  30.7 us (16%)
  Pallas kernels  26.8 us (14%)
  starting transfers between devices  23.5 us (12%)
  between operations  13.7 us (7%)
  local copies, waits for them, and re-layouts  8.04 us (4%)
  other arithmetic  2.08 us (1%)
    all_to_all x1, blocking collectives, sent_to_all(): return lax.all_to_all(copies, axis, split_axis=0, concat_axis=0, tiled=True)  41.5 us
    all_to_all x1, blocking collectives, local(): lax.all_to_all(terms, 'tp', split_axis=0, concat_axis=0, tiled=True)  29.1 us
    pallas_call x7, Pallas kernels, call(): pl.pallas_call(kernel, grid=(1,), in_specs=[specs.get(k, whole(a.shape))...  26.8 us
    ppermute x3, waiting for transfers between devices, local(): pieces.append(lax.ppermute(sent, 'tp', pairs))  19 us
    all_gather x1, blocking collectives, local(): row_pieces = lax.all_gather(payload, ('sp_1', 'sp_2'))  18.1 us
    all_to_all x2, waiting for transfers between devices, sent_to_all(): return lax.all_to_all(copies, axis, split_axis=0, concat_axis=0, tiled=True)  10.9 us
    ppermute x3, starting transfers between devices, local(): pieces.append(lax.ppermute(sent, 'tp', pairs))  10.5 us
    all_to_all x2, starting transfers between devices, sent_to_all(): return lax.all_to_all(copies, axis, split_axis=0, concat_axis=0, tiled=True)  8.72 us
  transfers between devices with their start and end apart: 8, of which 5 were waited for; matrix products, arithmetic and copies ran while one was open for 3% of the time, Pallas kernels for 9%

profile of v11, /device:TPU:2, one launch (start us, length us, event | category | flops | bytes accessed | tf_op | source)
XLA Modules:
  0.0 193.6 jit_solution(13991258294289537396)
XLA Ops:
  6.5 1.5 concatenate.16
  8.0 0.0 all-gather.3.cloned.1.call-update
  8.1 0.8 copy.21
  8.8 0.1 pad.40.clone
  8.9 0.8 maximum_maximum_fusion
  9.7 0.1 broadcast_in_dim.54
  9.8 0.0 copy-start.13
  9.8 0.0 copy-start.14
  9.8 0.0 copy-start.7
  9.8 0.0 copy-start.12
  9.8 0.0 copy-start.10
  9.8 0.0 copy-start.11
  9.9 0.0 copy-start.5
  9.9 0.0 copy-start.6
  9.9 0.0 copy-start.8
  9.9 41.5 %all_to_all.20.mine = bf16[64,16,384]{2,1,0:T(8,128)(2,1)S(1)} all-to-all(bf16[64,16,384]{2,1,0:T(8,128)(2,1)S(1)} %broadcast_in_dim.54), channel_id=1, replica_groups=mesh['sp_0'=8,'sp_1'=8,'sp_2'=2,'tp'=4] {'sp_0','sp_1'}, dimensions={0} | all-to-all | bytes 1572864 | tf_op jit(solution)/shard_map/all_to_all | solution.py:25
  51.4 1.9 collective-permute-start.4
  53.3 2.4 %collective-permute-start = (bf16[16,512]{1,0:T(8,128)(2,1)S(1)}, bf16[16,512]{1,0:T(8,128)(2,1)S(1)}, u32[]{:S(2)}, u32[]{:S(2)}) collective-permute-start(bf16[16,512]{1,0:T(8,128)(2,1)S(1)} %slice.3), channel_id=1, source_target_pairs={{0,4},{4,8},{8,12},{12,16},{16,20},{20,24},{24,28},{28,32},{32,36}... | collective-permute-start | bytes 49160 | tf_op jit(solution)/shard_map/ppermute | solution.py:344
  55.7 0.8 collective-permute-done
  56.6 3.4 %collective-permute-start.1 = (bf16[544,512]{1,0:T(8,128)(2,1)S(1)}, bf16[544,512]{1,0:T(8,128)(2,1)S(1)}, u32[]{:S(2)}, u32[]{:S(2)}) collective-permute-start(bf16[544,512]{1,0:T(8,128)(2,1)S(1)} %pad_maximum_fusion.x0), channel_id=1, source_target_pairs={{0,1},{1,2},{2,3},{3,0},{4,5},{5,6},{6,7},{7,4},{8,9},{9,10},{10,1... | collective-permute-start | bytes 1671176 | tf_op jit(solution)/shard_map/ppermute | solution.py:350
  60.0 3.0 %collective-permute-start.2 = (bf16[544,512]{1,0:T(8,128)(2,1)S(1)}, bf16[544,512]{1,0:T(8,128)(2,1)S(1)}, u32[]{:S(2)}, u32[]{:S(2)}) collective-permute-start(bf16[544,512]{1,0:T(8,128)(2,1)S(1)} %pad_maximum_fusion.x0), channel_id=1, source_target_pairs={{0,2},{1,3},{2,0},{3,1},{4,6},{5,7},{6,4},{7,5},{8,10},{9,11},{10,... | collective-permute-start | bytes 1671176 | tf_op jit(solution)/shard_map/ppermute | solution.py:350
  63.0 4.1 %collective-permute-start.3 = (bf16[544,512]{1,0:T(8,128)(2,1)S(1)}, bf16[544,512]{1,0:T(8,128)(2,1)}, u32[]{:S(2)}, u32[]{:S(2)}) collective-permute-start(bf16[544,512]{1,0:T(8,128)(2,1)S(1)} %pad_maximum_fusion.x0), channel_id=1, source_target_pairs={{0,3},{1,0},{2,1},{3,2},{4,7},{5,4},{6,5},{7,6},{8,11},{9,8},{10,9... | collective-permute-start | bytes 1671176 | tf_op jit(solution)/shard_map/ppermute | solution.py:350
  67.2 0.1 broadcast_in_dim.49
  67.2 0.1 broadcast_in_dim_reshape.3
  67.4 0.6 pad.36.extra
  68.0 0.1 broadcast_in_dim.48
  68.1 0.1 broadcast_in_dim.47
  68.1 2.4 %concatenate.18.params = f32[32,384]{1,0:T(8,128)} concatenate(f32[4,384]{1,0:T(4,128)S(1)} %select_maximum_fusion, f32[4,384]{1,0:T(4,128)S(1)} %pad.30, f32[8,384]{1,0:T(8,128)S(1)} %broadcast_in_dim.47, f32[8,384]{1,0:T(8,128)S(1)} %broadcast_in_dim.48, f32[1,384]{1,0:T(1,128)S(1)} %pad.33, f32[1,384]{1,0:T(1,128)S(1)} %pad.34, f32[1,384]{1,0:T(1,128)S(1)} %pad.35, ...), dimensions={0} | concatenate | bytes 98304 | tf_op jit(solution)/shard_map/concatenate | solution.py:361
  70.6 3.4 %collective-permute-done.1.x1 = bf16[544,512]{1,0:T(8,128)(2,1)S(1)} collective-permute-done((bf16[544,512]{1,0:T(8,128)(2,1)S(1)}, bf16[544,512]{1,0:T(8,128)(2,1)S(1)}, u32[]{:S(2)}, u32[]{:S(2)}) %collective-permute-start.1) | collective-permute-done | bytes 557088 | tf_op jit(solution)/shard_map/ppermute | solution.py:350
  74.0 5.0 %collective-permute-done.2.x2 = bf16[544,512]{1,0:T(8,128)(2,1)S(1)} collective-permute-done((bf16[544,512]{1,0:T(8,128)(2,1)S(1)}, bf16[544,512]{1,0:T(8,128)(2,1)S(1)}, u32[]{:S(2)}, u32[]{:S(2)}) %collective-permute-start.2) | collective-permute-done | bytes 557088 | tf_op jit(solution)/shard_map/ppermute | solution.py:350
  78.9 0.9 copy-done.4
  79.8 10.6 %collective-permute-done.3.x3 = bf16[544,512]{1,0:T(8,128)(2,1)} collective-permute-done((bf16[544,512]{1,0:T(8,128)(2,1)S(1)}, bf16[544,512]{1,0:T(8,128)(2,1)}, u32[]{:S(2)}, u32[]{:S(2)}) %collective-permute-start.3) | collective-permute-done | bytes 557088 | tf_op jit(solution)/shard_map/ppermute | solution.py:350
  90.4 2.5 %shard_map.190.normed = bf16[4,528,512]{2,1,0:T(8,128)(2,1)S(1)} custom-call(bf16[544,512]{1,0:T(8,128)(2,1)} %copy-done.1, bf16[544,512]{1,0:T(8,128)(2,1)} %copy-done.3, bf16[544,512]{1,0:T(8,128)(2,1)} %copy-done.4, bf16[544,512]{1,0:T(8,128)(2,1)} %collective-permute-done.3.x3), custom_call_target="tpu_custom_call" | custom-call | flops 1000000 | bytes 2228224 | tf_op jit(solution)/shard_map/pallas_call | solution.py:271
  92.9 0.0 collective-permute-done.4.other
  92.9 5.4 %shard_map.192 = (bf16[512,256]{1,0:T(8,128)(2,1)}, bf16[512,128]{1,0:T(8,128)(2,1)}, f32[8,512]{1,0:T(8,128)}, f32[8,512]{1,0:T(8,128)}, bf16[80,256]{1,0:T(8,128)(2,1)S(1)}) custom-call(bf16[4,528,512]{2,1,0:T(8,128)(2,1)S(1)} %shard_map.190.normed, bf16[64,16,384]{2,1,0:T(8,128)(2,1)S(1)} %all_to_all.20.mine, ...), custom_call_target="tpu_custom_call" | custom-call | flops 830472192 | bytes 3801088 | tf_op jit(solution)/shard_map/pallas_call | solution.py:271
  98.3 18.1 %all-gather = bf16[1280,256]{1,0:T(8,128)(2,1)S(1)} all-gather(bf16[80,256]{1,0:T(8,128)(2,1)S(1)} %get-tuple-element.23), channel_id=2, replica_groups=mesh['sp_0'=8,'sp_1'=8,'sp_2'=2,'tp'=4] {'sp_1','sp_2'}, dimensions={0}, use_global_device_ids=true | all-gather | bytes 696320 | tf_op jit(solution)/shard_map/all_gather | solution.py:391
  116.5 0.8 shard_map.194
  117.3 0.7 broadcast_in_dim.55
  118.1 4.5 %all-to-all-start.1 = ((bf16[8,80,256]{2,1,0:T(8,128)(2,1)}), bf16[8,80,256]{2,1,0:T(8,128)(2,1)S(1)}, u32[]{:S(2)}, u32[]{:S(2)}) async-start(bf16[8,80,256]{2,1,0:T(8,128)(2,1)} %broadcast_in_dim.55), calls=%async_computation.1 | async-start | bytes 655360 | tf_op jit(solution)/shard_map/all_to_all | solution.py:25
  122.6 2.9 %shard_map.193 = (bf16[40,128,128]{2,1,0:T(8,128)(2,1)}, bf16[512,256]{1,0:T(8,128)(2,1)}) custom-call(bf16[512,256]{1,0:T(8,128)(2,1)} %get-tuple-element.17.value, f32[8,512]{1,0:T(8,128)} %get-tuple-element.19.cum, f32[8,512]{1,0:T(8,128)} %get-tuple-element.20.step), custom_call_target="tpu_custom_call" | custom-call | flops 10000000 | bytes 294912 | tf_op jit(solution)/shard_map/pallas_call | solution.py:271
  125.5 10.9 %all-to-all-done.1.planes = bf16[8,80,256]{2,1,0:T(8,128)(2,1)S(1)} async-done(((bf16[8,80,256]{2,1,0:T(8,128)(2,1)}), bf16[8,80,256]{2,1,0:T(8,128)(2,1)S(1)}, u32[]{:S(2)}, u32[]{:S(2)}) %all-to-all-start.1) | async-done | bytes 327712 | tf_op jit(solution)/shard_map/all_to_all | solution.py:25
  136.4 7.3 %shard_map.195 = (bf16[512,256]{1,0:T(8,128)(2,1)S(1)}, f32[1,512]{1,0:T(1,128)S(1)}) custom-call(bf16[4,528,512]{2,1,0:T(8,128)(2,1)} %copy-done, bf16[2048,1152]{1,0:T(8,128)(2,1)} %all-gather.3.cloned.1.call-done.weight, bf16[512,256]{1,0:T(8,128)(2,1)} %get-tuple-element.17.value, bf16[512,128]{1,0:T(8,128)(2,1)} %get-tuple-element.18.key, ...), custom_call_target="tpu_custom_call" | custom-call | flops 830472192 | bytes 9314304 | tf_op jit(solution)/shard_map/pallas_call | solution.py:271
  143.7 0.6 broadcast_in_dim.56
  144.3 4.2 %all-to-all-start.2 = ((f32[4,1,512]{2,1,0:T(1,128)}), f32[4,1,512]{2,1,0:T(1,128)S(1)}, u32[]{:S(2)}, u32[]{:S(2)}) async-start(f32[4,1,512]{2,1,0:T(1,128)} %broadcast_in_dim.56), calls=%async_computation.2 | async-start | bytes 16384 | tf_op jit(solution)/shard_map/all_to_all | solution.py:25
  148.5 4.8 %shard_map.191.pool = bf16[512,256]{1,0:T(8,128)(2,1)} custom-call(bf16[4,528,512]{2,1,0:T(8,128)(2,1)} %copy-done, bf16[2048,1152]{1,0:T(8,128)(2,1)} %all-gather.3.cloned.1.call-done.weight, f32[32,384]{1,0:T(8,128)} %concatenate.18.params, bf16[256,256]{1,0:T(8,128)(2,1)} %bitcast.10), custom_call_target="tpu_custom_call" | custom-call | flops 553648128 | bytes 7061504 | tf_op jit(solution)/shard_map/pallas_call | solution.py:271
  153.4 3.0 %shard_map.196 = bf16[4,512,512]{2,1,0:T(8,128)(2,1)S(1)} custom-call(bf16[512,256]{1,0:T(8,128)(2,1)} %shard_map.191.pool, bf16[512,256]{1,0:T(8,128)(2,1)S(1)} %get-tuple-element.27.rows, bf16[2048,1152]{1,0:T(8,128)(2,1)} %all-gather.3.cloned.1.call-done.weight, f32[4,1,512]{2,1,0:T(1,128)S(1)} %all-to-all-done.2.squares), custom_call_target="tpu_custom_call" | custom-call | flops 1073741824 | bytes 5251072 | tf_op jit(solution)/shard_map/pallas_call | solution.py:271
  156.4 29.1 %all_to_all.21 = bf16[4,512,512]{2,1,0:T(8,128)(2,1)S(1)} all-to-all(bf16[4,512,512]{2,1,0:T(8,128)(2,1)S(1)} %shard_map.196), channel_id=1, replica_groups=mesh['sp_0'=8,'sp_1'=8,'sp_2'=2,'tp'=4] {'tp'}, dimensions={0} | all-to-all | bytes 4194304 | tf_op jit(solution)/shard_map/all_to_all | solution.py:457
  185.5 1.2 reduce_sum.12
  (37 shorter events, 0.1 us)
Async XLA Ops:
  6.5 46.7 %copy-start.2 = (bf16[512,512]{1,0:T(8,128)(2,1)S(1)}, bf16[512,512]{1,0:T(8,128)(2,1)}, u32[]{:S(2)}) copy-start(bf16[512,512]{1,0:T(8,128)(2,1)} %param.20) | copy-start | bytes 1572868
  6.5 50.0 %copy-start.9 = (bf16[512]{0:T(512)(128)(2,1)S(1)}, bf16[512]{0:T(512)(128)(2,1)}, u32[]{:S(2)}) copy-start(bf16[512]{0:T(512)(128)(2,1)} %param.21) | copy-start | bytes 3076
  6.5 129.9 %all-gather.3.cloned.1.call-start = ((), (), s32[]{:S(2)}) async-start(), calls=%async_computation.4 | async-start | bytes 4755456 | tf_op jit(solution)/shard_map/all_gather | solution.py:338
  9.8 57.3 %copy-start.13 = (f32[4]{0:T(128)S(1)}, f32[4]{0:T(128)}, u32[]{:S(2)}) copy-start(f32[4]{0:T(128)} %param.34) | copy-start | bytes 52
  9.8 57.3 %copy-start.14 = (f32[4]{0:T(128)S(1)}, f32[4]{0:T(128)}, u32[]{:S(2)}) copy-start(f32[4]{0:T(128)} %param.33) | copy-start | bytes 52
  9.8 57.3 %copy-start.7 = (f32[4,64]{1,0:T(4,128)S(1)}, f32[4,64]{1,0:T(4,128)}, u32[]{:S(2)}) copy-start(f32[4,64]{1,0:T(4,128)} %param.32) | copy-start | bytes 3076
  9.8 57.3 %copy-start.12 = (f32[4]{0:T(128)S(1)}, f32[4]{0:T(128)}, u32[]{:S(2)}) copy-start(f32[4]{0:T(128)} %param.36) | copy-start | bytes 52
  9.8 57.5 %copy-start.10 = (f32[256]{0:T(256)S(1)}, f32[256]{0:T(256)}, u32[]{:S(2)}) copy-start(f32[256]{0:T(256)} %param.29) | copy-start | bytes 3076
  9.8 57.5 %copy-start.11 = (f32[256]{0:T(256)S(1)}, f32[256]{0:T(256)}, u32[]{:S(2)}) copy-start(f32[256]{0:T(256)} %param.37) | copy-start | bytes 3076
  9.9 57.5 %copy-start.5 = (f32[512,4]{0,1:T(4,128)S(1)}, f32[512,4]{0,1:T(4,128)}, u32[]{:S(2)}) copy-start(f32[512,4]{0,1:T(4,128)} %param.35) | copy-start | bytes 24580
  9.9 58.1 %copy-start.6 = (f32[4,256]{1,0:T(4,128)S(1)}, f32[4,256]{1,0:T(4,128)}, u32[]{:S(2)}) copy-start(f32[4,256]{1,0:T(4,128)} %param.30) | copy-start | bytes 12292
  9.9 58.1 %copy-start.8 = (f32[4,64]{1,0:T(4,128)S(1)}, f32[4,64]{1,0:T(4,128)}, u32[]{:S(2)}) copy-start(f32[4,64]{1,0:T(4,128)} %param.31) | copy-start | bytes 3076
  51.4 41.5 %collective-permute-start.4 = (bf16[64,16,384]{2,1,0:T(8,128)(2,1)S(1)}, bf16[64,16,384]{2,1,0:T(8,128)(2,1)}, u32[]{:S(2)}, u32[]{:S(2)}) collective-permute-start(bf16[64,16,384]{2,1,0:T(8,128)(2,1)S(1)} %all_to_all.20.mine), channel_id=1, source_target_pairs={{0,4},{4,0},{1,5},{5,1},{2,6},{6,2},{3,7},{7,3},{8,12},{12,8},{9,1... | collective-permute-start | bytes 2359304 | tf_op jit(solution)/shard_map/ppermute | solution.py:342
  53.3 3.2 %collective-permute-start = (bf16[16,512]{1,0:T(8,128)(2,1)S(1)}, bf16[16,512]{1,0:T(8,128)(2,1)S(1)}, u32[]{:S(2)}, u32[]{:S(2)}) collective-permute-start(bf16[16,512]{1,0:T(8,128)(2,1)S(1)} %slice.3), channel_id=1, source_target_pairs={{0,4},{4,8},{8,12},{12,16},{16,20},{20,24},{24,28},{28,32},{32,36}... | collective-permute-start | bytes 49160 | tf_op jit(solution)/shard_map/ppermute | solution.py:344
  56.6 33.8 %copy-start.1 = (bf16[544,512]{1,0:T(8,128)(2,1)}, bf16[544,512]{1,0:T(8,128)(2,1)S(1)}, u32[]{:S(2)}) copy-start(bf16[544,512]{1,0:T(8,128)(2,1)S(1)} %pad_maximum_fusion.x0) | copy-start | bytes 1671172
  56.6 17.4 %collective-permute-start.1 = (bf16[544,512]{1,0:T(8,128)(2,1)S(1)}, bf16[544,512]{1,0:T(8,128)(2,1)S(1)}, u32[]{:S(2)}, u32[]{:S(2)}) collective-permute-start(bf16[544,512]{1,0:T(8,128)(2,1)S(1)} %pad_maximum_fusion.x0), channel_id=1, source_target_pairs={{0,1},{1,2},{2,3},{3,0},{4,5},{5,6},{6,7},{7,4},{8,9},{9,10},{10,1... | collective-permute-start | bytes 1671176 | tf_op jit(solution)/shard_map/ppermute | solution.py:350
  60.0 18.9 %collective-permute-start.2 = (bf16[544,512]{1,0:T(8,128)(2,1)S(1)}, bf16[544,512]{1,0:T(8,128)(2,1)S(1)}, u32[]{:S(2)}, u32[]{:S(2)}) collective-permute-start(bf16[544,512]{1,0:T(8,128)(2,1)S(1)} %pad_maximum_fusion.x0), channel_id=1, source_target_pairs={{0,2},{1,3},{2,0},{3,1},{4,6},{5,7},{6,4},{7,5},{8,10},{9,11},{10,... | collective-permute-start | bytes 1671176 | tf_op jit(solution)/shard_map/ppermute | solution.py:350
  63.0 27.4 %collective-permute-start.3 = (bf16[544,512]{1,0:T(8,128)(2,1)S(1)}, bf16[544,512]{1,0:T(8,128)(2,1)}, u32[]{:S(2)}, u32[]{:S(2)}) collective-permute-start(bf16[544,512]{1,0:T(8,128)(2,1)S(1)} %pad_maximum_fusion.x0), channel_id=1, source_target_pairs={{0,3},{1,0},{2,1},{3,2},{4,7},{5,4},{6,5},{7,6},{8,11},{9,8},{10,9... | collective-permute-start | bytes 1671176 | tf_op jit(solution)/shard_map/ppermute | solution.py:350
  74.0 5.0 %copy-start.3 = (bf16[544,512]{1,0:T(8,128)(2,1)}, bf16[544,512]{1,0:T(8,128)(2,1)S(1)}, u32[]{:S(2)}) copy-start(bf16[544,512]{1,0:T(8,128)(2,1)S(1)} %collective-permute-done.1.x1) | copy-start | bytes 1671172
  78.9 0.9 copy-start.4
  92.9 5.4 %copy-start = (bf16[4,528,512]{2,1,0:T(8,128)(2,1)}, bf16[4,528,512]{2,1,0:T(8,128)(2,1)S(1)}, u32[]{:S(2)}) copy-start(bf16[4,528,512]{2,1,0:T(8,128)(2,1)S(1)} %shard_map.190.normed) | copy-start | bytes 6488068
  118.1 18.3 %all-to-all-start.1 = ((bf16[8,80,256]{2,1,0:T(8,128)(2,1)}), bf16[8,80,256]{2,1,0:T(8,128)(2,1)S(1)}, u32[]{:S(2)}, u32[]{:S(2)}) async-start(bf16[8,80,256]{2,1,0:T(8,128)(2,1)} %broadcast_in_dim.55), calls=%async_computation.1 | async-start | bytes 655360 | tf_op jit(solution)/shard_map/all_to_all | solution.py:25
  144.3 9.0 %all-to-all-start.2 = ((f32[4,1,512]{2,1,0:T(1,128)}), f32[4,1,512]{2,1,0:T(1,128)S(1)}, u32[]{:S(2)}, u32[]{:S(2)}) async-start(f32[4,1,512]{2,1,0:T(1,128)} %broadcast_in_dim.56), calls=%async_computation.2 | async-start | bytes 16384 | tf_op jit(solution)/shard_map/all_to_all | solution.py:25
Sparse Core Ops, SparseCore 0:
  10.5 95.7 all-gather.2
